TPU v7x, 128 devices: a whole 4x4x4 slice. The times are simulated.
128 devices in a mesh: sp: 16 (over z, y), tp: 8 (over x, core).
Axes of the slice: x: 4, y: 4, z: 4, core: 2. Of those that a mesh axis runs over, the one named last changes fastest.
Arguments:
- gate_branch: bfloat16 [12288, 1024], P('sp', 'tp'), may hold values from -6 to 6
- recur_input: bfloat16 [12288, 1024], P('sp', 'tp'), may hold values from -6 to 6
- doc_ids: int32 [12288], P('sp'), may hold values from 0 to 7, never falling along the last dimension, each value on 1 to 4608 neighbouring positions
- conv_taps: bfloat16 [4, 1024], P(None, 'tp'), may hold values from -3 to 3
- gate_map: bfloat16 [16, 64, 64], P('tp'), may hold values from -0.75 to 0.75
- input_map: bfloat16 [16, 64, 64], P('tp'), may hold values from -0.75 to 0.75
- decay_level: float32 [1024], P('tp'), may hold values from 4.8 to 12.3
- decay_extra: float32 [12288, 1024], P('sp', 'tp'), may hold values from -2.1 to -1.9e-05
- out_weight: bfloat16 [1024, 2048], P(None, 'tp'), may hold values from -0.7875 to 0.7875
- residual: bfloat16 [12288, 2048], P('sp', 'tp'), may hold values from -44 to 44
- mix_gain: float32 [2048], P('tp'), may hold values from 0.1 to 1.9
- pre_gain: float32 [2048], P('tp'), may hold values from 0.1 to 1.9
- ffn_gain: float32 [2048], P('tp'), may hold values from 0.1 to 1.9
- gate_weight: bfloat16 [2048, 5632], P('sp', 'tp'), may hold values from -0.125 to 0.125
- up_weight: bfloat16 [2048, 5632], P('sp', 'tp'), may hold values from -0.125 to 0.125
- down_weight: bfloat16 [5632, 2048], P('tp', 'sp'), may hold values from -0.33579113 to 0.33579113
Outputs:
- layer_out: bfloat16 [12288, 2048], P('sp', 'tp')
Inputs may be any that keep to these rules, and one draw needn't show every extreme that they name: `doc_ids`: document numbers start at 0 and never fall along the sequence; a document has 1 to 4608 positions, and one has exactly that many.
All inputs are finite; a program needn't handle non-finite values.
Results may differ from a plain program's by a relative error of at most 0.013.
Values may be sent and summed in bfloat16 or wider, within the bound.
No kernel may reach another device: no remote copies, remote signals or barrier semaphores. Data moves between devices by JAX's collectives and lax.ppermute only.
A program may use at most 64 MiB of HBM per device.

v0:
```python
import math

import jax
import jax.numpy as jnp
from jax import lax
from jax.sharding import Mesh
from jax.sharding import PartitionSpec as P

D = 2048
TP = ("tp_0", "tp_1")


epsilon = 1e-06
gate_power = 8.0


def in_one_piece(arrays, axis, dim, along):
    both = jnp.concatenate(arrays, axis=along)
    out, at, finished = (lax.all_gather(both, axis, axis=dim, tiled=True), 0, [])
    for a in arrays:
        finished.append(lax.slice_in_dim(out, at, at + a.shape[along], axis=along))
        at += a.shape[along]
    return tuple(finished)


def passed_along(block, axis, distance):
    devices = range(lax.axis_size(axis))
    route = [(i - distance, i) for i in devices if i - distance in devices]
    return lax.ppermute(block, axis, route)


def from_everyone(shard, axis):
    count = lax.axis_size(axis)
    return lax.all_to_all(
        jnp.broadcast_to(shard[None], (count, *shard.shape)), axis, 0, 0, tiled=True
    )


def collected_together(shard, axis):
    leaves = jax.tree.leaves(shard)
    order = sorted(range(len(leaves)), key=lambda k: -leaves[k].size)
    width = (1, *leaves[order[0]].shape)[-1]
    lines = [
        jnp.pad(leaves[k].reshape(-1), (0, -leaves[k].size % width)).reshape(-1, width)
        for k in order
    ]
    both, at, found = (from_everyone(jnp.concatenate(lines), axis), 0, {})
    for k, line in zip(order, lines):
        share = both[:, at : at + len(line)].reshape(len(both), -1)
        found[k] = share[:, : leaves[k].size].reshape(-1, *leaves[k].shape)
        at += len(line)
    numbers = iter(range(len(leaves)))
    return jax.tree.map(lambda _: found[next(numbers)], shard)


def combined_pairwise(pieces, combine):
    while len(jax.tree.leaves(pieces)[0]) > 1:
        pieces = jax.vmap(combine)(
            *(jax.tree.map(lambda part: part[side::2], pieces) for side in (0, 1))
        )
    return jax.tree.map(lambda part: part[0], pieces)


def carried_in(shard, axis, combine, identity):
    count, here = (lax.axis_size(axis), lax.axis_index(axis))
    passed = jnp.arange(count) < here

    def kept(part, zero, own):
        part = jnp.where(
            passed.reshape(-1, *(1 for _ in own.shape)), part, jnp.asarray(zero, own.dtype)
        )
        return part

    pieces = collected_together(shard, axis)
    return combined_pairwise(jax.tree.map(kept, pieces, identity, shard), combine)


def joined_along(blocks, dim):
    blocks = jnp.moveaxis(blocks, 0, dim)
    shape = blocks.shape
    return blocks.reshape(*shape[:dim], shape[dim] * shape[dim + 1], *shape[dim + 2 :])


def gathered_by_axis(shard, axes, dim):
    far, near = axes
    blocks = from_everyone(from_everyone(shard, far), near)
    return joined_along(blocks.swapaxes(0, 1).reshape(-1, *shard.shape), dim)


def taken_together(shard, axis):
    everything = from_everyone(shard, axis)
    return jnp.sum(everything, axis=0)


def combine(earlier, latter):
    return (earlier[0] * latter[0], latter[0] * earlier[1] + latter[1])


def block_recurrence(log_decay, driven, doc_ids, before_ids):
    tok_rows, local_width = log_decay.shape
    block_rows = math.gcd(tok_rows, 128)
    block_count = tok_rows // block_rows
    log_blocks = log_decay.reshape(block_count, block_rows, local_width)
    drive_blocks = driven.reshape(block_count, block_rows, local_width)
    id_blocks = doc_ids.reshape(block_count, block_rows)
    lower = jnp.arange(block_rows)[:, None] >= jnp.arange(block_rows)[None, :]

    def step(carry, pieces):
        prod_carry, state_carry = carry
        logs, drives, ids, before = pieces
        cumulative = jnp.cumsum(logs, axis=0)
        linked = jnp.logical_and(lower, ids[:, None] == ids[None, :])[:, :, None]
        spread = jnp.where(linked, cumulative[:, None, :] - cumulative[None, :, :], 0.0)
        weights = jnp.where(linked, jnp.exp(spread), 0.0)
        local = jnp.einsum("ijc,jc->ic", weights, drives)
        reach = jnp.exp(cumulative) * (ids == before).astype(jnp.float32)[:, None]
        block_states = local + reach * state_carry[None, :]
        block_prods = reach * prod_carry[None, :]
        return ((block_prods[-1], block_states[-1]), (block_prods, block_states))

    start = (jnp.ones((local_width,), jnp.float32), jnp.zeros((local_width,), jnp.float32))
    ends, outputs = lax.scan(step, start, (log_blocks, drive_blocks, id_blocks, before_ids))
    return (
        ends,
        outputs[0].reshape(tok_rows, local_width),
        outputs[1].reshape(tok_rows, local_width),
    )


def body(
    gate_branch,
    recur_input,
    doc_ids,
    conv_taps,
    gate_map,
    input_map,
    decay_level,
    decay_extra,
    out_weight,
    residual,
    mix_gain,
    pre_gain,
    ffn_gain,
    gate_weight,
    up_weight,
    down_weight,
):
    tok_rows, local_width = recur_input.shape
    reach_rows = conv_taps.shape[0] - 1
    head_size = gate_map.shape[1]
    gate_whole, up_whole = in_one_piece((gate_weight, up_weight), "sp", 0, 1)
    down_whole = lax.all_gather(down_weight, "sp", axis=1, tiled=True)
    rim_rows, rim_ids = passed_along(
        (recur_input[tok_rows - reach_rows :], doc_ids[tok_rows - reach_rows :]), "sp", 1
    )
    padded_ids = jnp.concatenate([rim_ids, doc_ids])
    padded_rows = jnp.concatenate([rim_rows, recur_input])
    tap_weights = conv_taps.astype(jnp.float32)
    convolved = recur_input.astype(jnp.float32) * tap_weights[0]
    for offset in range(1, reach_rows + 1):
        start_row = reach_rows - offset
        same_doc = (padded_ids[start_row : start_row + tok_rows] == doc_ids).astype(jnp.float32)[
            :, None
        ]
        convolved = (
            convolved
            + same_doc
            * padded_rows[start_row : start_row + tok_rows].astype(jnp.float32)
            * tap_weights[offset]
        )
    conv_out = convolved.astype(jnp.bfloat16)
    head_rows = conv_out.reshape(tok_rows, local_width // head_size, head_size)
    recur_gate = jax.nn.sigmoid(
        jnp.einsum("thd,hde->the", head_rows, gate_map, preferred_element_type=jnp.float32).reshape(
            tok_rows, local_width
        )
    )
    input_gate = jax.nn.sigmoid(
        jnp.einsum(
            "thd,hde->the", head_rows, input_map, preferred_element_type=jnp.float32
        ).reshape(tok_rows, local_width)
    )
    log_decay = gate_power * -jax.nn.softplus(-decay_level) * recur_gate + decay_extra
    driven = jnp.sqrt(-jnp.expm1(2.0 * log_decay)) * input_gate * conv_out.astype(jnp.float32)
    block_rows = math.gcd(tok_rows, 128)
    before_ids = padded_ids[reach_rows - 1 : reach_rows - 1 + tok_rows : block_rows]
    ends, products, states = block_recurrence(log_decay, driven, doc_ids, before_ids)
    identity = (jnp.ones((local_width,), jnp.float32), jnp.zeros((local_width,), jnp.float32))
    carried = carried_in(ends, "sp", combine, identity)
    states = states + products * carried[1][None, :]
    branch = (states * jax.nn.gelu(gate_branch.astype(jnp.float32))).astype(jnp.bfloat16)
    mixed_out = jnp.dot(
        gathered_by_axis(branch, ("tp_0", "tp_1"), 1),
        out_weight,
        preferred_element_type=jnp.float32,
    ).astype(jnp.bfloat16)
    mixed_f = mixed_out.astype(jnp.float32)
    mix_square = taken_together(jnp.sum(mixed_f * mixed_f, axis=1), TP)
    stream = (
        residual.astype(jnp.float32)
        + mixed_f * lax.rsqrt(mix_square / D + epsilon)[:, None] * mix_gain
    ).astype(jnp.bfloat16)
    stream_f = stream.astype(jnp.float32)
    pre_square = taken_together(jnp.sum(stream_f * stream_f, axis=1), TP)
    normed = (stream_f * lax.rsqrt(pre_square / D + epsilon)[:, None] * pre_gain).astype(
        jnp.bfloat16
    )
    whole_normed = gathered_by_axis(normed, ("tp_0", "tp_1"), 1)
    gate_act = jnp.dot(whole_normed, gate_whole, preferred_element_type=jnp.float32)
    up_act = jnp.dot(whole_normed, up_whole, preferred_element_type=jnp.float32)
    hidden = (jax.nn.silu(gate_act) * up_act).astype(jnp.bfloat16)
    partial_value = jnp.dot(hidden, down_whole, preferred_element_type=jnp.float32)
    ffn_out = lax.psum_scatter(
        partial_value.astype(jnp.bfloat16), TP, scatter_dimension=1, tiled=True
    )
    ffn_f = ffn_out.astype(jnp.float32)
    ffn_square = taken_together(jnp.sum(ffn_f * ffn_f, axis=1), TP)
    return (stream_f + ffn_f * lax.rsqrt(ffn_square / D + epsilon)[:, None] * ffn_gain).astype(
        jnp.bfloat16
    )


def solution(mesh):
    split = Mesh(mesh.devices.reshape(mesh.shape["sp"], 4, 2), ("sp", "tp_0", "tp_1"))
    return jax.shard_map(
        body,
        mesh=split,
        in_specs=(
            P("sp", TP),
            P("sp", TP),
            P("sp"),
            P(None, TP),
            P(TP, None, None),
            P(TP, None, None),
            P(TP),
            P("sp", TP),
            P(None, TP),
            P("sp", TP),
            P(TP),
            P(TP),
            P(TP),
            P("sp", TP),
            P("sp", TP),
            P(TP, "sp"),
        ),
        out_specs=P("sp", TP),
        check_vma=False,
    )
```

profile of v0, /device:TPU:1, one launch (start us, length us, event | category | flops | bytes accessed | tf_op | source)
XLA Modules:
  0.0 220.4 jit_solution(9097874307135880774)
XLA Ops:
  9.2 4.0 %collective-permute-start = (s32[3]{0:T(128)S(1)}, s32[3]{0:T(128)S(1)}, u32[]{:S(2)}, u32[]{:S(2)}) collective-permute-start(s32[3]{0:T(128)S(1)} %slice.106), channel_id=1, source_target_pairs={{0,8},{8,16},{16,24},{24,32},{32,40},{40,48},{48,56},{56,64},{64,7... | collective-permute-start | bytes 44 | tf_op jit(solution)/shard_map/ppermute | solution.py:29
  14.0 3.2 %collective-permute-start.1 = (bf16[3,128]{0,1:T(8,128)(2,1)S(1)}, bf16[3,128]{0,1:T(8,128)(2,1)S(1)}, u32[]{:S(2)}, u32[]{:S(2)}) collective-permute-start(bf16[3,128]{0,1:T(8,128)(2,1)S(1)} %copy.91), channel_id=1, source_target_pairs={{0,8},{8,16},{16,24},{24,32},{32,40},{40,48},{48,56},{56,64},{64,7... | collective-permute-start | bytes 2312 | tf_op jit(solution)/shard_map/ppermute | solution.py:29
  24.3 35.9 %while.17 = (s32[]{:T(128)}, f32[128]{0:T(128)S(1)}, f32[128]{0:T(128)S(1)}, f32[6,128,128]{2,1,0:T(8,128)S(1)}, f32[6,128,128]{2,1,0:T(8,128)S(1)}, /*index=5*/...) while((s32[]{:T(128)}, f32[128]{0:T(128)S(1)}, ...), condition=%wide.region_2.3_spmd.clone, body=%wide.region_0.2_spmd.clone.sunk | while | flops 12681602 | bytes 1023637 | solution.py:122
  26.6 3.6 %multiply_reduce_fusion.3 = f32[128,128]{0,1:T(8,128)S(1)} fusion(f32[128,128]{0,1:T(8,128)S(1)} %get-tuple-element.205, f32[128,128]{1,0:T(8,128)S(1)} %reduce_window_sum.13, pred[128,128]{1,0:T(8,128)(4,1)S(1)} %fusion.63), kind=kLoop, calls=%fused_computation.1.clone.1 | loop fusion | flops 10469376 | bytes 212992 | tf_op jit(solution)/shard_map/while/body/eval_jaxpr/ijc,jc->ic/dot_general | solution.py:115
  32.6 3.6 %multiply_reduce_fusion.3 = f32[128,128]{0,1:T(8,128)S(1)} fusion(f32[128,128]{0,1:T(8,128)S(1)} %get-tuple-element.205, f32[128,128]{1,0:T(8,128)S(1)} %reduce_window_sum.13, pred[128,128]{1,0:T(8,128)(4,1)S(1)} %fusion.63), kind=kLoop, calls=%fused_computation.1.clone.1 | loop fusion | flops 10469376 | bytes 212992 | tf_op jit(solution)/shard_map/while/body/eval_jaxpr/ijc,jc->ic/dot_general | solution.py:115
  38.6 3.6 %multiply_reduce_fusion.3 = f32[128,128]{0,1:T(8,128)S(1)} fusion(f32[128,128]{0,1:T(8,128)S(1)} %get-tuple-element.205, f32[128,128]{1,0:T(8,128)S(1)} %reduce_window_sum.13, pred[128,128]{1,0:T(8,128)(4,1)S(1)} %fusion.63), kind=kLoop, calls=%fused_computation.1.clone.1 | loop fusion | flops 10469376 | bytes 212992 | tf_op jit(solution)/shard_map/while/body/eval_jaxpr/ijc,jc->ic/dot_general | solution.py:115
  44.5 3.6 %multiply_reduce_fusion.3 = f32[128,128]{0,1:T(8,128)S(1)} fusion(f32[128,128]{0,1:T(8,128)S(1)} %get-tuple-element.205, f32[128,128]{1,0:T(8,128)S(1)} %reduce_window_sum.13, pred[128,128]{1,0:T(8,128)(4,1)S(1)} %fusion.63), kind=kLoop, calls=%fused_computation.1.clone.1 | loop fusion | flops 10469376 | bytes 212992 | tf_op jit(solution)/shard_map/while/body/eval_jaxpr/ijc,jc->ic/dot_general | solution.py:115
  50.5 3.6 %multiply_reduce_fusion.3 = f32[128,128]{0,1:T(8,128)S(1)} fusion(f32[128,128]{0,1:T(8,128)S(1)} %get-tuple-element.205, f32[128,128]{1,0:T(8,128)S(1)} %reduce_window_sum.13, pred[128,128]{1,0:T(8,128)(4,1)S(1)} %fusion.63), kind=kLoop, calls=%fused_computation.1.clone.1 | loop fusion | flops 10469376 | bytes 212992 | tf_op jit(solution)/shard_map/while/body/eval_jaxpr/ijc,jc->ic/dot_general | solution.py:115
  56.5 3.6 %multiply_reduce_fusion.3 = f32[128,128]{0,1:T(8,128)S(1)} fusion(f32[128,128]{0,1:T(8,128)S(1)} %get-tuple-element.205, f32[128,128]{1,0:T(8,128)S(1)} %reduce_window_sum.13, pred[128,128]{1,0:T(8,128)(4,1)S(1)} %fusion.63), kind=kLoop, calls=%fused_computation.1.clone.1 | loop fusion | flops 10469376 | bytes 212992 | tf_op jit(solution)/shard_map/while/body/eval_jaxpr/ijc,jc->ic/dot_general | solution.py:115
  60.9 7.1 %all-to-all-start = ((f32[16,2,128]{2,1,0:T(2,128)}), f32[16,2,128]{2,1,0:T(2,128)S(1)}, u32[]{:S(2)}, u32[]{:S(2)}) async-start(f32[16,2,128]{2,1,0:T(2,128)} %broadcast_in_dim.64), calls=%async_computation | async-start | bytes 32768 | tf_op jit(solution)/shard_map/all_to_all | solution.py:34
  68.1 6.5 %all-to-all-done = f32[16,2,128]{2,1,0:T(2,128)S(1)} async-done(((f32[16,2,128]{2,1,0:T(2,128)}), f32[16,2,128]{2,1,0:T(2,128)S(1)}, u32[]{:S(2)}, u32[]{:S(2)}) %all-to-all-start) | async-done | bytes 16416 | tf_op jit(solution)/shard_map/all_to_all | solution.py:34
  75.2 13.1 %all_to_all.43 = bf16[4,768,128]{2,1,0:T(8,128)(2,1)S(1)} all-to-all(bf16[4,768,128]{2,1,0:T(8,128)(2,1)S(1)} %broadcast_in_dim.67), channel_id=1, replica_groups=mesh['sp'=16,'tp_0'=4,'tp_1'=2] {'tp_0'}, dimensions={0} | all-to-all | bytes 1572864 | tf_op jit(solution)/shard_map/all_to_all | solution.py:34
  88.5 8.6 %all_to_all.44 = bf16[2,4,768,128]{3,2,1,0:T(8,128)(2,1)S(1)} all-to-all(bf16[2,4,768,128]{3,2,1,0:T(8,128)(2,1)S(1)} %broadcast_in_dim.68), channel_id=1, replica_groups=mesh['sp'=16,'tp_0'=4,'tp_1'=2] {'tp_1'}, dimensions={0} | all-to-all | bytes 3145728 | tf_op jit(solution)/shard_map/all_to_all | solution.py:34
  98.8 2.1 multiply_reduce_fusion.1
  101.5 3.6 %all-to-all-start.3 = ((f32[8,1,768]{2,1,0:T(1,128)}), f32[8,1,768]{2,1,0:T(1,128)S(1)}, u32[]{:S(2)}, u32[]{:S(2)}) async-start(f32[8,1,768]{2,1,0:T(1,128)} %broadcast_in_dim.69), calls=%async_computation.3 | async-start | bytes 49152 | tf_op jit(solution)/shard_map/all_to_all | solution.py:34
  105.3 4.5 %all-to-all-done.3 = f32[8,1,768]{2,1,0:T(1,128)S(1)} async-done(((f32[8,1,768]{2,1,0:T(1,128)}), f32[8,1,768]{2,1,0:T(1,128)S(1)}, u32[]{:S(2)}, u32[]{:S(2)}) %all-to-all-start.3) | async-done | bytes 24608 | tf_op jit(solution)/shard_map/all_to_all | solution.py:34
  110.1 7.8 %all_to_all.45 = f32[8,1,768]{2,1,0:T(1,128)S(1)} all-to-all(f32[8,1,768]{2,1,0:T(1,128)S(1)} %broadcast_in_dim.70), channel_id=1, replica_groups=mesh['sp'=16,'tp_0'=4,'tp_1'=2] {'tp_0','tp_1'}, dimensions={0} | all-to-all | bytes 49152 | tf_op jit(solution)/shard_map/all_to_all | solution.py:34
  118.4 22.2 %all_to_all.46 = bf16[4,768,256]{2,1,0:T(8,128)(2,1)S(1)} all-to-all(bf16[4,768,256]{2,1,0:T(8,128)(2,1)S(1)} %broadcast_in_dim.71), channel_id=1, replica_groups=mesh['sp'=16,'tp_0'=4,'tp_1'=2] {'tp_0'}, dimensions={0} | all-to-all | bytes 3145728 | tf_op jit(solution)/shard_map/all_to_all | solution.py:34
  140.8 7.8 %all_to_all.47 = bf16[2,4,768,256]{3,2,1,0:T(8,128)(2,1)S(1)} all-to-all(bf16[2,4,768,256]{3,2,1,0:T(8,128)(2,1)S(1)} %broadcast_in_dim.72), channel_id=1, replica_groups=mesh['sp'=16,'tp_0'=4,'tp_1'=2] {'tp_1'}, dimensions={0} | all-to-all | bytes 6291456 | tf_op jit(solution)/shard_map/all_to_all | solution.py:34
  150.5 4.7 %copy.105 = bf16[768,8,256]{0,2,1:T(8,128)(2,1)} copy(bf16[768,8,256]{2,0,1:T(8,128)(2,1)} %bitcast.101) | data formatting | bytes 6291456 | tf_op jit(solution)/shard_map/transpose | solution.py:79
  155.2 5.2 %fusion.9 = f32[768,704]{0,1:T(8,128)S(1)} fusion(bf16[768,2048]{0,1:T(8,128)(2,1)} %bitcast.103, bf16[2048,1408]{0,1:T(8,128)(2,1)} %all-gather.3.cloned.1.call-done), kind=kOutput, calls=%fused_computation.21 | convolution fusion | flops 2214592512 | bytes 8192000 | tf_op jit(solution)/shard_map/dot_general | solution.py:209
  160.4 10.7 %convolution_convert_fusion = bf16[768,2048]{0,1:T(8,128)(2,1)} fusion(bf16[704,2048]{1,0:T(8,128)(2,1)} %all-gather.5.cloned.1.call-done, f32[768,704]{0,1:T(8,128)S(1)} %fusion.9, bf16[768,2048]{0,1:T(8,128)(2,1)} %bitcast.104, bf16[2048,1408]{0,1:T(8,128)(2,1)} %all-gather.3.cloned.1.call-done), kind=kOutput, calls=%fused_computation.18 | convolution fusion | flops 4434001920 | bytes 14221312 | tf_op jit(solution)/shard_map/dot_general | solution.py:212
  171.1 28.8 %reduce-scatter.2.cloned.1.call-done = bf16[768,256]{0,1:T(8,128)(2,1)} async-done(((bf16[768,2048]{0,1:T(8,128)(2,1)}), bf16[768,256]{0,1:T(8,128)(2,1)}) %reduce-scatter.2.cloned.1.call-update) | async-done | bytes 393232 | tf_op jit(solution)/shard_map/reduce_scatter | solution.py:213
  201.1 10.6 %all_to_all.48 = f32[8,1,768]{2,1,0:T(1,128)S(1)} all-to-all(f32[8,1,768]{2,1,0:T(1,128)S(1)} %broadcast_in_dim.73), channel_id=1, replica_groups=mesh['sp'=16,'tp_0'=4,'tp_1'=2] {'tp_0','tp_1'}, dimensions={0} | all-to-all | bytes 49152 | tf_op jit(solution)/shard_map/all_to_all | solution.py:34
  (147 shorter events, 34.3 us)
Async XLA Ops:
  6.5 92.3 %copy-start = (bf16[1024,256]{1,0:T(8,128)(2,1)S(1)}, bf16[1024,256]{1,0:T(8,128)(2,1)}, u32[]{:S(2)}) copy-start(bf16[1024,256]{1,0:T(8,128)(2,1)} %param.26) | copy-start | bytes 1572868
  6.5 16.4 %copy-start.6 = (bf16[2,64,64]{2,1,0:T(8,128)(2,1)S(1)}, bf16[2,64,64]{2,1,0:T(8,128)(2,1)}, u32[]{:S(2)}) copy-start(bf16[2,64,64]{2,1,0:T(8,128)(2,1)} %param.23) | copy-start | bytes 49156
  6.5 16.7 %copy-start.7 = (bf16[2,64,64]{2,1,0:T(8,128)(2,1)S(1)}, bf16[2,64,64]{2,1,0:T(8,128)(2,1)}, u32[]{:S(2)}) copy-start(bf16[2,64,64]{2,1,0:T(8,128)(2,1)} %param.22) | copy-start | bytes 49156
  6.5 148.7 %all-gather.3.cloned.1.call-start = ((), (), s32[]{:S(2)}) async-start(), calls=%async_computation.9 | async-start | bytes 6127616 | tf_op jit(solution)/shard_map/all_gather | solution.py:19
  8.4 152.0 %all-gather.5.cloned.1.call-start = ((), (), s32[]{:S(2)}) async-start(), calls=%async_computation.10 | async-start | bytes 3063808 | tf_op jit(solution)/shard_map/all_gather | solution.py:152
  9.2 11.7 %collective-permute-start = (s32[3]{0:T(128)S(1)}, s32[3]{0:T(128)S(1)}, u32[]{:S(2)}, u32[]{:S(2)}) collective-permute-start(s32[3]{0:T(128)S(1)} %slice.106), channel_id=1, source_target_pairs={{0,8},{8,16},{16,24},{24,32},{32,40},{40,48},{48,56},{56,64},{64,7... | collective-permute-start | bytes 44 | tf_op jit(solution)/shard_map/ppermute | solution.py:29
  14.0 8.5 %collective-permute-start.1 = (bf16[3,128]{0,1:T(8,128)(2,1)S(1)}, bf16[3,128]{0,1:T(8,128)(2,1)S(1)}, u32[]{:S(2)}, u32[]{:S(2)}) collective-permute-start(bf16[3,128]{0,1:T(8,128)(2,1)S(1)} %copy.91), channel_id=1, source_target_pairs={{0,8},{8,16},{16,24},{24,32},{32,40},{40,48},{48,56},{56,64},{64,7... | collective-permute-start | bytes 2312 | tf_op jit(solution)/shard_map/ppermute | solution.py:29
  24.3 50.6 %copy-start.2 = (bf16[768,128]{1,0:T(8,128)(2,1)S(1)}, bf16[768,128]{1,0:T(8,128)(2,1)}, u32[]{:S(2)}) copy-start(bf16[768,128]{1,0:T(8,128)(2,1)} %param.18) | copy-start | bytes 589828
  60.9 13.7 %all-to-all-start = ((f32[16,2,128]{2,1,0:T(2,128)}), f32[16,2,128]{2,1,0:T(2,128)S(1)}, u32[]{:S(2)}, u32[]{:S(2)}) async-start(f32[16,2,128]{2,1,0:T(2,128)} %broadcast_in_dim.64), calls=%async_computation | async-start | bytes 32768 | tf_op jit(solution)/shard_map/all_to_all | solution.py:34
  98.8 6.3 %copy-start.1 = (bf16[768,256]{1,0:T(8,128)(2,1)S(1)}, bf16[768,256]{1,0:T(8,128)(2,1)}, u32[]{:S(2)}) copy-start(bf16[768,256]{1,0:T(8,128)(2,1)} %param.27) | copy-start | bytes 1179652
  98.8 11.1 %copy-start.4 = (f32[256]{0:T(256)S(1)}, f32[256]{0:T(256)}, u32[]{:S(2)}) copy-start(f32[256]{0:T(256)} %param.28) | copy-start | bytes 3076
  98.8 19.1 %copy-start.3 = (f32[256]{0:T(256)S(1)}, f32[256]{0:T(256)}, u32[]{:S(2)}) copy-start(f32[256]{0:T(256)} %param.29) | copy-start | bytes 3076
  101.5 8.3 %all-to-all-start.3 = ((f32[8,1,768]{2,1,0:T(1,128)}), f32[8,1,768]{2,1,0:T(1,128)S(1)}, u32[]{:S(2)}, u32[]{:S(2)}) async-start(f32[8,1,768]{2,1,0:T(1,128)} %broadcast_in_dim.69), calls=%async_computation.3 | async-start | bytes 49152 | tf_op jit(solution)/shard_map/all_to_all | solution.py:34
  105.1 94.8 %reduce-scatter.2.cloned.1.call-start = ((), (), s32[]{:S(2)}) async-start(), calls=%async_computation.11 | async-start | bytes 3538944 | tf_op jit(solution)/shard_map/reduce_scatter | solution.py:213
  171.1 40.7 %copy-start.5 = (f32[256]{0:T(256)S(1)}, f32[256]{0:T(256)}, u32[]{:S(2)}) copy-start(f32[256]{0:T(256)} %param.30) | copy-start | bytes 3076
Sparse Core Ops, SparseCore 0:
  9.4 66.3 all-gather.2
  78.0 50.0 all-gather.4
  171.3 28.6 reduce-scatter.1
where the time goes:
time: 222 us; the launch traced here: 220 us
  blocking collectives  70.1 us (32%)
  other arithmetic  40.3 us (18%)
  waiting for transfers between devices  39.9 us (18%)
  local copies, waits for them, and re-layouts  19.7 us (9%)
  matrix products  18.6 us (8%)
  starting transfers between devices  18 us (8%)
  between operations  13.5 us (6%)
    all_to_all x6, blocking collectives, from_everyone(): lax.all_to_all(jnp.broadcast_to(shard[None], (count, *shard.shape)), axis...  70.1 us
    reduce_scatter x1, waiting for transfers between devices, body(): lax.psum_scatter(partial_value.astype(jnp.bfloat16), TP, scatter_dimensio...  28.8 us
    dot_general x6, other arithmetic, step(): local = jnp.einsum('ijc,jc->ic', weights, drives)  21.6 us
    all_to_all x2, waiting for transfers between devices, from_everyone(): lax.all_to_all(jnp.broadcast_to(shard[None], (count, *shard.shape)), axis...  11 us
    all_to_all x2, starting transfers between devices, from_everyone(): lax.all_to_all(jnp.broadcast_to(shard[None], (count, *shard.shape)), axis...  10.8 us
    dot_general x1, matrix products, body(): jnp.dot(hidden, down_whole, preferred_element_type=jnp.float32)  10.7 us
    convert_element_type x6, other arithmetic, step(): reach = jnp.exp(cumulative) * (ids == before).astype(jnp.float32)[:, None]  7.95 us
    ppermute x2, starting transfers between devices, passed_along(): return lax.ppermute(block, axis, route)  7.2 us
  transfers between devices with their start and end apart: 7, of which 3 were waited for; matrix products, arithmetic and copies ran while one was open for 28% of the time, Pallas kernels for 0%

commit v1 on v0

v1 whole, which is shorter than its diff:
```python
import functools

import jax
import jax.numpy as jnp
from jax import lax
from jax.experimental import pallas as pl
from jax.experimental.pallas import tpu as pltpu
from jax.sharding import Mesh
from jax.sharding import PartitionSpec as P

SP = ("z", "y")
TP = ("x", "c")
EPS = 1e-06
BF = jnp.bfloat16
F32 = jnp.float32
VM = pl.BlockSpec(memory_space=pltpu.VMEM)
SM = pl.BlockSpec(memory_space=pltpu.SMEM)
HB = pl.BlockSpec(memory_space=pltpu.HBM)
SEGS = 8


def cyc(count, step):
    return [(i, (i + step) % count) for i in range(count)]


def stretch(row, lanes=128):
    return jnp.broadcast_to(row, (lanes, 128)).T


def taylor_expm1_neg(y):
    p = 1.0 + y * (1.0 / 8.0)
    for k in (7.0, 6.0, 5.0, 4.0, 3.0, 2.0):
        p = 1.0 + y * (1.0 / k) * p
    return -y * p


def pack_kernel(g_ref, u_ref, d_ref, out_ref):
    for j in range(5):
        at = slice(128 * j, 128 * j + 128)
        out_ref[at, :] = g_ref[:, at]
        out_ref[640 + 128 * j : 768 + 128 * j, :] = u_ref[:, at]
    out_ref[1280:1408, :] = jnp.concatenate([g_ref[:, 640:704], u_ref[:, 640:704]], axis=1)
    out_ref[1408:2112, :] = d_ref[...]


def scan_kernel(
    x_ref, rim_ref, ids_ref, taps_ref, gm_ref, im_ref, nsp_ref, extra_ref,
    s_ref, p_ref, e_ref, xs, idx, fs, ds,
):
    rows = x_ref.shape[0]
    taps = taps_ref[...].astype(F32)
    head = gm_ref.shape[1]

    def blockdiag(ref):
        zero = jnp.zeros((head, head), BF)
        return jnp.concatenate(
            [
                jnp.concatenate([ref[0], zero], axis=1),
                jnp.concatenate([zero, ref[1]], axis=1),
            ],
            axis=0,
        )

    gate = blockdiag(gm_ref)
    inp = blockdiag(im_ref)
    xs[0:8, :] = rim_ref[0:8, :]
    idx[0:8, :] = rim_ref[8:16, :]
    for j in range(rows // 128):
        at = 8 + 128 * j
        xs[at : at + 128, :] = x_ref[128 * j : 128 * j + 128, :].astype(F32)
        idx[at : at + 128, :] = stretch(ids_ref[j : j + 1, :])
    for j in range(rows // 128):
        at = 8 + 128 * j
        here = idx[at : at + 128, :]
        before = idx[at - 1 : at + 127, :]
        conv = xs[at : at + 128, :] * taps[0:1, :]
        for k in range(1, 4):
            old = idx[at - k : at - k + 128, :]
            conv = conv + jnp.where(old == here, xs[at - k : at - k + 128, :], 0.0) * taps[k : k + 1, :]
        conv = conv.astype(BF)
        rg = jax.nn.sigmoid(jnp.dot(conv, gate, preferred_element_type=F32))
        ig = jax.nn.sigmoid(jnp.dot(conv, inp, preferred_element_type=F32))
        ld = nsp_ref[...] * rg + extra_ref[128 * j : 128 * j + 128, :]
        e = jnp.exp(ld)
        y = 2.0 * ld
        em = jnp.where(y > -0.5, taylor_expm1_neg(jnp.maximum(y, -0.5)), 1.0 - e * e)
        fs[128 * j : 128 * j + 128, :] = jnp.where(before == here, e, 0.0)
        ds[128 * j : 128 * j + 128, :] = jnp.sqrt(em) * ig * conv.astype(F32)
    seg = rows // SEGS

    def step(j, carry):
        h, p = carry
        f = fs[pl.ds(j, SEGS, stride=seg), :]
        d = ds[pl.ds(j, SEGS, stride=seg), :]
        h = f * h + d
        p = p * f
        s_ref[pl.ds(j, SEGS, stride=seg), :] = h
        p_ref[pl.ds(j, SEGS, stride=seg), :] = p
        return h, p

    zero = jnp.zeros((SEGS, 128), F32)
    h, p = lax.fori_loop(0, seg, step, (zero, zero + 1.0), unroll=8)
    a = p[0:1, :]
    b = h[0:1, :]
    for s in range(1, SEGS):
        b = p[s : s + 1, :] * b + h[s : s + 1, :]
        a = p[s : s + 1, :] * a
    for i in range(16):
        e_ref[i, 0:1, :] = a
        e_ref[i, 1:2, :] = b


def branch_kernel(pos_ref, s_ref, p_ref, e_ref, g_ref, out_ref):
    rows = s_ref.shape[0]
    seg = rows // SEGS
    me = pos_ref[0]
    h = jnp.zeros((1, 128), F32)
    for i in range(16):
        a = e_ref[i, 0:1, :]
        b = e_ref[i, 1:2, :]
        h = jnp.where(i < me, a * h + b, h)
    half = SEGS // 2
    for s in range(SEGS):
        at = s * seg
        st = s_ref[at : at + seg, :]
        pr = p_ref[at : at + seg, :]
        states = st + pr * h
        out = (states * jax.nn.gelu(g_ref[at : at + seg, :].astype(F32), approximate=True)).astype(BF)
        h = states[seg - 1 : seg, :]
        to = (s % half) * seg
        for i in range(4):
            out_ref[2 * i + s // half, to : to + seg, :] = out


def mix_kernel(
    pos_ref, br_ref, w0, w1, w2, w3, v0, v1, v2, v3, g0, g1, g2, g3,
    norm_ref, keep_ref, send_ref, full, mixed, stream,
):
    x = pos_ref[2]
    c = pos_ref[1]
    rows = br_ref.shape[1]
    for i in range(8):
        full[:, 128 * i : 128 * i + 128] = br_ref[i]
    lhs = full[...]
    total = jnp.zeros((rows, 128), F32)
    pieces = []
    for d, w, v, g in ((0, w0, v0, g0), (3, w1, v1, g1), (1, w2, v2, g2), (2, w3, v3, g3)):
        block = lax.rem(x + d, 4)
        for k, core, ref in ((0, c, w), (1, 1 - c, v)):
            at = pl.ds(pl.multiple_of((2 * block + core) * 256, 256), 256)
            pieces.append((at, w, k, g))
            m = jnp.dot(lhs, ref[0:1024, :], preferred_element_type=F32).astype(BF)
            mixed[:, at] = m
            mf = m.astype(F32)
            mf = mf * mf
            total = total + mf[:, :128] + mf[:, 128:]
    scale = lax.rsqrt(jnp.sum(total, axis=1, keepdims=True) / 2048.0 + EPS)
    total = jnp.zeros((rows, 128), F32)
    for at, w, k, g in pieces:
        r = w[1024 + rows * k : 1024 + rows * k + rows, :].astype(F32)
        s = (r + mixed[:, at].astype(F32) * scale * g[2 * k : 2 * k + 1, :]).astype(BF)
        stream[:, at] = s
        sf = s.astype(F32)
        sf = sf * sf
        total = total + sf[:, :128] + sf[:, 128:]
    scale = lax.rsqrt(jnp.sum(total, axis=1, keepdims=True) / 2048.0 + EPS)
    for at, w, k, g in pieces:
        norm_ref[:, at] = (stream[:, at].astype(F32) * scale * g[2 * k + 1 : 2 * k + 2, :]).astype(BF)
    keep_ref[...] = stream[:, pl.ds(pl.multiple_of((2 * x + c) * 256, 256), 256)]
    send_ref[...] = stream[:, pl.ds(pl.multiple_of((2 * x + 1 - c) * 256, 256), 256)]


def down_copies(w_ref, dn, sem):
    return [
        pltpu.make_async_copy(w_ref.at[s, pl.ds(1408, 704)], dn.at[s], sem) for s in range(16)
    ]


def down_dot(lhs, dn, out_ref):
    for j in range(8):
        both = jnp.concatenate([dn[2 * j], dn[2 * j + 1]], axis=1)
        out_ref[:, 256 * j : 256 * j + 256] = jnp.dot(
            lhs, both, preferred_element_type=F32
        ).astype(BF)


def ffn_kernel(oth_ref, own_ref, w_ref, out_ref, hid_ref, gu, dn, hoth, sem):
    def tile(j):
        return [
            pltpu.make_async_copy(
                w_ref.at[s, pl.ds(128 * j, 128)], gu.at[j, pl.ds(128 * s, 128)], sem.at[j]
            )
            for s in range(16)
        ]

    order = [0, 5, 1, 6, 2, 7, 3, 8, 4, 9, 10]
    tiles = {j: tile(j) for j in order}
    downs = down_copies(w_ref, dn, sem.at[11])
    for j in order:
        for cp in tiles[j]:
            cp.start()
    for cp in downs:
        cp.start()
    for j in range(5):
        for k in (j, j + 5):
            for cp in tiles[k]:
                cp.wait()
        both = jnp.concatenate([gu[j], gu[j + 5]], axis=1)
        for src, dst in ((oth_ref, hoth), (own_ref, hid_ref)):
            act = jnp.dot(src[...], both, preferred_element_type=F32)
            dst[:, 128 * j : 128 * j + 128] = (jax.nn.silu(act[:, :128]) * act[:, 128:]).astype(BF)
    for cp in tiles[10]:
        cp.wait()
    for src, dst in ((oth_ref, hoth), (own_ref, hid_ref)):
        act = jnp.dot(src[...], gu[10], preferred_element_type=F32)
        dst[:, 640:704] = (jax.nn.silu(act[:, :64]) * act[:, 64:]).astype(BF)
    for cp in downs:
        cp.wait()
    down_dot(hoth[...], dn, out_ref)


def down_kernel(hid_ref, w_ref, out_ref, dn, sem):
    downs = down_copies(w_ref, dn, sem)
    for cp in downs:
        cp.start()
    for cp in downs:
        cp.wait()
    down_dot(hid_ref[...], dn, out_ref)


def summed(pos_ref, a_ref, b_ref, d, lo):
    h = a_ref.shape[0] // 2
    at = pl.ds(pl.multiple_of(lax.rem(pos_ref[2] + d, 4) * 512, 512), 512)
    return a_ref[lo : lo + h, at].astype(F32) + b_ref[lo : lo + h, at].astype(F32)


def far_kernel(pos_ref, a_ref, b_ref, right_ref, left_ref):
    h = a_ref.shape[0] // 2
    right_ref[...] = summed(pos_ref, a_ref, b_ref, 2, 0).astype(BF)
    left_ref[...] = summed(pos_ref, a_ref, b_ref, 2, h).astype(BF)


def near_kernel(pos_ref, a_ref, b_ref, right_ref, left_ref, accr_ref, accl_ref, own_ref):
    h = a_ref.shape[0] // 2
    right_ref[...] = summed(pos_ref, a_ref, b_ref, 1, h).astype(BF)
    left_ref[...] = summed(pos_ref, a_ref, b_ref, 3, 0).astype(BF)
    accr_ref[...] = summed(pos_ref, a_ref, b_ref, 1, 0)
    accl_ref[...] = summed(pos_ref, a_ref, b_ref, 3, h)
    own_ref[0:h, :] = summed(pos_ref, a_ref, b_ref, 0, 0)
    own_ref[h : 2 * h, :] = summed(pos_ref, a_ref, b_ref, 0, h)


def joined_kernel(pos_ref, own_ref, fl_ref, fr_ref, top_ref, bot_ref, keep_ref, send_ref, sq_ref):
    c = pos_ref[1]
    q = top_ref.shape[0]
    for k in range(2 * q // 64):
        lo = 64 * k
        at = slice(lo, lo + 64)
        if lo < q:
            more = fr_ref[at, :].astype(F32) + top_ref[at, :].astype(F32)
        else:
            more = fl_ref[lo - q : lo - q + 64, :].astype(F32) + bot_ref[lo - q : lo - q + 64, :].astype(F32)
        v = (own_ref[at, :] + more).astype(BF)
        for first, core in ((0, 0), (256, 1)):

            @pl.when(c == core)
            def _():
                keep_ref[at, :] = v[:, first : first + 256]

            @pl.when(c != core)
            def _():
                send_ref[at, :] = v[:, first : first + 256]

    for k in range(2 * q // 128):
        t = jnp.zeros((128, 128), F32)
        for ref in (keep_ref, send_ref):
            f = ref[128 * k : 128 * k + 128, :].astype(F32)
            f = f * f
            t = t + f[:, :128] + f[:, 128:]
        row = jnp.sum(t.T, axis=0, keepdims=True)
        for i in range(8):
            sq_ref[i, k : k + 1, :] = row


def final_kernel(pos_ref, keep_ref, got_ref, skeep_ref, sgot_ref, sq_ref, gain_ref, out_ref):
    c = pos_ref[1]
    half = keep_ref.shape[0]
    for f_ref, s_ref, core in ((keep_ref, skeep_ref, c), (got_ref, sgot_ref, 1 - c)):
        total = sq_ref[core]
        for i in range(1, 4):
            total = total + sq_ref[2 * i + core]
        scale = lax.rsqrt(total / 2048.0 + EPS)
        for k in range(half // 128):
            at = slice(128 * k, 128 * k + 128)
            col = stretch(scale[k : k + 1, :])
            for j in range(2):
                ln = slice(128 * j, 128 * j + 128)
                v = s_ref[at, ln].astype(F32) + f_ref[at, ln].astype(F32) * col * gain_ref[:, ln]
                out_ref[pl.ds(pl.multiple_of(core * half + 128 * k, 128), 128), ln] = v.astype(BF)


def call(fn, outs, specs, scratch=(), name=None):
    return pl.pallas_call(
        fn,
        out_shape=tuple(jax.ShapeDtypeStruct(s, d) for s, d in outs),
        in_specs=list(specs),
        out_specs=tuple(VM for _ in outs),
        scratch_shapes=list(scratch),
        name=name or fn.__name__,
    )


def swapped(block):
    return lax.ppermute(block, "c", cyc(2, 1))


def body(
    gate_branch, recur_input, doc_ids, conv_taps, gate_map, input_map, decay_level, decay_extra,
    out_weight, residual, mix_gain, pre_gain, ffn_gain, gate_weight, up_weight, down_weight,
):
    rows, width = recur_input.shape
    half = rows // 2
    x, c = lax.axis_index("x"), lax.axis_index("c")
    me = lax.axis_index(SP)
    pos = jnp.stack([me, c, x]).astype(jnp.int32)

    (stacked,) = call(pack_kernel, [((2112, 128), BF)], [VM] * 3)(
        gate_weight, up_weight, down_weight
    )
    weights = lax.all_gather(stacked, SP, axis=0)

    res_keep = lax.dynamic_slice_in_dim(residual, c * half, half, 0)
    res_send = lax.dynamic_slice_in_dim(residual, (1 - c) * half, half, 0)
    ahead = jnp.concatenate([out_weight, res_keep, swapped(res_send)])
    gains = jnp.stack([mix_gain, pre_gain])
    gains = jnp.concatenate([gains, swapped(gains)])
    near = [lax.ppermute(v, "x", cyc(4, d)) for v, d in ((ahead, 1), (ahead, 3), (gains, 1), (gains, 3), (gains, 2))]

    tail = jnp.pad(recur_input[rows - 3 :].astype(F32), ((5, 0), (0, 0)))
    tail_ids = jnp.pad(
        jnp.broadcast_to(doc_ids[rows - 3 :].astype(F32)[:, None], (3, width)), ((5, 0), (0, 0))
    )
    rim = lax.ppermute(
        jnp.concatenate([tail, tail_ids]), SP, [(i, i + 1) for i in range(15)]
    )
    nsp = (-8.0 * jax.nn.softplus(-decay_level))[None, :]
    states, products, ends = call(
        scan_kernel,
        [((rows, width), F32), ((rows, width), F32), ((16, 2, width), F32)],
        [VM] * 8,
        [
            pltpu.VMEM((rows + 8, width), F32),
            pltpu.VMEM((rows + 8, width), F32),
            pltpu.VMEM((rows, width), F32),
            pltpu.VMEM((rows, width), F32),
        ],
    )(
        recur_input, rim, doc_ids.astype(F32).reshape(rows // 128, 128), conv_taps, gate_map,
        input_map, nsp, decay_extra,
    )
    all_ends = lax.all_to_all(ends, SP, 0, 0, tiled=True)
    (branch,) = call(branch_kernel, [((8, half, width), BF)], [SM, VM, VM, VM, VM])(
        pos, states, products, all_ends, gate_branch
    )
    branch, near = lax.optimization_barrier((branch, near))
    branch = lax.all_to_all(branch, TP, 0, 0, tiled=True)
    from_left, from_right = near[:2]
    cut = from_left.shape[0] // 2
    far = jnp.concatenate(
        [
            lax.ppermute(from_left[:cut], "x", cyc(4, 1)),
            lax.ppermute(from_right[cut:], "x", cyc(4, 3)),
        ]
    )
    blocks = [ahead, from_left, from_right, far]
    norm_own, skeep, ssend = call(
        mix_kernel,
        [((half, 2048), BF), ((half, 256), BF), ((half, 256), BF)],
        [SM] + [VM] * 13,
        [
            pltpu.VMEM((half, 1024), BF),
            pltpu.VMEM((half, 2048), BF),
            pltpu.VMEM((half, 2048), BF),
        ],
    )(pos, branch, *blocks, *[swapped(b) for b in blocks], gains, *near[2:])
    norm_oth = swapped(norm_own)
    sgot = swapped(ssend)
    norm_own, norm_oth, skeep, sgot = lax.optimization_barrier((norm_own, norm_oth, skeep, sgot))

    part_oth, hid_own = call(
        ffn_kernel,
        [((half, 2048), BF), ((half, 704), BF)],
        [VM, VM, HB],
        [
            pltpu.VMEM((11, 2048, 128), BF),
            pltpu.VMEM((16, 704, 128), BF),
            pltpu.VMEM((half, 704), BF),
            pltpu.SemaphoreType.DMA((12,)),
        ],
    )(norm_oth, norm_own, weights)
    part_in = swapped(part_oth)
    (part_own,) = call(
        down_kernel,
        [((half, 2048), BF)],
        [VM, HB],
        [pltpu.VMEM((16, 704, 128), BF), pltpu.SemaphoreType.DMA],
    )(hid_own, weights)
    q = half // 2
    far_r, far_l = call(far_kernel, [((q, 512), BF)] * 2, [SM, VM, VM])(pos, part_own, part_in)
    near_r, near_l, acc_r, acc_l, own = call(
        near_kernel,
        [((q, 512), BF)] * 2 + [((q, 512), F32)] * 2 + [((half, 512), F32)],
        [SM, VM, VM],
    )(pos, part_own, part_in)
    pass_r = lax.ppermute(far_r, "x", cyc(4, 1))
    pass_l = lax.ppermute(far_l, "x", cyc(4, 3))
    from_left = lax.ppermute(near_r, "x", cyc(4, 1))
    from_right = lax.ppermute(near_l, "x", cyc(4, 3))
    pass_r, pass_l = lax.optimization_barrier((pass_r, pass_l))
    right2 = (pass_r.astype(F32) + acc_r).astype(BF)
    left2 = (pass_l.astype(F32) + acc_l).astype(BF)
    top = lax.ppermute(right2, "x", cyc(4, 1))
    bottom = lax.ppermute(left2, "x", cyc(4, 3))
    from_left, from_right, top, bottom = lax.optimization_barrier(
        (from_left, from_right, top, bottom)
    )
    fkeep, fsend, square = call(
        joined_kernel,
        [((half, 256), BF)] * 2 + [((8, 3, 128), F32)],
        [SM] + [VM] * 5,
    )(pos, own, from_left, from_right, top, bottom)
    fgot = swapped(fsend)
    square = lax.all_to_all(square, TP, 0, 0, tiled=True)
    (out,) = call(final_kernel, [((rows, 256), BF)], [SM] + [VM] * 6)(
        pos, fkeep, fgot, skeep, sgot, square, ffn_gain[None, :]
    )
    return out


def solution(mesh):
    split = Mesh(mesh.devices.reshape(4, 4, 4, 2), ("z", "y", "x", "c"))
    return jax.shard_map(
        body,
        mesh=split,
        in_specs=(
            P(SP, TP), P(SP, TP), P(SP), P(None, TP), P(TP, None, None), P(TP, None, None), P(TP),
            P(SP, TP), P(None, TP), P(SP, TP), P(TP), P(TP), P(TP), P(SP, TP), P(SP, TP), P(TP, SP),
        ),
        out_specs=P(SP, TP),
        check_vma=False,
    )
```

time: 222 us -> 159 us (0.72)
  blocking collectives: 70.1 us -> 8.57 us
  Pallas kernels: 0 us -> 44.1 us
  other arithmetic: 40.3 us -> 4.12 us
  starting transfers between devices: 18 us -> 42.5 us
  matrix products: 18.6 us -> 0 us
  local copies, waits for them, and re-layouts: 19.7 us -> 11.5 us
  waiting for transfers between devices: 39.9 us -> 33.4 us
    all_to_all x6 -> x1, blocking collectives: 70.1 us -> 8.57 us  [body(): square = lax.all_to_all(square, TP, 0, 0, tiled=True)]
    pallas_call x0 -> x10, Pallas kernels: none -> 44.1 us  [the longest x1 11.7 us: body(): call(ffn_kernel, [((half, 2048), BF), ((half, 704), BF)], [VM, VM, HB], [...]
    reduce_scatter x1 -> x0, waiting for transfers between devices: 28.8 us -> none  [body(): lax.psum_scatter(partial_value.astype(jnp.bfloat16), TP, scatter_dimensio...]
    ppermute x2 -> x24, starting transfers between devices: 7.2 us -> 31.4 us  [the longest x10 12.5 us: swapped(): return lax.ppermute(block, 'c', cyc(2, 1))]
    dot_general x6 -> x0, other arithmetic: 21.6 us -> none  [step(): local = jnp.einsum('ijc,jc->ic', weights, drives)]
    dot_general x5 -> x0, matrix products: 18.6 us -> none  [the longest x1 10.7 us: body(): jnp.dot(hidden, down_whole, preferred_element_type=jnp.float32)]
    ppermute x2 -> x24, waiting for transfers between devices: 0.01 us -> 15.4 us  [the longest x1 5.8 us: body(): lax.ppermute(from_left[:cut], 'x', cyc(4, 1))]
    convert_element_type x12 -> x3, other arithmetic: 11.3 us -> 2.14 us  [the longest x1 1.04 us: body(): left2 = (pass_l.astype(F32) + acc_l).astype(BF)]
  transfers between devices with their start and end apart: 7 -> 27, of which waited for: 3 -> 8; matrix products, arithmetic and copies ran while one was open for 28% -> 4% of each run, Pallas kernels for 0% -> 15%
where the time goes in v1:
time: 159 us; the launch traced here: 158 us
  Pallas kernels  44.1 us (28%)
  starting transfers between devices  42.5 us (27%)
  waiting for transfers between devices  33.4 us (21%)
  between operations  13.7 us (9%)
  local copies, waits for them, and re-layouts  11.5 us (7%)
  blocking collectives  8.57 us (5%)
  other arithmetic  4.12 us (3%)
    ppermute x10, starting transfers between devices, swapped(): return lax.ppermute(block, 'c', cyc(2, 1))  12.5 us
    all_to_all x1, waiting for transfers between devices, body(): branch = lax.all_to_all(branch, TP, 0, 0, tiled=True)  12.2 us
    pallas_call x1, Pallas kernels, body(): call(ffn_kernel, [((half, 2048), BF), ((half, 704), BF)], [VM, VM, HB], [...  11.7 us
    unnamed x51, local copies, waits for them, and re-layouts  9.84 us
    all_to_all x1, blocking collectives, body(): square = lax.all_to_all(square, TP, 0, 0, tiled=True)  8.57 us
    pallas_call x1, Pallas kernels, body(): call(mix_kernel, [((half, 2048), BF), ((half, 256), BF), ((half, 256), BF...  8.1 us
    all_to_all x1, starting transfers between devices, body(): all_ends = lax.all_to_all(ends, SP, 0, 0, tiled=True)  7.47 us
    all_to_all x1, waiting for transfers between devices, body(): all_ends = lax.all_to_all(ends, SP, 0, 0, tiled=True)  5.83 us
  transfers between devices with their start and end apart: 27, of which 8 were waited for; matrix products, arithmetic and copies ran while one was open for 4% of the time, Pallas kernels for 15%

profile of v1, /device:TPU:1, one launch (start us, length us, event | category | flops | bytes accessed | tf_op | source)
XLA Modules:
  0.0 157.9 jit_solution(8928632212693112496)
XLA Ops:
  17.6 3.3 %collective-permute-start = (f32[16,128]{1,0:T(8,128)S(1)}, f32[16,128]{1,0:T(8,128)S(1)}, u32[]{:S(2)}, u32[]{:S(2)}) collective-permute-start(f32[16,128]{1,0:T(8,128)S(1)} %pad_maximum_fusion.1), channel_id=1, source_target_pairs={{0,8},{8,16},{16,24},{24,32},{32,40},{40,48},{48,56},{56,64},{64,7... | collective-permute-start | bytes 24584 | tf_op jit(solution)/shard_map/ppermute | solution.py:343
  23.5 2.7 %collective-permute-start.6 = (f32[4,256]{1,0:T(4,128)S(1)}, f32[4,256]{1,0:T(4,128)S(1)}, u32[]{:S(2)}, u32[]{:S(2)}) collective-permute-start(f32[4,256]{1,0:T(4,128)S(1)} %pad_maximum_fusion.2.g0), channel_id=1, source_target_pairs={{0,6},{2,0},{4,2},{6,4},{1,7},{3,1},{5,3},{7,5},{8,14},{10,8},{12,... | collective-permute-start | bytes 12296 | tf_op jit(solution)/shard_map/ppermute | solution.py:337
  26.8 4.0 %scan_kernel.1 = (f32[768,128]{1,0:T(8,128)}, f32[768,128]{1,0:T(8,128)}, f32[16,2,128]{2,1,0:T(2,128)}) custom-call(bf16[768,128]{1,0:T(8,128)(2,1)} %x_ref.1, f32[16,128]{1,0:T(8,128)} %copy-done.16, f32[6,128]{1,0:T(8,128)} %convert_bitcast_fusion.ids_ref, bf16[4,128]{1,0:T(4,128)(2,1)} %taps_ref.1, bf16[2,64,64]{2,1,0:T(8,128)(2,1)} %gm_ref.1, ...), custom_call_target="tpu_custom_call" | custom-call | tf_op jit(solution)/shard_map/scan_kernel/pallas_call | solution.py:347
  30.8 7.5 %all-to-all-start = ((f32[16,2,128]{2,1,0:T(2,128)}), f32[16,2,128]{2,1,0:T(2,128)S(1)}, u32[]{:S(2)}, u32[]{:S(2)}) async-start(f32[16,2,128]{2,1,0:T(2,128)} %get-tuple-element.41), calls=%async_computation | async-start | bytes 32768 | tf_op jit(solution)/shard_map/all_to_all | solution.py:361
  38.9 5.8 %all-to-all-done.e_ref = f32[16,2,128]{2,1,0:T(2,128)S(1)} async-done(((f32[16,2,128]{2,1,0:T(2,128)}), f32[16,2,128]{2,1,0:T(2,128)S(1)}, u32[]{:S(2)}, u32[]{:S(2)}) %all-to-all-start) | async-done | bytes 16416 | tf_op jit(solution)/shard_map/all_to_all | solution.py:361
  45.3 2.3 %branch_kernel.1 = bf16[8,384,128]{2,1,0:T(8,128)(2,1)} custom-call(s32[3]{0:T(128)} %pad_add_fusion.pos_ref, f32[768,128]{1,0:T(8,128)} %get-tuple-element.39.s_ref, f32[768,128]{1,0:T(8,128)} %get-tuple-element.40.p_ref, f32[16,2,128]{2,1,0:T(2,128)} %copy-done.14, bf16[768,128]{1,0:T(8,128)(2,1)} %g_ref.2), custom_call_target="tpu_custom_call" | custom-call | tf_op jit(solution)/shard_map/branch_kernel/pallas_call | solution.py:362
  48.0 2.6 %collective-permute-start.9 = (bf16[896,256]{1,0:T(8,128)(2,1)S(1)}, bf16[896,256]{1,0:T(8,128)(2,1)S(1)}, u32[]{:S(2)}, u32[]{:S(2)}) collective-permute-start(bf16[896,256]{1,0:T(8,128)(2,1)S(1)} %slice.15), channel_id=1, source_target_pairs={{0,6},{2,0},{4,2},{6,4},{1,7},{3,1},{5,3},{7,5},{8,14},{10,8},{12,... | collective-permute-start | bytes 1376264 | tf_op jit(solution)/shard_map/ppermute | solution.py:372
  50.6 2.4 %collective-permute-start.10 = (bf16[1792,256]{1,0:T(8,128)(2,1)S(1)}, bf16[1792,256]{1,0:T(8,128)(2,1)}, u32[]{:S(2)}, u32[]{:S(2)}) collective-permute-start(bf16[1792,256]{1,0:T(8,128)(2,1)S(1)} %pad_maximum_fusion.w0), channel_id=1, source_target_pairs={{0,1},{1,0},{2,3},{3,2},{4,5},{5,4},{6,7},{7,6},{8,9},{9,8},{10,11... | collective-permute-start | bytes 2752520 | tf_op jit(solution)/shard_map/ppermute | solution.py:314
  53.5 5.8 %collective-permute-done.8 = bf16[896,256]{1,0:T(8,128)(2,1)S(1)} collective-permute-done((bf16[896,256]{1,0:T(8,128)(2,1)S(1)}, bf16[896,256]{1,0:T(8,128)(2,1)S(1)}, u32[]{:S(2)}, u32[]{:S(2)}) %collective-permute-start.8) | collective-permute-done | bytes 458784 | tf_op jit(solution)/shard_map/ppermute | solution.py:371
  61.0 2.7 %collective-permute-start.13 = (bf16[1792,256]{1,0:T(8,128)(2,1)}, bf16[1792,256]{1,0:T(8,128)(2,1)}, u32[]{:S(2)}, u32[]{:S(2)}) collective-permute-start(bf16[1792,256]{1,0:T(8,128)(2,1)} %constant_dynamic-update-slice_fusion.w3), channel_id=1, source_target_pairs={{0,1},{1,0},{2,3},{3,2},{4,5},{5,4},{6,7},{7,6},{8,9},{9,8},{10,11... | collective-permute-start | bytes 2752520 | tf_op jit(solution)/shard_map/ppermute | solution.py:314
  63.7 3.6 %all-to-all-start.1 = ((bf16[8,384,128]{2,1,0:T(8,128)(2,1)}), bf16[8,384,128]{2,1,0:T(8,128)(2,1)S(1)}, u32[]{:S(2)}, u32[]{:S(2)}) async-start(bf16[8,384,128]{2,1,0:T(8,128)(2,1)} %branch_kernel.1), calls=%async_computation.1 | async-start | bytes 1572864 | tf_op jit(solution)/shard_map/all_to_all | solution.py:366
  67.3 12.2 %all-to-all-done.1.br_ref = bf16[8,384,128]{2,1,0:T(8,128)(2,1)S(1)} async-done(((bf16[8,384,128]{2,1,0:T(8,128)(2,1)}), bf16[8,384,128]{2,1,0:T(8,128)(2,1)S(1)}, u32[]{:S(2)}, u32[]{:S(2)}) %all-to-all-start.1) | async-done | bytes 786464 | tf_op jit(solution)/shard_map/all_to_all | solution.py:366
  80.3 8.1 %mix_kernel.1 = (bf16[384,2048]{1,0:T(8,128)(2,1)}, bf16[384,256]{1,0:T(8,128)(2,1)}, bf16[384,256]{1,0:T(8,128)(2,1)}) custom-call(s32[3]{0:T(128)} %pad_add_fusion.pos_ref, bf16[8,384,128]{2,1,0:T(8,128)(2,1)} %copy-done.2, bf16[1792,256]{1,0:T(8,128)(2,1)} %copy-done.1, bf16[1792,256]{1,0:T(8,128)(2,1)} %copy-done.3, bf16[1792,256]{1,0:T(8,128)(2,1)} %copy-done.4, ...), custom_call_target="tpu_custom_call" | custom-call | tf_op jit(solution)/shard_map/mix_kernel/pallas_call | solution.py:376
  89.6 3.3 %collective-permute-done.15.sgot_ref = bf16[384,256]{1,0:T(8,128)(2,1)S(1)} collective-permute-done((bf16[384,256]{1,0:T(8,128)(2,1)}, bf16[384,256]{1,0:T(8,128)(2,1)S(1)}, u32[]{:S(2)}, u32[]{:S(2)}) %collective-permute-start.15) | collective-permute-done | bytes 196640 | tf_op jit(solution)/shard_map/ppermute | solution.py:314
  94.1 11.7 %ffn_kernel.1 = (bf16[384,2048]{1,0:T(8,128)(2,1)}, bf16[384,704]{1,0:T(8,128)(2,1)}) custom-call(bf16[384,2048]{1,0:T(8,128)(2,1)} %copy-done.5, bf16[384,2048]{1,0:T(8,128)(2,1)} %get-tuple-element.52.own_ref, bf16[16,2112,128]{2,1,0:T(8,128)(2,1)} %bitcast.11), custom_call_target="tpu_custom_call" | custom-call | tf_op jit(solution)/shard_map/ffn_kernel/pallas_call | solution.py:390
  106.3 5.4 %down_kernel.1.a_ref = bf16[384,2048]{1,0:T(8,128)(2,1)} custom-call(bf16[384,704]{1,0:T(8,128)(2,1)} %get-tuple-element.53.hid_ref, bf16[16,2112,128]{2,1,0:T(8,128)(2,1)} %bitcast.12), custom_call_target="tpu_custom_call" | custom-call | tf_op jit(solution)/shard_map/down_kernel/pallas_call | solution.py:402
  112.9 2.7 %far_kernel.1 = (bf16[192,512]{1,0:T(8,128)(2,1)}, bf16[192,512]{1,0:T(8,128)(2,1)}) custom-call(s32[3]{0:T(128)} %pad_add_fusion.pos_ref, bf16[384,2048]{1,0:T(8,128)(2,1)} %down_kernel.1.a_ref, bf16[384,2048]{1,0:T(8,128)(2,1)} %copy-done), custom_call_target="tpu_custom_call" | custom-call | tf_op jit(solution)/shard_map/far_kernel/pallas_call | solution.py:409
  115.9 2.4 %collective-permute-start.20 = (bf16[192,512]{1,0:T(8,128)(2,1)}, bf16[192,512]{1,0:T(8,128)(2,1)S(1)}, u32[]{:S(2)}, u32[]{:S(2)}) collective-permute-start(bf16[192,512]{1,0:T(8,128)(2,1)} %get-tuple-element.59), channel_id=1, source_target_pairs={{0,6},{2,0},{4,2},{6,4},{1,7},{3,1},{5,3},{7,5},{8,14},{10,8},{12,... | collective-permute-start | bytes 589832 | tf_op jit(solution)/shard_map/ppermute | solution.py:416
  118.3 3.3 %near_kernel.1 = (bf16[192,512]{1,0:T(8,128)(2,1)}, bf16[192,512]{1,0:T(8,128)(2,1)}, f32[192,512]{1,0:T(8,128)}, f32[192,512]{1,0:T(8,128)}, f32[384,512]{1,0:T(8,128)}) custom-call(s32[3]{0:T(128)} %pad_add_fusion.pos_ref, bf16[384,2048]{1,0:T(8,128)(2,1)} %down_kernel.1.a_ref, bf16[384,2048]{1,0:T(8,128)(2,1)} %copy-done), custom_call_target="tpu_custom_call" | custom-call | tf_op jit(solution)/shard_map/near_kernel/pallas_call | solution.py:410
  121.6 2.7 %collective-permute-start.18 = (bf16[192,512]{1,0:T(8,128)(2,1)}, bf16[192,512]{1,0:T(8,128)(2,1)S(1)}, u32[]{:S(2)}, u32[]{:S(2)}) collective-permute-start(bf16[192,512]{1,0:T(8,128)(2,1)} %get-tuple-element.57), channel_id=1, source_target_pairs={{0,6},{2,0},{4,2},{6,4},{1,7},{3,1},{5,3},{7,5},{8,14},{10,8},{12,... | collective-permute-start | bytes 589832 | tf_op jit(solution)/shard_map/ppermute | solution.py:418
  128.8 3.2 %collective-permute-done.22.bot_ref = bf16[192,512]{1,0:T(8,128)(2,1)S(1)} collective-permute-done((bf16[192,512]{1,0:T(8,128)(2,1)S(1)}, bf16[192,512]{1,0:T(8,128)(2,1)S(1)}, u32[]{:S(2)}, u32[]{:S(2)}) %collective-permute-start.22) | collective-permute-done | bytes 196640 | tf_op jit(solution)/shard_map/ppermute | solution.py:423
  134.8 2.4 %joined_kernel.1 = (bf16[384,256]{1,0:T(8,128)(2,1)}, bf16[384,256]{1,0:T(8,128)(2,1)}, f32[8,3,128]{2,1,0:T(4,128)}) custom-call(s32[3]{0:T(128)} %pad_add_fusion.pos_ref, f32[384,512]{1,0:T(8,128)} %get-tuple-element.55.own_ref, bf16[192,512]{1,0:T(8,128)(2,1)} %copy-done.10, bf16[192,512]{1,0:T(8,128)(2,1)} %copy-done.11, bf16[192,512]{1,0:T(8,128)(2,1)} %copy-done.13, ...), custom_call_target="tpu_custom_call" | custom-call | tf_op jit(solution)/shard_map/joined_kernel/pallas_call | solution.py:427
  137.1 2.4 %collective-permute-start.23 = (bf16[384,256]{1,0:T(8,128)(2,1)}, bf16[384,256]{1,0:T(8,128)(2,1)S(1)}, u32[]{:S(2)}, u32[]{:S(2)}) collective-permute-start(bf16[384,256]{1,0:T(8,128)(2,1)} %get-tuple-element.69), channel_id=1, source_target_pairs={{0,1},{1,0},{2,3},{3,2},{4,5},{5,4},{6,7},{7,6},{8,9},{9,8},{10,11... | collective-permute-start | bytes 589832 | tf_op jit(solution)/shard_map/ppermute | solution.py:314
  139.6 8.6 %all_to_all.15.sq_ref = f32[8,3,128]{2,1,0:T(4,128)} all-to-all(f32[8,3,128]{2,1,0:T(4,128)} %get-tuple-element.72), channel_id=1, replica_groups=mesh['z'=4,'y'=4,'x'=4,'c'=2] {'x','c'}, dimensions={0} | all-to-all | bytes 24576 | tf_op jit(solution)/shard_map/all_to_all | solution.py:433
  (110 shorter events, 33.3 us)
Async XLA Ops:
  6.5 86.4 %all-gather.3.cloned.1.call-start = ((), (), s32[]{:S(2)}) async-start(), calls=%async_computation.3 | async-start | bytes 9191424 | tf_op jit(solution)/shard_map/all_gather | solution.py:330
  14.8 32.8 %collective-permute-start.2 = (bf16[1792,256]{1,0:T(8,128)(2,1)S(1)}, bf16[1792,256]{1,0:T(8,128)(2,1)S(1)}, u32[]{:S(2)}, u32[]{:S(2)}) collective-permute-start(bf16[1792,256]{1,0:T(8,128)(2,1)S(1)} %pad_maximum_fusion.w0), channel_id=1, source_target_pairs={{0,2},{2,4},{4,6},{6,0},{1,3},{3,5},{5,7},{7,1},{8,10},{10,12},{12... | collective-permute-start | bytes 2752520 | tf_op jit(solution)/shard_map/ppermute | solution.py:337
  16.2 31.4 %collective-permute-start.3 = (bf16[1792,256]{1,0:T(8,128)(2,1)S(1)}, bf16[1792,256]{1,0:T(8,128)(2,1)S(1)}, u32[]{:S(2)}, u32[]{:S(2)}) collective-permute-start(bf16[1792,256]{1,0:T(8,128)(2,1)S(1)} %pad_maximum_fusion.w0), channel_id=1, source_target_pairs={{0,6},{2,0},{4,2},{6,4},{1,7},{3,1},{5,3},{7,5},{8,14},{10,8},{12,... | collective-permute-start | bytes 2752520 | tf_op jit(solution)/shard_map/ppermute | solution.py:337
  17.6 8.5 %collective-permute-start = (f32[16,128]{1,0:T(8,128)S(1)}, f32[16,128]{1,0:T(8,128)S(1)}, u32[]{:S(2)}, u32[]{:S(2)}) collective-permute-start(f32[16,128]{1,0:T(8,128)S(1)} %pad_maximum_fusion.1), channel_id=1, source_target_pairs={{0,8},{8,16},{16,24},{24,32},{32,40},{40,48},{48,56},{56,64},{64,7... | collective-permute-start | bytes 24584 | tf_op jit(solution)/shard_map/ppermute | solution.py:343
  23.4 24.2 %collective-permute-start.5 = (f32[4,256]{1,0:T(4,128)S(1)}, f32[4,256]{1,0:T(4,128)S(1)}, u32[]{:S(2)}, u32[]{:S(2)}) collective-permute-start(f32[4,256]{1,0:T(4,128)S(1)} %pad_maximum_fusion.2.g0), channel_id=1, source_target_pairs={{0,2},{2,4},{4,6},{6,0},{1,3},{3,5},{5,7},{7,1},{8,10},{10,12},{12... | collective-permute-start | bytes 12296 | tf_op jit(solution)/shard_map/ppermute | solution.py:337
  23.5 24.1 %collective-permute-start.6 = (f32[4,256]{1,0:T(4,128)S(1)}, f32[4,256]{1,0:T(4,128)S(1)}, u32[]{:S(2)}, u32[]{:S(2)}) collective-permute-start(f32[4,256]{1,0:T(4,128)S(1)} %pad_maximum_fusion.2.g0), channel_id=1, source_target_pairs={{0,6},{2,0},{4,2},{6,4},{1,7},{3,1},{5,3},{7,5},{8,14},{10,8},{12,... | collective-permute-start | bytes 12296 | tf_op jit(solution)/shard_map/ppermute | solution.py:337
  26.2 21.4 %collective-permute-start.7 = (f32[4,256]{1,0:T(4,128)S(1)}, f32[4,256]{1,0:T(4,128)S(1)}, u32[]{:S(2)}, u32[]{:S(2)}) collective-permute-start(f32[4,256]{1,0:T(4,128)S(1)} %pad_maximum_fusion.2.g0), channel_id=1, source_target_pairs={{0,4},{2,6},{4,0},{6,2},{1,5},{3,7},{5,1},{7,3},{8,12},{10,14},{12... | collective-permute-start | bytes 12296 | tf_op jit(solution)/shard_map/ppermute | solution.py:337
  30.8 13.9 %all-to-all-start = ((f32[16,2,128]{2,1,0:T(2,128)}), f32[16,2,128]{2,1,0:T(2,128)S(1)}, u32[]{:S(2)}, u32[]{:S(2)}) async-start(f32[16,2,128]{2,1,0:T(2,128)} %get-tuple-element.41), calls=%async_computation | async-start | bytes 32768 | tf_op jit(solution)/shard_map/all_to_all | solution.py:361
  47.7 11.6 %collective-permute-start.8 = (bf16[896,256]{1,0:T(8,128)(2,1)S(1)}, bf16[896,256]{1,0:T(8,128)(2,1)S(1)}, u32[]{:S(2)}, u32[]{:S(2)}) collective-permute-start(bf16[896,256]{1,0:T(8,128)(2,1)S(1)} %slice.14), channel_id=1, source_target_pairs={{0,2},{2,4},{4,6},{6,0},{1,3},{3,5},{5,7},{7,1},{8,10},{10,12},{12... | collective-permute-start | bytes 1376264 | tf_op jit(solution)/shard_map/ppermute | solution.py:371
  48.0 12.1 %collective-permute-start.9 = (bf16[896,256]{1,0:T(8,128)(2,1)S(1)}, bf16[896,256]{1,0:T(8,128)(2,1)S(1)}, u32[]{:S(2)}, u32[]{:S(2)}) collective-permute-start(bf16[896,256]{1,0:T(8,128)(2,1)S(1)} %slice.15), channel_id=1, source_target_pairs={{0,6},{2,0},{4,2},{6,4},{1,7},{3,1},{5,3},{7,5},{8,14},{10,8},{12,... | collective-permute-start | bytes 1376264 | tf_op jit(solution)/shard_map/ppermute | solution.py:372
  50.6 16.8 %collective-permute-start.10 = (bf16[1792,256]{1,0:T(8,128)(2,1)S(1)}, bf16[1792,256]{1,0:T(8,128)(2,1)}, u32[]{:S(2)}, u32[]{:S(2)}) collective-permute-start(bf16[1792,256]{1,0:T(8,128)(2,1)S(1)} %pad_maximum_fusion.w0), channel_id=1, source_target_pairs={{0,1},{1,0},{2,3},{3,2},{4,5},{5,4},{6,7},{7,6},{8,9},{9,8},{10,11... | collective-permute-start | bytes 2752520 | tf_op jit(solution)/shard_map/ppermute | solution.py:314
  53.0 26.5 %collective-permute-start.11 = (bf16[1792,256]{1,0:T(8,128)(2,1)S(1)}, bf16[1792,256]{1,0:T(8,128)(2,1)}, u32[]{:S(2)}, u32[]{:S(2)}) collective-permute-start(bf16[1792,256]{1,0:T(8,128)(2,1)S(1)} %collective-permute-done.2.w1), channel_id=1, source_target_pairs={{0,1},{1,0},{2,3},{3,2},{4,5},{5,4},{6,7},{7,6},{8,9},{9,8},{10,11... | collective-permute-start | bytes 2752520 | tf_op jit(solution)/shard_map/ppermute | solution.py:314
  53.0 26.5 %collective-permute-start.12 = (bf16[1792,256]{1,0:T(8,128)(2,1)S(1)}, bf16[1792,256]{1,0:T(8,128)(2,1)}, u32[]{:S(2)}, u32[]{:S(2)}) collective-permute-start(bf16[1792,256]{1,0:T(8,128)(2,1)S(1)} %collective-permute-done.3.w2), channel_id=1, source_target_pairs={{0,1},{1,0},{2,3},{3,2},{4,5},{5,4},{6,7},{7,6},{8,9},{9,8},{10,11... | collective-permute-start | bytes 2752520 | tf_op jit(solution)/shard_map/ppermute | solution.py:314
  61.0 18.5 %collective-permute-start.13 = (bf16[1792,256]{1,0:T(8,128)(2,1)}, bf16[1792,256]{1,0:T(8,128)(2,1)}, u32[]{:S(2)}, u32[]{:S(2)}) collective-permute-start(bf16[1792,256]{1,0:T(8,128)(2,1)} %constant_dynamic-update-slice_fusion.w3), channel_id=1, source_target_pairs={{0,1},{1,0},{2,3},{3,2},{4,5},{5,4},{6,7},{7,6},{8,9},{9,8},{10,11... | collective-permute-start | bytes 2752520 | tf_op jit(solution)/shard_map/ppermute | solution.py:314
  63.7 15.8 %all-to-all-start.1 = ((bf16[8,384,128]{2,1,0:T(8,128)(2,1)}), bf16[8,384,128]{2,1,0:T(8,128)(2,1)S(1)}, u32[]{:S(2)}, u32[]{:S(2)}) async-start(bf16[8,384,128]{2,1,0:T(8,128)(2,1)} %branch_kernel.1), calls=%async_computation.1 | async-start | bytes 1572864 | tf_op jit(solution)/shard_map/all_to_all | solution.py:366
  88.4 4.5 %collective-permute-start.14 = (bf16[384,2048]{1,0:T(8,128)(2,1)}, bf16[384,2048]{1,0:T(8,128)(2,1)S(1)}, u32[]{:S(2)}, u32[]{:S(2)}) collective-permute-start(bf16[384,2048]{1,0:T(8,128)(2,1)} %get-tuple-element.52.own_ref), channel_id=1, source_target_pairs={{0,1},{1,0},{2,3},{3,2},{4,5},{5,4},{6,7},{7,6},{8,9},{9,8},{10,11... | collective-permute-start | bytes 4718600 | tf_op jit(solution)/shard_map/ppermute | solution.py:314
  105.8 5.9 %collective-permute-start.16 = (bf16[384,2048]{1,0:T(8,128)(2,1)}, bf16[384,2048]{1,0:T(8,128)(2,1)S(1)}, u32[]{:S(2)}, u32[]{:S(2)}) collective-permute-start(bf16[384,2048]{1,0:T(8,128)(2,1)} %get-tuple-element.54), channel_id=1, source_target_pairs={{0,1},{1,0},{2,3},{3,2},{4,5},{5,4},{6,7},{7,6},{8,9},{9,8},{10,11... | collective-permute-start | bytes 4718600 | tf_op jit(solution)/shard_map/ppermute | solution.py:314
  115.6 8.7 %collective-permute-start.19 = (bf16[192,512]{1,0:T(8,128)(2,1)}, bf16[192,512]{1,0:T(8,128)(2,1)S(1)}, u32[]{:S(2)}, u32[]{:S(2)}) collective-permute-start(bf16[192,512]{1,0:T(8,128)(2,1)} %get-tuple-element.58), channel_id=1, source_target_pairs={{0,2},{2,4},{4,6},{6,0},{1,3},{3,5},{5,7},{7,1},{8,10},{10,12},{12... | collective-permute-start | bytes 589832 | tf_op jit(solution)/shard_map/ppermute | solution.py:415
  115.9 8.3 %collective-permute-start.20 = (bf16[192,512]{1,0:T(8,128)(2,1)}, bf16[192,512]{1,0:T(8,128)(2,1)S(1)}, u32[]{:S(2)}, u32[]{:S(2)}) collective-permute-start(bf16[192,512]{1,0:T(8,128)(2,1)} %get-tuple-element.59), channel_id=1, source_target_pairs={{0,6},{2,0},{4,2},{6,4},{1,7},{3,1},{5,3},{7,5},{8,14},{10,8},{12,... | collective-permute-start | bytes 589832 | tf_op jit(solution)/shard_map/ppermute | solution.py:416
  121.6 7.2 %collective-permute-start.17 = (bf16[192,512]{1,0:T(8,128)(2,1)}, bf16[192,512]{1,0:T(8,128)(2,1)S(1)}, u32[]{:S(2)}, u32[]{:S(2)}) collective-permute-start(bf16[192,512]{1,0:T(8,128)(2,1)} %get-tuple-element.56), channel_id=1, source_target_pairs={{0,2},{2,4},{4,6},{6,0},{1,3},{3,5},{5,7},{7,1},{8,10},{10,12},{12... | collective-permute-start | bytes 589832 | tf_op jit(solution)/shard_map/ppermute | solution.py:417
  121.6 7.2 %collective-permute-start.18 = (bf16[192,512]{1,0:T(8,128)(2,1)}, bf16[192,512]{1,0:T(8,128)(2,1)S(1)}, u32[]{:S(2)}, u32[]{:S(2)}) collective-permute-start(bf16[192,512]{1,0:T(8,128)(2,1)} %get-tuple-element.57), channel_id=1, source_target_pairs={{0,6},{2,0},{4,2},{6,4},{1,7},{3,1},{5,3},{7,5},{8,14},{10,8},{12,... | collective-permute-start | bytes 589832 | tf_op jit(solution)/shard_map/ppermute | solution.py:418
  125.3 6.7 %collective-permute-start.22 = (bf16[192,512]{1,0:T(8,128)(2,1)S(1)}, bf16[192,512]{1,0:T(8,128)(2,1)S(1)}, u32[]{:S(2)}, u32[]{:S(2)}) collective-permute-start(bf16[192,512]{1,0:T(8,128)(2,1)S(1)} %add_convert_fusion), channel_id=1, source_target_pairs={{0,6},{2,0},{4,2},{6,4},{1,7},{3,1},{5,3},{7,5},{8,14},{10,8},{12,... | collective-permute-start | bytes 589832 | tf_op jit(solution)/shard_map/ppermute | solution.py:423
  127.9 6.2 %collective-permute-start.21 = (bf16[192,512]{1,0:T(8,128)(2,1)S(1)}, bf16[192,512]{1,0:T(8,128)(2,1)S(1)}, u32[]{:S(2)}, u32[]{:S(2)}) collective-permute-start(bf16[192,512]{1,0:T(8,128)(2,1)S(1)} %add_convert_fusion.1), channel_id=1, source_target_pairs={{0,2},{2,4},{4,6},{6,0},{1,3},{3,5},{5,7},{7,1},{8,10},{10,12},{12... | collective-permute-start | bytes 589832 | tf_op jit(solution)/shard_map/ppermute | solution.py:422
  137.1 11.0 %collective-permute-start.23 = (bf16[384,256]{1,0:T(8,128)(2,1)}, bf16[384,256]{1,0:T(8,128)(2,1)S(1)}, u32[]{:S(2)}, u32[]{:S(2)}) collective-permute-start(bf16[384,256]{1,0:T(8,128)(2,1)} %get-tuple-element.69), channel_id=1, source_target_pairs={{0,1},{1,0},{2,3},{3,2},{4,5},{5,4},{6,7},{7,6},{8,9},{9,8},{10,11... | collective-permute-start | bytes 589832 | tf_op jit(solution)/shard_map/ppermute | solution.py:314
  (27 other events, 248.5 us)
Sparse Core Ops, SparseCore 0:
  12.3 75.2 all-gather.2

commit v2 on v1

v2 whole, which is shorter than its diff:
```python
import jax
import jax.numpy as jnp
from jax import lax
from jax.experimental import pallas as pl
from jax.experimental.pallas import tpu as pltpu
from jax.sharding import Mesh
from jax.sharding import PartitionSpec as P

SP = ("z", "y")
TP = ("x", "c")
EPS = 1e-06
BF = jnp.bfloat16
F32 = jnp.float32
VM = pl.BlockSpec(memory_space=pltpu.VMEM)
HB = pl.BlockSpec(memory_space=pltpu.HBM)
SEGS = 8


def cyc(count, step):
    return [(i, (i + step) % count) for i in range(count)]


def stretch(row, lanes=128):
    return jnp.broadcast_to(row, (lanes, 128)).T


def taylor_expm1_neg(y):
    p = 1.0 + y * (1.0 / 8.0)
    for k in (7.0, 6.0, 5.0, 4.0, 3.0, 2.0):
        p = 1.0 + y * (1.0 / k) * p
    return -y * p


def pack_kernel(g_ref, u_ref, d_ref, out_ref):
    for i, ref in enumerate((g_ref, u_ref, d_ref)):
        out_ref[704 * i : 704 * i + 704, :] = ref[...]


def scan_kernel(
    x_ref, rim_ref, ids_ref, taps_ref, gm_ref, im_ref, nsp_ref, extra_ref,
    s_ref, p_ref, e_ref, xs, idx, fs, ds,
):
    rows = x_ref.shape[0]
    taps = taps_ref[...].astype(F32)
    head = gm_ref.shape[1]

    def blockdiag(ref):
        zero = jnp.zeros((head, head), BF)
        return jnp.concatenate(
            [
                jnp.concatenate([ref[0], zero], axis=1),
                jnp.concatenate([zero, ref[1]], axis=1),
            ],
            axis=0,
        )

    gate = blockdiag(gm_ref)
    inp = blockdiag(im_ref)
    xs[0:8, :] = rim_ref[0:8, :]
    idx[0:8, :] = rim_ref[8:16, :]
    for j in range(rows // 128):
        at = 8 + 128 * j
        xs[at : at + 128, :] = x_ref[128 * j : 128 * j + 128, :].astype(F32)
        idx[at : at + 128, :] = stretch(ids_ref[j : j + 1, :])
    for j in range(rows // 128):
        at = 8 + 128 * j
        here = idx[at : at + 128, :]
        before = idx[at - 1 : at + 127, :]
        conv = xs[at : at + 128, :] * taps[0:1, :]
        for k in range(1, 4):
            old = idx[at - k : at - k + 128, :]
            conv = conv + jnp.where(old == here, xs[at - k : at - k + 128, :], 0.0) * taps[k : k + 1, :]
        conv = conv.astype(BF)
        rg = jax.nn.sigmoid(jnp.dot(conv, gate, preferred_element_type=F32))
        ig = jax.nn.sigmoid(jnp.dot(conv, inp, preferred_element_type=F32))
        ld = nsp_ref[...] * rg + extra_ref[128 * j : 128 * j + 128, :]
        e = jnp.exp(ld)
        y = 2.0 * ld
        em = jnp.where(y > -0.5, taylor_expm1_neg(jnp.maximum(y, -0.5)), 1.0 - e * e)
        fs[128 * j : 128 * j + 128, :] = jnp.where(before == here, e, 0.0)
        ds[128 * j : 128 * j + 128, :] = jnp.sqrt(em) * ig * conv.astype(F32)
    seg = rows // SEGS

    def step(j, carry):
        h, p = carry
        f = fs[pl.ds(j, SEGS, stride=seg), :]
        d = ds[pl.ds(j, SEGS, stride=seg), :]
        h = f * h + d
        p = p * f
        s_ref[pl.ds(j, SEGS, stride=seg), :] = h
        p_ref[pl.ds(j, SEGS, stride=seg), :] = p
        return h, p

    zero = jnp.zeros((SEGS, 128), F32)
    h, p = lax.fori_loop(0, seg, step, (zero, zero + 1.0), unroll=8)
    a = p[0:1, :]
    b = h[0:1, :]
    for s in range(1, SEGS):
        b = p[s : s + 1, :] * b + h[s : s + 1, :]
        a = p[s : s + 1, :] * a
    for i in range(16):
        e_ref[i, 0:1, :] = a
        e_ref[i, 1:2, :] = b


def branch_kernel(s_ref, p_ref, e_ref, g_ref, out_ref):
    rows = s_ref.shape[0]
    seg = rows // SEGS
    me = lax.axis_index(SP)
    h = jnp.zeros((1, 128), F32)
    for i in range(16):
        a = e_ref[i, 0:1, :]
        b = e_ref[i, 1:2, :]
        h = jnp.where(i < me, a * h + b, h)
    half = SEGS // 2
    for s in range(SEGS):
        at = s * seg
        st = s_ref[at : at + seg, :]
        pr = p_ref[at : at + seg, :]
        states = st + pr * h
        out = (states * jax.nn.gelu(g_ref[at : at + seg, :].astype(F32), approximate=True)).astype(BF)
        h = states[seg - 1 : seg, :]
        to = (s % half) * seg
        for i in range(4):
            out_ref[2 * i + s // half, to : to + seg, :] = out


def mix_kernel(
    br_ref, w0, w1, w2, w3, v0, v1, v2, v3, g_ref,
    norm_ref, keep_ref, send_ref, full, mixed, stream,
):
    x = lax.axis_index("x")
    c = lax.axis_index("c")
    rows = br_ref.shape[1]
    for i in range(8):
        full[:, 128 * i : 128 * i + 128] = br_ref[i]
    lhs = full[...]
    total = jnp.zeros((rows, 128), F32)
    pieces = []
    for d, w, v, g in ((0, w0, v0, 0), (3, w1, v1, 4), (1, w2, v2, 8), (2, w3, v3, 12)):
        block = lax.rem(x + d, 4)
        for k, core, ref in ((0, c, w), (1, 1 - c, v)):
            at = pl.ds(pl.multiple_of((2 * block + core) * 256, 256), 256)
            pieces.append((at, w, k, g))
            m = jnp.dot(lhs, ref[0:1024, :], preferred_element_type=F32).astype(BF)
            mixed[:, at] = m
            mf = m.astype(F32)
            mf = mf * mf
            total = total + mf[:, :128] + mf[:, 128:]
    scale = lax.rsqrt(jnp.sum(total, axis=1, keepdims=True) / 2048.0 + EPS)
    total = jnp.zeros((rows, 128), F32)
    for at, w, k, g in pieces:
        r = w[1024 + rows * k : 1024 + rows * k + rows, :].astype(F32)
        s = (r + mixed[:, at].astype(F32) * scale * g_ref[g + 2 * k : g + 2 * k + 1, :]).astype(BF)
        stream[:, at] = s
        sf = s.astype(F32)
        sf = sf * sf
        total = total + sf[:, :128] + sf[:, 128:]
    scale = lax.rsqrt(jnp.sum(total, axis=1, keepdims=True) / 2048.0 + EPS)
    for at, w, k, g in pieces:
        norm_ref[:, at] = (stream[:, at].astype(F32) * scale * g_ref[g + 2 * k + 1 : g + 2 * k + 2, :]).astype(BF)
    keep_ref[...] = stream[:, pl.ds(pl.multiple_of((2 * x + c) * 256, 256), 256)]
    send_ref[...] = stream[:, pl.ds(pl.multiple_of((2 * x + 1 - c) * 256, 256), 256)]


def down_copies(w_ref, dn, sem):
    return [
        pltpu.make_async_copy(w_ref.at[s, pl.ds(1408, 704)], dn.at[s], sem) for s in range(16)
    ]


def down_dot(lhs, dn, d):
    first = 4 * lax.rem(lax.axis_index("x") + d, 4)
    part = jnp.concatenate([dn[first + i] for i in range(4)], axis=1)
    return jnp.dot(lhs, part, preferred_element_type=F32).astype(BF)


def ffn_kernel(oth_ref, own_ref, w_ref, foth_ref, fown_ref, hoth, hid_ref, dn, gu, sem):
    cuts = ((0, 128), (128, 384), (384, 704))
    groups = []
    for i, (lo, hi) in enumerate(cuts):
        groups.append(
            [
                pltpu.make_async_copy(
                    w_ref.at[s, pl.ds(base + lo, hi - lo)],
                    gu.at[s, pl.ds(base + lo, hi - lo)],
                    sem.at[i],
                )
                for s in range(16)
                for base in (0, 704)
            ]
        )
    downs = down_copies(w_ref, dn, sem.at[3])
    for group in groups + [downs]:
        for cp in group:
            cp.start()
    turned = (((1,), (1,)), ((), ()))
    for (lo, hi), group in zip(cuts, groups):
        for cp in group:
            cp.wait()
        gate = jnp.concatenate([gu[s, lo:hi, :] for s in range(16)], axis=1)
        up = jnp.concatenate([gu[s, 704 + lo : 704 + hi, :] for s in range(16)], axis=1)
        for src, dst in ((oth_ref, hoth), (own_ref, hid_ref)):
            g = lax.dot_general(src[...], gate, turned, preferred_element_type=F32)
            u = lax.dot_general(src[...], up, turned, preferred_element_type=F32)
            dst[:, lo:hi] = (jax.nn.silu(g) * u).astype(BF)
    for cp in downs:
        cp.wait()
    foth_ref[...] = down_dot(hoth[...], dn, 2)
    fown_ref[...] = down_dot(hid_ref[...], dn, 2)


def down_kernel(hoth_ref, hid_ref, dn, oth_ref, own_ref):
    for src, dst in ((hoth_ref, oth_ref), (hid_ref, own_ref)):
        lhs = src[...]
        for i, d in enumerate((1, 3, 0)):
            dst[i] = down_dot(lhs, dn, d)


def far_kernel(a_ref, b_ref, right_ref, left_ref):
    h = a_ref.shape[0] // 2
    total = a_ref[...].astype(F32) + b_ref[...].astype(F32)
    right_ref[...] = total[:h].astype(BF)
    left_ref[...] = total[h:].astype(BF)


def near_kernel(a_ref, b_ref, right_ref, left_ref, accr_ref, accl_ref, own_ref):
    h = a_ref.shape[1] // 2
    right_ref[...] = (a_ref[0, h:].astype(F32) + b_ref[0, h:].astype(F32)).astype(BF)
    left_ref[...] = (a_ref[1, :h].astype(F32) + b_ref[1, :h].astype(F32)).astype(BF)
    accr_ref[...] = a_ref[0, :h].astype(F32) + b_ref[0, :h].astype(F32)
    accl_ref[...] = a_ref[1, h:].astype(F32) + b_ref[1, h:].astype(F32)
    own_ref[...] = a_ref[2].astype(F32) + b_ref[2].astype(F32)


def relay_kernel(r_ref, l_ref, accr_ref, accl_ref, right_ref, left_ref):
    right_ref[...] = (r_ref[...].astype(F32) + accr_ref[...]).astype(BF)
    left_ref[...] = (l_ref[...].astype(F32) + accl_ref[...]).astype(BF)


def joined_kernel(own_ref, fl_ref, fr_ref, top_ref, bot_ref, keep_ref, send_ref, sq_ref):
    c = lax.axis_index("c")
    q = top_ref.shape[0]
    for k in range(2 * q // 64):
        lo = 64 * k
        at = slice(lo, lo + 64)
        if lo < q:
            more = fr_ref[at, :].astype(F32) + top_ref[at, :].astype(F32)
        else:
            more = fl_ref[lo - q : lo - q + 64, :].astype(F32) + bot_ref[lo - q : lo - q + 64, :].astype(F32)
        v = (own_ref[at, :] + more).astype(BF)
        for first, core in ((0, 0), (256, 1)):

            @pl.when(c == core)
            def _():
                keep_ref[at, :] = v[:, first : first + 256]

            @pl.when(c != core)
            def _():
                send_ref[at, :] = v[:, first : first + 256]

    for k in range(2 * q // 128):
        t = jnp.zeros((128, 128), F32)
        for ref in (keep_ref, send_ref):
            f = ref[128 * k : 128 * k + 128, :].astype(F32)
            f = f * f
            t = t + f[:, :128] + f[:, 128:]
        row = jnp.sum(t.T, axis=0, keepdims=True)
        for i in range(8):
            sq_ref[i, k : k + 1, :] = row


def final_kernel(keep_ref, got_ref, skeep_ref, sgot_ref, sq_ref, gain_ref, out_ref):
    c = lax.axis_index("c")
    half = keep_ref.shape[0]
    for f_ref, s_ref, core in ((keep_ref, skeep_ref, c), (got_ref, sgot_ref, 1 - c)):
        total = sq_ref[core]
        for i in range(1, 4):
            total = total + sq_ref[2 * i + core]
        scale = lax.rsqrt(total / 2048.0 + EPS)
        for k in range(half // 128):
            at = slice(128 * k, 128 * k + 128)
            col = stretch(scale[k : k + 1, :])
            for j in range(2):
                ln = slice(128 * j, 128 * j + 128)
                v = s_ref[at, ln].astype(F32) + f_ref[at, ln].astype(F32) * col * gain_ref[:, ln]
                out_ref[pl.ds(pl.multiple_of(core * half + 128 * k, 128), 128), ln] = v.astype(BF)


def call(fn, outs, specs, scratch=(), limit=8):
    return pl.pallas_call(
        fn,
        out_shape=tuple(jax.ShapeDtypeStruct(s, d) for s, d in outs),
        in_specs=list(specs),
        out_specs=tuple(VM for _ in outs),
        scratch_shapes=list(scratch),
        compiler_params=pltpu.CompilerParams(vmem_limit_bytes=limit << 20),
    )


def kept_in_hbm(*arrays):
    return [pltpu.with_memory_space_constraint(a, pltpu.HBM) for a in arrays]


def swapped(block):
    return lax.ppermute(block, "c", cyc(2, 1))


def steps(
    gate_branch, recur_input, doc_ids, conv_taps, gate_map, input_map, decay_level, decay_extra,
    out_weight, residual, mix_gain, pre_gain, ffn_gain, gate_weight, up_weight, down_weight,
):
    rows, width = recur_input.shape
    half = rows // 2
    c = lax.axis_index("c")

    (stacked,) = call(
        pack_kernel, [((2112, 128), BF)], [VM] * 3
    )(*kept_in_hbm(gate_weight.T, up_weight.T, down_weight))
    (weights,) = kept_in_hbm(lax.all_gather(stacked, SP, axis=0))

    res_keep = lax.dynamic_slice_in_dim(residual, c * half, half, 0)
    res_send = lax.dynamic_slice_in_dim(residual, (1 - c) * half, half, 0)
    ahead = jnp.concatenate([out_weight, res_keep, swapped(res_send)])
    from_left = lax.ppermute(ahead, "x", cyc(4, 1))
    from_right = lax.ppermute(ahead, "x", cyc(4, 3))
    gains = jnp.stack([mix_gain, pre_gain])
    gains = jnp.concatenate([gains, swapped(gains)])
    all_gains = [gains]
    for d in (1, 3, 2):
        all_gains.append(lax.ppermute(gains, "x", cyc(4, d)))

    tail = jnp.pad(recur_input[rows - 3 :].astype(F32), ((5, 0), (0, 0)))
    tail_ids = jnp.pad(
        jnp.broadcast_to(doc_ids[rows - 3 :].astype(F32)[:, None], (3, width)), ((5, 0), (0, 0))
    )
    rim = lax.ppermute(
        jnp.concatenate([tail, tail_ids]), SP, [(i, i + 1) for i in range(15)]
    )
    nsp = (-8.0 * jax.nn.softplus(-decay_level))[None, :]
    states, products, ends = call(
        scan_kernel,
        [((rows, width), F32), ((rows, width), F32), ((16, 2, width), F32)],
        [VM] * 8,
        [
            pltpu.VMEM((rows + 8, width), F32),
            pltpu.VMEM((rows + 8, width), F32),
            pltpu.VMEM((rows, width), F32),
            pltpu.VMEM((rows, width), F32),
        ],
    )(
        *kept_in_hbm(recur_input),
        rim,
        doc_ids.astype(F32).reshape(rows // 128, 128),
        *kept_in_hbm(conv_taps, gate_map, input_map),
        nsp,
        *kept_in_hbm(decay_extra),
    )
    all_ends = lax.all_to_all(ends, SP, 0, 0, tiled=True)
    (branch,) = call(branch_kernel, [((8, half, width), BF)], [VM] * 4)(
        states, products, all_ends, *kept_in_hbm(gate_branch)
    )
    branch = lax.all_to_all(branch, TP, 0, 0, tiled=True)
    cut = from_left.shape[0] // 2
    far_top = lax.ppermute(from_left[:cut], "x", cyc(4, 1))
    far_bottom = lax.ppermute(from_right[cut:], "x", cyc(4, 3))
    far = jnp.concatenate([far_top, far_bottom])
    blocks = [ahead, from_left, from_right, far]
    others = [swapped(b) for b in blocks[:3]]
    others.append(swapped(far))
    norm_own, skeep, ssend = call(
        mix_kernel,
        [((half, 2048), BF), ((half, 256), BF), ((half, 256), BF)],
        [VM] * 10,
        [
            pltpu.VMEM((half, 1024), BF),
            pltpu.VMEM((half, 2048), BF),
            pltpu.VMEM((half, 2048), BF),
        ],
        limit=12,
    )(branch, *blocks, *others, jnp.concatenate(all_gains))
    norm_oth = swapped(norm_own)
    sgot = swapped(ssend)

    far_oth, far_own, hid_oth, hid_own, down = call(
        ffn_kernel,
        [((half, 512), BF)] * 2 + [((half, 704), BF)] * 2 + [((16, 704, 128), BF)],
        [VM, VM, HB],
        [pltpu.VMEM((16, 1408, 128), BF), pltpu.SemaphoreType.DMA((4,))],
        limit=15,
    )(norm_oth, norm_own, weights)
    far_in = swapped(far_oth)
    rest_oth, rest_own = call(
        down_kernel, [((3, half, 512), BF)] * 2, [VM] * 3, limit=14
    )(hid_oth, hid_own, down)
    rest_in = swapped(rest_oth)
    q = half // 2
    far_r, far_l = call(far_kernel, [((q, 512), BF)] * 2, [VM] * 2)(far_own, far_in)
    pass_r = lax.ppermute(far_r, "x", cyc(4, 1))
    pass_l = lax.ppermute(far_l, "x", cyc(4, 3))
    near_r, near_l, acc_r, acc_l, own = call(
        near_kernel,
        [((q, 512), BF)] * 2 + [((q, 512), F32)] * 2 + [((half, 512), F32)],
        [VM] * 2,
        limit=10,
    )(rest_own, rest_in)
    from_left = lax.ppermute(near_r, "x", cyc(4, 1))
    from_right = lax.ppermute(near_l, "x", cyc(4, 3))
    pass_r, pass_l = lax.optimization_barrier((pass_r, pass_l))
    right2, left2 = call(relay_kernel, [((q, 512), BF)] * 2, [VM] * 4)(pass_r, pass_l, acc_r, acc_l)
    top = lax.ppermute(right2, "x", cyc(4, 1))
    bottom = lax.ppermute(left2, "x", cyc(4, 3))
    from_left, from_right, top, bottom = lax.optimization_barrier(
        (from_left, from_right, top, bottom)
    )
    fkeep, fsend, square = call(
        joined_kernel,
        [((half, 256), BF)] * 2 + [((8, 3, 128), F32)],
        [VM] * 5,
    )(own, from_left, from_right, top, bottom)
    fgot = swapped(fsend)
    square = lax.all_to_all(square, TP, 0, 0, tiled=True)
    (out,) = call(final_kernel, [((rows, 256), BF)], [VM] * 6)(
        fkeep, fgot, skeep, sgot, square, ffn_gain[None, :]
    )
    return out


def solution(mesh):
    split = Mesh(mesh.devices.reshape(4, 4, 4, 2), ("z", "y", "x", "c"))
    return jax.shard_map(
        steps,
        mesh=split,
        in_specs=(
            P(SP, TP), P(SP, TP), P(SP), P(None, TP), P(TP, None, None), P(TP, None, None), P(TP),
            P(SP, TP), P(None, TP), P(SP, TP), P(TP), P(TP), P(TP), P(SP, TP), P(SP, TP), P(TP, SP),
        ),
        out_specs=P(SP, TP),
        check_vma=False,
    )
```

time: 159 us -> 163 us (1.025)
  waiting for transfers between devices: 33.4 us -> 52.8 us
  Pallas kernels: 44.1 us -> 26.3 us
  blocking collectives: 8.57 us -> 14.3 us
  starting transfers between devices: 42.5 us -> 47 us
  other arithmetic: 4.12 us -> 0.32 us
  local copies, waits for them, and re-layouts: 11.5 us -> 7.81 us
    ppermute x14, waiting for transfers between devices: 11.9 us -> 41.2 us  [the longest x1 19.4 us: steps(): from_left = lax.ppermute(ahead, 'x', cyc(4, 1))]
    pallas_call x10 -> x11, Pallas kernels: 44.1 us -> 26.3 us  [the longest x1 9.03 us: steps(): call(ffn_kernel, [((half, 512), BF)] * 2 + [((half, 704), BF)] * 2 + [((1...]
    all_to_all x2, waiting for transfers between devices: 18 us -> 4.65 us  [the longest x1 4.65 us: steps(): square = lax.all_to_all(square, TP, 0, 0, tiled=True)]
    all_to_all x1, blocking collectives: 8.57 us -> 14.3 us  [steps(): all_ends = lax.all_to_all(ends, SP, 0, 0, tiled=True)]
    ppermute x14, starting transfers between devices: 18.9 us -> 24.2 us  [the longest x3 6.51 us: steps(): all_gains.append(lax.ppermute(gains, 'x', cyc(4, d)))]
    unnamed x51 -> x33, local copies, waits for them, and re-layouts: 9.84 us -> 4.8 us
    ppermute x10 -> x11, waiting for transfers between devices: 3.51 us -> 6.91 us  [swapped(): return lax.ppermute(block, 'c', cyc(2, 1))]
    convert_element_type x3 -> x1, other arithmetic: 2.14 us -> 0.07 us  [steps(): doc_ids[rows - 3:].astype(F32)[:, None]]
  transfers between devices with their start and end apart: 27 -> 28, of which waited for: 8 -> 12; matrix products, arithmetic and copies ran while one was open for 4% -> 3% of each run, Pallas kernels for 15% -> 7%
where the time goes in v2:
time: 163 us; the launch traced here: 162 us
  waiting for transfers between devices  52.8 us (32%)
  starting transfers between devices  47 us (29%)
  Pallas kernels  26.3 us (16%)
  blocking collectives  14.3 us (9%)
  between operations  13.6 us (8%)
  local copies, waits for them, and re-layouts  7.81 us (5%)
    ppermute x1, waiting for transfers between devices, steps(): from_left = lax.ppermute(ahead, 'x', cyc(4, 1))  19.4 us
    all_to_all x1, blocking collectives, steps(): all_ends = lax.all_to_all(ends, SP, 0, 0, tiled=True)  14.3 us
    ppermute x11, starting transfers between devices, swapped(): return lax.ppermute(block, 'c', cyc(2, 1))  13.1 us
    ppermute x3, waiting for transfers between devices, steps(): all_gains.append(lax.ppermute(gains, 'x', cyc(4, d)))  9.69 us
    pallas_call x1, Pallas kernels, steps(): call(ffn_kernel, [((half, 512), BF)] * 2 + [((half, 704), BF)] * 2 + [((1...  9.03 us
    ppermute x11, waiting for transfers between devices, swapped(): return lax.ppermute(block, 'c', cyc(2, 1))  6.91 us
    ppermute x3, starting transfers between devices, steps(): all_gains.append(lax.ppermute(gains, 'x', cyc(4, d)))  6.51 us
    pallas_call x1, Pallas kernels, steps(): call(mix_kernel, [((half, 2048), BF), ((half, 256), BF), ((half, 256), BF...  5.87 us
  transfers between devices with their start and end apart: 28, of which 12 were waited for; matrix products, arithmetic and copies ran while one was open for 3% of the time, Pallas kernels for 7%

profile of v2, /device:TPU:1, one launch (start us, length us, event | category | flops | bytes accessed | tf_op | source)
XLA Modules:
  0.0 162.2 jit_solution(4789174101328936962)
XLA Ops:
  14.8 19.4 %collective-permute-done.2.w1 = bf16[1792,256]{1,0:T(8,128)(2,1)S(1)} collective-permute-done((bf16[1792,256]{1,0:T(8,128)(2,1)S(1)}, bf16[1792,256]{1,0:T(8,128)(2,1)S(1)}, u32[]{:S(2)}, u32[]{:S(2)}) %collective-permute-start.2) | collective-permute-done | bytes 917536 | tf_op jit(solution)/shard_map/ppermute | solution.py:325
  34.5 2.6 %collective-permute-start.5 = (bf16[896,256]{1,0:T(8,128)(2,1)S(1)}, bf16[896,256]{1,0:T(8,128)(2,1)S(1)}, u32[]{:S(2)}, u32[]{:S(2)}) collective-permute-start(bf16[896,256]{1,0:T(8,128)(2,1)S(1)} %slice.17), channel_id=1, source_target_pairs={{0,6},{2,0},{4,2},{6,4},{1,7},{3,1},{5,3},{7,5},{8,14},{10,8},{12,... | collective-permute-start | bytes 1376264 | tf_op jit(solution)/shard_map/ppermute | solution.py:366
  37.2 3.3 %collective-permute-start = (f32[16,128]{1,0:T(8,128)S(1)}, f32[16,128]{1,0:T(8,128)S(1)}, u32[]{:S(2)}, u32[]{:S(2)}) collective-permute-start(f32[16,128]{1,0:T(8,128)S(1)} %pad_maximum_fusion.1), channel_id=1, source_target_pairs={{0,8},{8,16},{16,24},{24,32},{32,40},{40,48},{48,56},{56,64},{64,7... | collective-permute-start | bytes 24584 | tf_op jit(solution)/shard_map/ppermute | solution.py:337
  40.5 2.0 %collective-permute-start.6 = (bf16[1792,256]{1,0:T(8,128)(2,1)S(1)}, bf16[1792,256]{1,0:T(8,128)(2,1)}, u32[]{:S(2)}, u32[]{:S(2)}) collective-permute-start(bf16[1792,256]{1,0:T(8,128)(2,1)S(1)} %pad_maximum_fusion.w0), channel_id=1, source_target_pairs={{0,1},{1,0},{2,3},{3,2},{4,5},{5,4},{6,7},{7,6},{8,9},{9,8},{10,11... | collective-permute-start | bytes 2752520 | tf_op jit(solution)/shard_map/ppermute | solution.py:306
  42.6 3.8 %collective-permute-done.4 = bf16[896,256]{1,0:T(8,128)(2,1)S(1)} collective-permute-done((bf16[896,256]{1,0:T(8,128)(2,1)S(1)}, bf16[896,256]{1,0:T(8,128)(2,1)S(1)}, u32[]{:S(2)}, u32[]{:S(2)}) %collective-permute-start.4) | collective-permute-done | bytes 458784 | tf_op jit(solution)/shard_map/ppermute | solution.py:365
  50.1 3.0 %shard_map.154 = (f32[768,128]{1,0:T(8,128)S(1)}, f32[768,128]{1,0:T(8,128)S(1)}, f32[16,2,128]{2,1,0:T(2,128)S(1)}) custom-call(bf16[768,128]{1,0:T(8,128)(2,1)} %x_ref.1, f32[16,128]{1,0:T(8,128)S(1)} %collective-permute-done.rim_ref, f32[6,128]{1,0:T(8,128)S(1)} %convert_bitcast_fusion.ids_ref, bf16[4,128]{1,0:T(4,128)(2,1)} %taps_ref.1, ...), custom_call_target="tpu_custom_call" | custom-call | tf_op jit(solution)/shard_map/pallas_call | solution.py:341
  53.1 14.3 %all_to_all.15.e_ref = f32[16,2,128]{2,1,0:T(2,128)S(1)} all-to-all(f32[16,2,128]{2,1,0:T(2,128)S(1)} %get-tuple-element.38), channel_id=1, replica_groups=mesh['z'=4,'y'=4,'x'=4,'c'=2] {'z','y'}, dimensions={0} | all-to-all | bytes 32768 | tf_op jit(solution)/shard_map/all_to_all | solution.py:359
  67.4 2.0 %shard_map.155 = bf16[8,384,128]{2,1,0:T(8,128)(2,1)} custom-call(f32[768,128]{1,0:T(8,128)S(1)} %get-tuple-element.36.s_ref, f32[768,128]{1,0:T(8,128)S(1)} %get-tuple-element.37.p_ref, f32[16,2,128]{2,1,0:T(2,128)S(1)} %all_to_all.15.e_ref, bf16[768,128]{1,0:T(8,128)(2,1)} %g_ref.1), custom_call_target="tpu_custom_call" | custom-call | tf_op jit(solution)/shard_map/pallas_call | solution.py:360
  69.4 5.4 %all-to-all-start.1 = ((bf16[8,384,128]{2,1,0:T(8,128)(2,1)}), bf16[8,384,128]{2,1,0:T(8,128)(2,1)S(1)}, u32[]{:S(2)}, u32[]{:S(2)}) async-start(bf16[8,384,128]{2,1,0:T(8,128)(2,1)} %shard_map.155), calls=%async_computation.1 | async-start | bytes 1572864 | tf_op jit(solution)/shard_map/all_to_all | solution.py:363
  77.7 6.3 %collective-permute-done.11 = f32[4,256]{1,0:T(4,128)S(1)} collective-permute-done((f32[4,256]{1,0:T(4,128)S(1)}, f32[4,256]{1,0:T(4,128)S(1)}, u32[]{:S(2)}, u32[]{:S(2)}) %collective-permute-start.11) | collective-permute-done | bytes 4128 | tf_op jit(solution)/shard_map/ppermute | solution.py:331
  84.0 3.5 %collective-permute-start.12 = (f32[4,256]{1,0:T(4,128)S(1)}, f32[4,256]{1,0:T(4,128)S(1)}, u32[]{:S(2)}, u32[]{:S(2)}) collective-permute-start(f32[4,256]{1,0:T(4,128)S(1)} %pad_maximum_fusion.2), channel_id=1, source_target_pairs={{0,6},{2,0},{4,2},{6,4},{1,7},{3,1},{5,3},{7,5},{8,14},{10,8},{12,... | collective-permute-start | bytes 12296 | tf_op jit(solution)/shard_map/ppermute | solution.py:331
  89.7 2.6 %collective-permute-done.13 = f32[4,256]{1,0:T(4,128)} collective-permute-done((f32[4,256]{1,0:T(4,128)S(1)}, f32[4,256]{1,0:T(4,128)}, u32[]{:S(2)}, u32[]{:S(2)}) %collective-permute-start.13) | collective-permute-done | bytes 4128 | tf_op jit(solution)/shard_map/ppermute | solution.py:331
  93.8 5.9 %shard_map.156 = (bf16[384,2048]{1,0:T(8,128)(2,1)S(1)}, bf16[384,256]{1,0:T(8,128)(2,1)S(1)}, bf16[384,256]{1,0:T(8,128)(2,1)S(1)}) custom-call(bf16[8,384,128]{2,1,0:T(8,128)(2,1)S(1)} %all-to-all-done.1.br_ref, bf16[1792,256]{1,0:T(8,128)(2,1)S(1)} %pad_maximum_fusion.w0, bf16[1792,256]{1,0:T(8,128)(2,1)S(1)} %collective-permute-done.2.w1, ...), custom_call_target="tpu_custom_call" | custom-call | tf_op jit(solution)/shard_map/pallas_call | solution.py:371
  101.0 2.9 %collective-permute-start.14 = (bf16[384,2048]{1,0:T(8,128)(2,1)S(1)}, bf16[384,2048]{1,0:T(8,128)(2,1)S(1)}, u32[]{:S(2)}, u32[]{:S(2)}) collective-permute-start(bf16[384,2048]{1,0:T(8,128)(2,1)S(1)} %get-tuple-element.39.own_ref), channel_id=1, source_target_pairs={{0,1},{1,0},{2,3},{3,2},{4,5},{5,4},{6,7},{7,6},{8,9},{9,8},{10,11... | collective-permute-start | bytes 4718600 | tf_op jit(solution)/shard_map/ppermute | solution.py:306
  108.3 9.0 %shard_map.158 = (bf16[384,512]{1,0:T(8,128)(2,1)S(1)}, bf16[384,512]{1,0:T(8,128)(2,1)S(1)}, bf16[384,704]{1,0:T(8,128)(2,1)S(1)}, bf16[384,704]{1,0:T(8,128)(2,1)S(1)}, bf16[16,704,128]{2,1,0:T(8,128)(2,1)S(1)}) custom-call(bf16[384,2048]{1,0:T(8,128)(2,1)S(1)} %collective-permute-done.14.oth_ref, bf16[384,2048]{1,0:T(8,128)(2,1)S(1)} %copy-done.1, ...), custom_call_target="tpu_custom_call" | custom-call | tf_op jit(solution)/shard_map/pallas_call | solution.py:385
  120.0 2.9 %collective-permute-done.18.b_ref = bf16[384,512]{1,0:T(8,128)(2,1)S(1)} collective-permute-done((bf16[384,512]{1,0:T(8,128)(2,1)S(1)}, bf16[384,512]{1,0:T(8,128)(2,1)S(1)}, u32[]{:S(2)}, u32[]{:S(2)}) %collective-permute-start.18) | collective-permute-done | bytes 393248 | tf_op jit(solution)/shard_map/ppermute | solution.py:306
  123.6 2.8 %collective-permute-start.20 = (bf16[192,512]{1,0:T(8,128)(2,1)S(1)}, bf16[192,512]{1,0:T(8,128)(2,1)S(1)}, u32[]{:S(2)}, u32[]{:S(2)}) collective-permute-start(bf16[192,512]{1,0:T(8,128)(2,1)S(1)} %get-tuple-element.51), channel_id=1, source_target_pairs={{0,6},{2,0},{4,2},{6,4},{1,7},{3,1},{5,3},{7,5},{8,14},{10,8},{12,... | collective-permute-start | bytes 589832 | tf_op jit(solution)/shard_map/ppermute | solution.py:400
  126.4 4.8 %collective-permute-done.19.r_ref = bf16[192,512]{1,0:T(8,128)(2,1)S(1)} collective-permute-done((bf16[192,512]{1,0:T(8,128)(2,1)S(1)}, bf16[192,512]{1,0:T(8,128)(2,1)S(1)}, u32[]{:S(2)}, u32[]{:S(2)}) %collective-permute-start.19) | collective-permute-done | bytes 196640 | tf_op jit(solution)/shard_map/ppermute | solution.py:399
  132.2 2.1 %collective-permute-start.22 = (bf16[192,512]{1,0:T(8,128)(2,1)S(1)}, bf16[192,512]{1,0:T(8,128)(2,1)S(1)}, u32[]{:S(2)}, u32[]{:S(2)}) collective-permute-start(bf16[192,512]{1,0:T(8,128)(2,1)S(1)} %get-tuple-element.57), channel_id=1, source_target_pairs={{0,6},{2,0},{4,2},{6,4},{1,7},{3,1},{5,3},{7,5},{8,14},{10,8},{12,... | collective-permute-start | bytes 589832 | tf_op jit(solution)/shard_map/ppermute | solution.py:412
  134.3 2.7 %collective-permute-start.17 = (bf16[192,512]{1,0:T(8,128)(2,1)S(1)}, bf16[192,512]{1,0:T(8,128)(2,1)S(1)}, u32[]{:S(2)}, u32[]{:S(2)}) collective-permute-start(bf16[192,512]{1,0:T(8,128)(2,1)S(1)} %get-tuple-element.47), channel_id=1, source_target_pairs={{0,6},{2,0},{4,2},{6,4},{1,7},{3,1},{5,3},{7,5},{8,14},{10,8},{12,... | collective-permute-start | bytes 589832 | tf_op jit(solution)/shard_map/ppermute | solution.py:408
  137.0 2.1 %collective-permute-start.24 = (bf16[384,256]{1,0:T(8,128)(2,1)S(1)}, bf16[384,256]{1,0:T(8,128)(2,1)S(1)}, u32[]{:S(2)}, u32[]{:S(2)}) collective-permute-start(bf16[384,256]{1,0:T(8,128)(2,1)S(1)} %copy-done.6), channel_id=1, source_target_pairs={{0,1},{1,0},{2,3},{3,2},{4,5},{5,4},{6,7},{7,6},{8,9},{9,8},{10,11... | collective-permute-start | bytes 589832 | tf_op jit(solution)/shard_map/ppermute | solution.py:306
  139.0 3.5 %collective-permute-done.16.fl_ref = bf16[192,512]{1,0:T(8,128)(2,1)S(1)} collective-permute-done((bf16[192,512]{1,0:T(8,128)(2,1)S(1)}, bf16[192,512]{1,0:T(8,128)(2,1)S(1)}, u32[]{:S(2)}, u32[]{:S(2)}) %collective-permute-start.16) | collective-permute-done | bytes 196640 | tf_op jit(solution)/shard_map/ppermute | solution.py:407
  145.3 4.3 %all-to-all-start.2 = ((f32[8,3,128]{2,1,0:T(4,128)}), f32[8,3,128]{2,1,0:T(4,128)S(1)}, u32[]{:S(2)}, u32[]{:S(2)}) async-start(f32[8,3,128]{2,1,0:T(4,128)} %get-tuple-element.66), calls=%async_computation.2 | async-start | bytes 32768 | tf_op jit(solution)/shard_map/all_to_all | solution.py:422
  149.7 4.7 %all-to-all-done.2.sq_ref = f32[8,3,128]{2,1,0:T(4,128)S(1)} async-done(((f32[8,3,128]{2,1,0:T(4,128)}), f32[8,3,128]{2,1,0:T(4,128)S(1)}, u32[]{:S(2)}, u32[]{:S(2)}) %all-to-all-start.2) | async-done | bytes 12320 | tf_op jit(solution)/shard_map/all_to_all | solution.py:422
  (93 shorter events, 32.6 us)
Async XLA Ops:
  6.5 100.4 %all-gather.3.cloned.1.call-start = ((), (), s32[]{:S(2)}) async-start(), calls=%async_computation.3 | async-start | bytes 9191424 | tf_op jit(solution)/shard_map/all_gather | solution.py:320
  11.2 22.9 %collective-permute-start.2 = (bf16[1792,256]{1,0:T(8,128)(2,1)S(1)}, bf16[1792,256]{1,0:T(8,128)(2,1)S(1)}, u32[]{:S(2)}, u32[]{:S(2)}) collective-permute-start(bf16[1792,256]{1,0:T(8,128)(2,1)S(1)} %pad_maximum_fusion.w0), channel_id=1, source_target_pairs={{0,2},{2,4},{4,6},{6,0},{1,3},{3,5},{5,7},{7,1},{8,10},{10,12},{12... | collective-permute-start | bytes 2752520 | tf_op jit(solution)/shard_map/ppermute | solution.py:325
  12.6 21.8 %collective-permute-start.3 = (bf16[1792,256]{1,0:T(8,128)(2,1)S(1)}, bf16[1792,256]{1,0:T(8,128)(2,1)S(1)}, u32[]{:S(2)}, u32[]{:S(2)}) collective-permute-start(bf16[1792,256]{1,0:T(8,128)(2,1)S(1)} %pad_maximum_fusion.w0), channel_id=1, source_target_pairs={{0,6},{2,0},{4,2},{6,4},{1,7},{3,1},{5,3},{7,5},{8,14},{10,8},{12,... | collective-permute-start | bytes 2752520 | tf_op jit(solution)/shard_map/ppermute | solution.py:326
  34.2 12.2 %collective-permute-start.4 = (bf16[896,256]{1,0:T(8,128)(2,1)S(1)}, bf16[896,256]{1,0:T(8,128)(2,1)S(1)}, u32[]{:S(2)}, u32[]{:S(2)}) collective-permute-start(bf16[896,256]{1,0:T(8,128)(2,1)S(1)} %slice.16), channel_id=1, source_target_pairs={{0,2},{2,4},{4,6},{6,0},{1,3},{3,5},{5,7},{7,1},{8,10},{10,12},{12... | collective-permute-start | bytes 1376264 | tf_op jit(solution)/shard_map/ppermute | solution.py:365
  34.5 14.8 %collective-permute-start.5 = (bf16[896,256]{1,0:T(8,128)(2,1)S(1)}, bf16[896,256]{1,0:T(8,128)(2,1)S(1)}, u32[]{:S(2)}, u32[]{:S(2)}) collective-permute-start(bf16[896,256]{1,0:T(8,128)(2,1)S(1)} %slice.17), channel_id=1, source_target_pairs={{0,6},{2,0},{4,2},{6,4},{1,7},{3,1},{5,3},{7,5},{8,14},{10,8},{12,... | collective-permute-start | bytes 1376264 | tf_op jit(solution)/shard_map/ppermute | solution.py:366
  37.2 12.9 %collective-permute-start = (f32[16,128]{1,0:T(8,128)S(1)}, f32[16,128]{1,0:T(8,128)S(1)}, u32[]{:S(2)}, u32[]{:S(2)}) collective-permute-start(f32[16,128]{1,0:T(8,128)S(1)} %pad_maximum_fusion.1), channel_id=1, source_target_pairs={{0,8},{8,16},{16,24},{24,32},{32,40},{40,48},{48,56},{56,64},{64,7... | collective-permute-start | bytes 24584 | tf_op jit(solution)/shard_map/ppermute | solution.py:337
  40.5 53.2 %collective-permute-start.6 = (bf16[1792,256]{1,0:T(8,128)(2,1)S(1)}, bf16[1792,256]{1,0:T(8,128)(2,1)}, u32[]{:S(2)}, u32[]{:S(2)}) collective-permute-start(bf16[1792,256]{1,0:T(8,128)(2,1)S(1)} %pad_maximum_fusion.w0), channel_id=1, source_target_pairs={{0,1},{1,0},{2,3},{3,2},{4,5},{5,4},{6,7},{7,6},{8,9},{9,8},{10,11... | collective-permute-start | bytes 2752520 | tf_op jit(solution)/shard_map/ppermute | solution.py:306
  42.6 51.2 %collective-permute-start.7 = (bf16[1792,256]{1,0:T(8,128)(2,1)S(1)}, bf16[1792,256]{1,0:T(8,128)(2,1)}, u32[]{:S(2)}, u32[]{:S(2)}) collective-permute-start(bf16[1792,256]{1,0:T(8,128)(2,1)S(1)} %collective-permute-done.2.w1), channel_id=1, source_target_pairs={{0,1},{1,0},{2,3},{3,2},{4,5},{5,4},{6,7},{7,6},{8,9},{9,8},{10,11... | collective-permute-start | bytes 2752520 | tf_op jit(solution)/shard_map/ppermute | solution.py:306
  46.4 47.3 %collective-permute-start.8 = (bf16[1792,256]{1,0:T(8,128)(2,1)S(1)}, bf16[1792,256]{1,0:T(8,128)(2,1)}, u32[]{:S(2)}, u32[]{:S(2)}) collective-permute-start(bf16[1792,256]{1,0:T(8,128)(2,1)S(1)} %collective-permute-done.3.w2), channel_id=1, source_target_pairs={{0,1},{1,0},{2,3},{3,2},{4,5},{5,4},{6,7},{7,6},{8,9},{9,8},{10,11... | collective-permute-start | bytes 2752520 | tf_op jit(solution)/shard_map/ppermute | solution.py:306
  50.0 43.8 %collective-permute-start.9 = (bf16[1792,256]{1,0:T(8,128)(2,1)}, bf16[1792,256]{1,0:T(8,128)(2,1)}, u32[]{:S(2)}, u32[]{:S(2)}) collective-permute-start(bf16[1792,256]{1,0:T(8,128)(2,1)} %constant_dynamic-update-slice_fusion.w3), channel_id=1, source_target_pairs={{0,1},{1,0},{2,3},{3,2},{4,5},{5,4},{6,7},{7,6},{8,9},{9,8},{10,11... | collective-permute-start | bytes 2752520 | tf_op jit(solution)/shard_map/ppermute | solution.py:306
  69.4 24.3 %all-to-all-start.1 = ((bf16[8,384,128]{2,1,0:T(8,128)(2,1)}), bf16[8,384,128]{2,1,0:T(8,128)(2,1)S(1)}, u32[]{:S(2)}, u32[]{:S(2)}) async-start(bf16[8,384,128]{2,1,0:T(8,128)(2,1)} %shard_map.155), calls=%async_computation.1 | async-start | bytes 1572864 | tf_op jit(solution)/shard_map/all_to_all | solution.py:363
  76.1 7.9 %collective-permute-start.11 = (f32[4,256]{1,0:T(4,128)S(1)}, f32[4,256]{1,0:T(4,128)S(1)}, u32[]{:S(2)}, u32[]{:S(2)}) collective-permute-start(f32[4,256]{1,0:T(4,128)S(1)} %pad_maximum_fusion.2), channel_id=1, source_target_pairs={{0,2},{2,4},{4,6},{6,0},{1,3},{3,5},{5,7},{7,1},{8,10},{10,12},{12... | collective-permute-start | bytes 12296 | tf_op jit(solution)/shard_map/ppermute | solution.py:331
  84.0 4.3 %collective-permute-start.12 = (f32[4,256]{1,0:T(4,128)S(1)}, f32[4,256]{1,0:T(4,128)S(1)}, u32[]{:S(2)}, u32[]{:S(2)}) collective-permute-start(f32[4,256]{1,0:T(4,128)S(1)} %pad_maximum_fusion.2), channel_id=1, source_target_pairs={{0,6},{2,0},{4,2},{6,4},{1,7},{3,1},{5,3},{7,5},{8,14},{10,8},{12,... | collective-permute-start | bytes 12296 | tf_op jit(solution)/shard_map/ppermute | solution.py:331
  101.0 5.9 %collective-permute-start.14 = (bf16[384,2048]{1,0:T(8,128)(2,1)S(1)}, bf16[384,2048]{1,0:T(8,128)(2,1)S(1)}, u32[]{:S(2)}, u32[]{:S(2)}) collective-permute-start(bf16[384,2048]{1,0:T(8,128)(2,1)S(1)} %get-tuple-element.39.own_ref), channel_id=1, source_target_pairs={{0,1},{1,0},{2,3},{3,2},{4,5},{5,4},{6,7},{7,6},{8,9},{9,8},{10,11... | collective-permute-start | bytes 4718600 | tf_op jit(solution)/shard_map/ppermute | solution.py:306
  119.4 11.8 %collective-permute-start.15 = (bf16[3,384,512]{2,1,0:T(8,128)(2,1)S(1)}, bf16[3,384,512]{2,1,0:T(8,128)(2,1)S(1)}, u32[]{:S(2)}, u32[]{:S(2)}) collective-permute-start(bf16[3,384,512]{2,1,0:T(8,128)(2,1)S(1)} %get-tuple-element.44), channel_id=1, source_target_pairs={{0,1},{1,0},{2,3},{3,2},{4,5},{5,4},{6,7},{7,6},{8,9},{9,8},{10,11... | collective-permute-start | bytes 3538952 | tf_op jit(solution)/shard_map/ppermute | solution.py:306
  123.0 8.2 %collective-permute-start.19 = (bf16[192,512]{1,0:T(8,128)(2,1)S(1)}, bf16[192,512]{1,0:T(8,128)(2,1)S(1)}, u32[]{:S(2)}, u32[]{:S(2)}) collective-permute-start(bf16[192,512]{1,0:T(8,128)(2,1)S(1)} %get-tuple-element.50), channel_id=1, source_target_pairs={{0,2},{2,4},{4,6},{6,0},{1,3},{3,5},{5,7},{7,1},{8,10},{10,12},{12... | collective-permute-start | bytes 589832 | tf_op jit(solution)/shard_map/ppermute | solution.py:399
  123.6 7.6 %collective-permute-start.20 = (bf16[192,512]{1,0:T(8,128)(2,1)S(1)}, bf16[192,512]{1,0:T(8,128)(2,1)S(1)}, u32[]{:S(2)}, u32[]{:S(2)}) collective-permute-start(bf16[192,512]{1,0:T(8,128)(2,1)S(1)} %get-tuple-element.51), channel_id=1, source_target_pairs={{0,6},{2,0},{4,2},{6,4},{1,7},{3,1},{5,3},{7,5},{8,14},{10,8},{12,... | collective-permute-start | bytes 589832 | tf_op jit(solution)/shard_map/ppermute | solution.py:400
  131.5 7.5 %collective-permute-start.21 = (bf16[192,512]{1,0:T(8,128)(2,1)S(1)}, bf16[192,512]{1,0:T(8,128)(2,1)S(1)}, u32[]{:S(2)}, u32[]{:S(2)}) collective-permute-start(bf16[192,512]{1,0:T(8,128)(2,1)S(1)} %get-tuple-element.56), channel_id=1, source_target_pairs={{0,2},{2,4},{4,6},{6,0},{1,3},{3,5},{5,7},{7,1},{8,10},{10,12},{12... | collective-permute-start | bytes 589832 | tf_op jit(solution)/shard_map/ppermute | solution.py:411
  132.2 6.9 %collective-permute-start.22 = (bf16[192,512]{1,0:T(8,128)(2,1)S(1)}, bf16[192,512]{1,0:T(8,128)(2,1)S(1)}, u32[]{:S(2)}, u32[]{:S(2)}) collective-permute-start(bf16[192,512]{1,0:T(8,128)(2,1)S(1)} %get-tuple-element.57), channel_id=1, source_target_pairs={{0,6},{2,0},{4,2},{6,4},{1,7},{3,1},{5,3},{7,5},{8,14},{10,8},{12,... | collective-permute-start | bytes 589832 | tf_op jit(solution)/shard_map/ppermute | solution.py:412
  134.3 8.3 %collective-permute-start.16 = (bf16[192,512]{1,0:T(8,128)(2,1)S(1)}, bf16[192,512]{1,0:T(8,128)(2,1)S(1)}, u32[]{:S(2)}, u32[]{:S(2)}) collective-permute-start(bf16[192,512]{1,0:T(8,128)(2,1)S(1)} %get-tuple-element.46), channel_id=1, source_target_pairs={{0,2},{2,4},{4,6},{6,0},{1,3},{3,5},{5,7},{7,1},{8,10},{10,12},{12... | collective-permute-start | bytes 589832 | tf_op jit(solution)/shard_map/ppermute | solution.py:407
  134.3 8.3 %collective-permute-start.17 = (bf16[192,512]{1,0:T(8,128)(2,1)S(1)}, bf16[192,512]{1,0:T(8,128)(2,1)S(1)}, u32[]{:S(2)}, u32[]{:S(2)}) collective-permute-start(bf16[192,512]{1,0:T(8,128)(2,1)S(1)} %get-tuple-element.47), channel_id=1, source_target_pairs={{0,6},{2,0},{4,2},{6,4},{1,7},{3,1},{5,3},{7,5},{8,14},{10,8},{12,... | collective-permute-start | bytes 589832 | tf_op jit(solution)/shard_map/ppermute | solution.py:408
  137.0 12.7 %collective-permute-start.24 = (bf16[384,256]{1,0:T(8,128)(2,1)S(1)}, bf16[384,256]{1,0:T(8,128)(2,1)S(1)}, u32[]{:S(2)}, u32[]{:S(2)}) collective-permute-start(bf16[384,256]{1,0:T(8,128)(2,1)S(1)} %copy-done.6), channel_id=1, source_target_pairs={{0,1},{1,0},{2,3},{3,2},{4,5},{5,4},{6,7},{7,6},{8,9},{9,8},{10,11... | collective-permute-start | bytes 589832 | tf_op jit(solution)/shard_map/ppermute | solution.py:306
  143.5 10.8 %collective-permute-start.23 = (bf16[384,256]{1,0:T(8,128)(2,1)S(1)}, bf16[384,256]{1,0:T(8,128)(2,1)S(1)}, u32[]{:S(2)}, u32[]{:S(2)}) collective-permute-start(bf16[384,256]{1,0:T(8,128)(2,1)S(1)} %get-tuple-element.63), channel_id=1, source_target_pairs={{0,1},{1,0},{2,3},{3,2},{4,5},{5,4},{6,7},{7,6},{8,9},{9,8},{10,11... | collective-permute-start | bytes 589832 | tf_op jit(solution)/shard_map/ppermute | solution.py:306
  145.3 9.0 %all-to-all-start.2 = ((f32[8,3,128]{2,1,0:T(4,128)}), f32[8,3,128]{2,1,0:T(4,128)S(1)}, u32[]{:S(2)}, u32[]{:S(2)}) async-start(f32[8,3,128]{2,1,0:T(4,128)} %get-tuple-element.66), calls=%async_computation.2 | async-start | bytes 32768 | tf_op jit(solution)/shard_map/all_to_all | solution.py:422
  (20 other events, 186.8 us)
Sparse Core Ops, SparseCore 0:
  9.5 75.3 all-gather.2

commit v3 on v2

--- a/solution.py
+++ b/solution.py
@@ -31,9 +31,23 @@
     return -y * p
 
 
-def pack_kernel(g_ref, u_ref, d_ref, out_ref):
-    for i, ref in enumerate((g_ref, u_ref, d_ref)):
-        out_ref[704 * i : 704 * i + 704, :] = ref[...]
+def pack_kernel(g_ref, u_ref, d_ref, out_ref, buf, sem):
+    spans = [pl.ds(704 * i, 704) for i in range(3)]
+    fetches = [
+        pltpu.make_async_copy(ref, buf.at[span], sem.at[i])
+        for i, (ref, span) in enumerate(zip((g_ref, u_ref, d_ref), spans))
+    ]
+    stores = [
+        pltpu.make_async_copy(buf.at[span], out_ref.at[span], sem.at[3 + i])
+        for i, span in enumerate(spans)
+    ]
+    for cp in fetches:
+        cp.start()
+    for cp, then in zip(fetches, stores):
+        cp.wait()
+        then.start()
+    for cp in stores:
+        cp.wait()
 
 
 def scan_kernel(
@@ -126,8 +140,8 @@
 
 
 def mix_kernel(
-    br_ref, w0, w1, w2, w3, v0, v1, v2, v3, g_ref,
-    norm_ref, keep_ref, send_ref, full, mixed, stream,
+    br_ref, w0, w1, w2, w3, v0, v1, v2, v3, r0, r1, r2, r3,
+    norm_ref, also_ref, keep_ref, send_ref, full, mixed, stream,
 ):
     x = lax.axis_index("x")
     c = lax.axis_index("c")
@@ -137,28 +151,40 @@
     lhs = full[...]
     total = jnp.zeros((rows, 128), F32)
     pieces = []
-    for d, w, v, g in ((0, w0, v0, 0), (3, w1, v1, 4), (1, w2, v2, 8), (2, w3, v3, 12)):
+    for d, w, v, r in ((0, w0, v0, r0), (3, w1, v1, r1), (1, w2, v2, r2), (2, w3, v3, r3)):
         block = lax.rem(x + d, 4)
+        g = r[2 * rows : 2 * rows + 16, :].astype(F32)
         for k, core, ref in ((0, c, w), (1, 1 - c, v)):
             at = pl.ds(pl.multiple_of((2 * block + core) * 256, 256), 256)
-            pieces.append((at, w, k, g))
-            m = jnp.dot(lhs, ref[0:1024, :], preferred_element_type=F32).astype(BF)
+            m = 6 * k
+            pieces.append(
+                (
+                    at,
+                    r,
+                    rows * k,
+                    g[m : m + 1] + g[m + 1 : m + 2] + g[m + 2 : m + 3],
+                    g[m + 3 : m + 4] + g[m + 4 : m + 5] + g[m + 5 : m + 6],
+                )
+            )
+            m = jnp.dot(lhs, ref[...], preferred_element_type=F32).astype(BF)
             mixed[:, at] = m
             mf = m.astype(F32)
             mf = mf * mf
             total = total + mf[:, :128] + mf[:, 128:]
     scale = lax.rsqrt(jnp.sum(total, axis=1, keepdims=True) / 2048.0 + EPS)
     total = jnp.zeros((rows, 128), F32)
-    for at, w, k, g in pieces:
-        r = w[1024 + rows * k : 1024 + rows * k + rows, :].astype(F32)
-        s = (r + mixed[:, at].astype(F32) * scale * g_ref[g + 2 * k : g + 2 * k + 1, :]).astype(BF)
+    for at, res, lo, mg, _ in pieces:
+        r = res[lo : lo + rows, :].astype(F32)
+        s = (r + mixed[:, at].astype(F32) * scale * mg).astype(BF)
         stream[:, at] = s
         sf = s.astype(F32)
         sf = sf * sf
         total = total + sf[:, :128] + sf[:, 128:]
     scale = lax.rsqrt(jnp.sum(total, axis=1, keepdims=True) / 2048.0 + EPS)
-    for at, w, k, g in pieces:
-        norm_ref[:, at] = (stream[:, at].astype(F32) * scale * g_ref[g + 2 * k + 1 : g + 2 * k + 2, :]).astype(BF)
+    for at, _, _, _, pg in pieces:
+        n = (stream[:, at].astype(F32) * scale * pg).astype(BF)
+        norm_ref[:, at] = n
+        also_ref[:, at] = n
     keep_ref[...] = stream[:, pl.ds(pl.multiple_of((2 * x + c) * 256, 256), 256)]
     send_ref[...] = stream[:, pl.ds(pl.multiple_of((2 * x + 1 - c) * 256, 256), 256)]
 
@@ -175,7 +201,7 @@
     return jnp.dot(lhs, part, preferred_element_type=F32).astype(BF)
 
 
-def ffn_kernel(oth_ref, own_ref, w_ref, foth_ref, fown_ref, hoth, hid_ref, dn, gu, sem):
+def ffn_kernel(oth_ref, own_hbm, w_ref, foth_ref, fown_ref, hoth, hid_ref, dn, gu, own_ref, sem):
     cuts = ((0, 128), (128, 384), (384, 704))
     groups = []
     for i, (lo, hi) in enumerate(cuts):
@@ -191,7 +217,8 @@
             ]
         )
     downs = down_copies(w_ref, dn, sem.at[3])
-    for group in groups + [downs]:
+    own_copy = pltpu.make_async_copy(own_hbm, own_ref, sem.at[4])
+    for group in (groups[0], [own_copy], *groups[1:], downs):
         for cp in group:
             cp.start()
     turned = (((1,), (1,)), ((), ()))
@@ -201,6 +228,8 @@
         gate = jnp.concatenate([gu[s, lo:hi, :] for s in range(16)], axis=1)
         up = jnp.concatenate([gu[s, 704 + lo : 704 + hi, :] for s in range(16)], axis=1)
         for src, dst in ((oth_ref, hoth), (own_ref, hid_ref)):
+            if lo == 0 and src is own_ref:
+                own_copy.wait()
             g = lax.dot_general(src[...], gate, turned, preferred_element_type=F32)
             u = lax.dot_general(src[...], up, turned, preferred_element_type=F32)
             dst[:, lo:hi] = (jax.nn.silu(g) * u).astype(BF)
@@ -287,12 +316,12 @@
                 out_ref[pl.ds(pl.multiple_of(core * half + 128 * k, 128), 128), ln] = v.astype(BF)
 
 
-def call(fn, outs, specs, scratch=(), limit=8):
+def call(fn, outs, specs, scratch=(), limit=8, out_spec=VM):
     return pl.pallas_call(
         fn,
         out_shape=tuple(jax.ShapeDtypeStruct(s, d) for s, d in outs),
         in_specs=list(specs),
-        out_specs=tuple(VM for _ in outs),
+        out_specs=tuple(out_spec for _ in outs),
         scratch_shapes=list(scratch),
         compiler_params=pltpu.CompilerParams(vmem_limit_bytes=limit << 20),
     )
@@ -315,20 +344,28 @@
     c = lax.axis_index("c")
 
     (stacked,) = call(
-        pack_kernel, [((2112, 128), BF)], [VM] * 3
+        pack_kernel,
+        [((2112, 128), BF)],
+        [HB] * 3,
+        [pltpu.VMEM((2112, 128), BF), pltpu.SemaphoreType.DMA((6,))],
+        out_spec=HB,
     )(*kept_in_hbm(gate_weight.T, up_weight.T, down_weight))
     (weights,) = kept_in_hbm(lax.all_gather(stacked, SP, axis=0))
 
     res_keep = lax.dynamic_slice_in_dim(residual, c * half, half, 0)
     res_send = lax.dynamic_slice_in_dim(residual, (1 - c) * half, half, 0)
-    ahead = jnp.concatenate([out_weight, res_keep, swapped(res_send)])
-    from_left = lax.ppermute(ahead, "x", cyc(4, 1))
-    from_right = lax.ppermute(ahead, "x", cyc(4, 3))
-    gains = jnp.stack([mix_gain, pre_gain])
-    gains = jnp.concatenate([gains, swapped(gains)])
-    all_gains = [gains]
-    for d in (1, 3, 2):
-        all_gains.append(lax.ppermute(gains, "x", cyc(4, d)))
+    rest = jnp.stack([mix_gain, pre_gain])
+    levels = []
+    for _ in range(3):
+        levels.append(lax.reduce_precision(rest, 8, 7))
+        rest = rest - levels[-1]
+    coded = jnp.stack(levels, axis=1).reshape(6, 256).astype(BF)
+    coded = jnp.concatenate([coded, swapped(coded), jnp.zeros((4, 256), BF)])
+    res = jnp.concatenate([res_keep, swapped(res_send), coded])
+    out_left = lax.ppermute(out_weight, "x", cyc(4, 1))
+    res_right = lax.ppermute(res, "x", cyc(4, 3))
+    res_left = lax.ppermute(res, "x", cyc(4, 1))
+    out_right = lax.ppermute(out_weight, "x", cyc(4, 3))
 
     tail = jnp.pad(recur_input[rows - 3 :].astype(F32), ((5, 0), (0, 0)))
     tail_ids = jnp.pad(
@@ -361,33 +398,37 @@
         states, products, all_ends, *kept_in_hbm(gate_branch)
     )
     branch = lax.all_to_all(branch, TP, 0, 0, tiled=True)
-    cut = from_left.shape[0] // 2
-    far_top = lax.ppermute(from_left[:cut], "x", cyc(4, 1))
-    far_bottom = lax.ppermute(from_right[cut:], "x", cyc(4, 3))
-    far = jnp.concatenate([far_top, far_bottom])
-    blocks = [ahead, from_left, from_right, far]
-    others = [swapped(b) for b in blocks[:3]]
-    others.append(swapped(far))
-    norm_own, skeep, ssend = call(
+    out_far = lax.ppermute(out_left, "x", cyc(4, 1))
+    res_far = lax.ppermute(res_right, "x", cyc(4, 3))
+    outs = [out_weight, out_left, out_right]
+    others = [swapped(b) for b in outs]
+    others.append(swapped(out_far))
+    outs.append(out_far)
+    norm_send, norm_own, skeep, ssend = call(
         mix_kernel,
-        [((half, 2048), BF), ((half, 256), BF), ((half, 256), BF)],
-        [VM] * 10,
+        [((half, 2048), BF)] * 2 + [((half, 256), BF)] * 2,
+        [VM] * 13,
         [
             pltpu.VMEM((half, 1024), BF),
             pltpu.VMEM((half, 2048), BF),
             pltpu.VMEM((half, 2048), BF),
         ],
         limit=12,
-    )(branch, *blocks, *others, jnp.concatenate(all_gains))
-    norm_oth = swapped(norm_own)
+    )(branch, *outs, *others, res, res_left, res_right, res_far)
+    (norm_own,) = kept_in_hbm(norm_own)
+    norm_oth = swapped(norm_send)
     sgot = swapped(ssend)
 
     far_oth, far_own, hid_oth, hid_own, down = call(
         ffn_kernel,
         [((half, 512), BF)] * 2 + [((half, 704), BF)] * 2 + [((16, 704, 128), BF)],
-        [VM, VM, HB],
-        [pltpu.VMEM((16, 1408, 128), BF), pltpu.SemaphoreType.DMA((4,))],
-        limit=15,
+        [VM, HB, HB],
+        [
+            pltpu.VMEM((16, 1408, 128), BF),
+            pltpu.VMEM((half, 2048), BF),
+            pltpu.SemaphoreType.DMA((5,)),
+        ],
+        limit=17,
     )(norm_oth, norm_own, weights)
     far_in = swapped(far_oth)
     rest_oth, rest_own = call(

time: 163 us -> 143 us (0.88)
  waiting for transfers between devices: 52.8 us -> 43.9 us
  starting transfers between devices: 47 us -> 40.3 us
  local copies, waits for them, and re-layouts: 7.81 us -> 4.6 us
    ppermute x7 -> x6, waiting for transfers between devices: 32.9 us -> 25.5 us  [the longest x1 17.2 us: steps(): res_left = lax.ppermute(res, 'x', cyc(4, 1))]
    ppermute x11, starting transfers between devices: 13.1 us -> 8.12 us  [swapped(): return lax.ppermute(block, 'c', cyc(2, 1))]
    ppermute x7 -> x6, starting transfers between devices: 12.1 us -> 9.32 us  [the longest x1 2.72 us: steps(): res_right = lax.ppermute(res, 'x', cyc(4, 3))]
    concatenate x2 -> x1, local copies, waits for them, and re-layouts: 2.23 us -> 0.29 us  [steps(): res = jnp.concatenate([res_keep, swapped(res_send), coded])]
    all_to_all x1, starting transfers between devices: 5.38 us -> 7.16 us  [steps(): branch = lax.all_to_all(branch, TP, 0, 0, tiled=True)]
    unnamed x33 -> x24, local copies, waits for them, and re-layouts: 4.8 us -> 3.57 us
  transfers between devices with their start and end apart: 28 -> 27, of which waited for: 12 -> 7; matrix products, arithmetic and copies ran while one was open for 3% -> 1% of each run, Pallas kernels for 7% -> 8%
where the time goes in v3:
time: 143 us
  waiting for transfers between devices  43.9 us (31%)
  starting transfers between devices  40.3 us (28%)
  Pallas kernels  26.3 us (18%)
  blocking collectives  13.7 us (10%)
  between operations  13.6 us (10%)
  local copies, waits for them, and re-layouts  4.6 us (3%)
    ppermute x1, waiting for transfers between devices, steps(): res_left = lax.ppermute(res, 'x', cyc(4, 1))  17.2 us
    all_to_all x1, blocking collectives, steps(): all_ends = lax.all_to_all(ends, SP, 0, 0, tiled=True)  13.7 us
    pallas_call x1, Pallas kernels, steps(): call(ffn_kernel, [((half, 512), BF)] * 2 + [((half, 704), BF)] * 2 + [((1...  9.21 us
    ppermute x1, waiting for transfers between devices, steps(): out_left = lax.ppermute(out_weight, 'x', cyc(4, 1))  8.26 us
    ppermute x11, starting transfers between devices, swapped(): return lax.ppermute(block, 'c', cyc(2, 1))  8.12 us
    all_to_all x1, starting transfers between devices, steps(): branch = lax.all_to_all(branch, TP, 0, 0, tiled=True)  7.16 us
    ppermute x11, waiting for transfers between devices, swapped(): return lax.ppermute(block, 'c', cyc(2, 1))  5.96 us
    pallas_call x1, Pallas kernels, steps(): call(mix_kernel, [((half, 2048), BF)] * 2 + [((half, 256), BF)] * 2, [VM]...  5.57 us
  transfers between devices with their start and end apart: 27, of which 7 were waited for; matrix products, arithmetic and copies ran while one was open for 1% of the time, Pallas kernels for 8%

profile of v3, /device:TPU:1, one launch (start us, length us, event | category | flops | bytes accessed | tf_op | source)
XLA Modules:
  0.0 142.7 jit_solution(9161328231310894390)
XLA Ops:
  6.6 1.9 %shard_map.157 = bf16[2112,128]{1,0:T(8,128)(2,1)} custom-call(bf16[704,128]{1,0:T(8,128)(2,1)} %bitcast.12, bf16[704,128]{1,0:T(8,128)(2,1)} %bitcast.13, bf16[704,128]{1,0:T(8,128)(2,1)} %d_ref.1), custom_call_target="tpu_custom_call" | custom-call | tf_op jit(solution)/shard_map/pallas_call | solution.py:346
  8.5 2.1 %collective-permute-start.1 = (bf16[1024,256]{1,0:T(8,128)(2,1)S(1)}, bf16[1024,256]{1,0:T(8,128)(2,1)S(1)}, u32[]{:S(2)}, u32[]{:S(2)}) collective-permute-start(bf16[1024,256]{1,0:T(8,128)(2,1)S(1)} %copy-done.1), channel_id=1, source_target_pairs={{0,2},{2,4},{4,6},{6,0},{1,3},{3,5},{5,7},{7,1},{8,10},{10,12},{12... | collective-permute-start | bytes 1572872 | tf_op jit(solution)/shard_map/ppermute | solution.py:365
  14.9 8.3 %collective-permute-done.1.w1 = bf16[1024,256]{1,0:T(8,128)(2,1)S(1)} collective-permute-done((bf16[1024,256]{1,0:T(8,128)(2,1)S(1)}, bf16[1024,256]{1,0:T(8,128)(2,1)S(1)}, u32[]{:S(2)}, u32[]{:S(2)}) %collective-permute-start.1) | collective-permute-done | bytes 524320 | tf_op jit(solution)/shard_map/ppermute | solution.py:365
  23.4 3.2 %collective-permute-start = (f32[16,128]{1,0:T(8,128)S(1)}, f32[16,128]{1,0:T(8,128)S(1)}, u32[]{:S(2)}, u32[]{:S(2)}) collective-permute-start(f32[16,128]{1,0:T(8,128)S(1)} %pad_maximum_fusion), channel_id=1, source_target_pairs={{0,8},{8,16},{16,24},{24,32},{32,40},{40,48},{48,56},{56,64},{64,7... | collective-permute-start | bytes 24584 | tf_op jit(solution)/shard_map/ppermute | solution.py:374
  27.0 2.7 %collective-permute-start.11 = (bf16[784,256]{1,0:T(8,128)(2,1)S(1)}, bf16[784,256]{1,0:T(8,128)(2,1)}, u32[]{:S(2)}, u32[]{:S(2)}) collective-permute-start(bf16[784,256]{1,0:T(8,128)(2,1)S(1)} %concatenate.31.r0), channel_id=1, source_target_pairs={{0,6},{2,0},{4,2},{6,4},{1,7},{3,1},{5,3},{7,5},{8,14},{10,8},{12,... | collective-permute-start | bytes 1204232 | tf_op jit(solution)/shard_map/ppermute | solution.py:366
  29.7 3.2 %shard_map.154 = (f32[768,128]{1,0:T(8,128)S(1)}, f32[768,128]{1,0:T(8,128)S(1)}, f32[16,2,128]{2,1,0:T(2,128)S(1)}) custom-call(bf16[768,128]{1,0:T(8,128)(2,1)} %x_ref.1, f32[16,128]{1,0:T(8,128)S(1)} %collective-permute-done.rim_ref, f32[6,128]{1,0:T(8,128)S(1)} %convert_bitcast_fusion.ids_ref, bf16[4,128]{1,0:T(4,128)(2,1)} %taps_ref.1, ...), custom_call_target="tpu_custom_call" | custom-call | tf_op jit(solution)/shard_map/pallas_call | solution.py:378
  32.9 13.7 %all_to_all.15.e_ref = f32[16,2,128]{2,1,0:T(2,128)S(1)} all-to-all(f32[16,2,128]{2,1,0:T(2,128)S(1)} %get-tuple-element.39), channel_id=1, replica_groups=mesh['z'=4,'y'=4,'x'=4,'c'=2] {'z','y'}, dimensions={0} | all-to-all | bytes 32768 | tf_op jit(solution)/shard_map/all_to_all | solution.py:396
  46.6 2.2 %shard_map.155 = bf16[8,384,128]{2,1,0:T(8,128)(2,1)} custom-call(f32[768,128]{1,0:T(8,128)S(1)} %get-tuple-element.37.s_ref, f32[768,128]{1,0:T(8,128)S(1)} %get-tuple-element.38.p_ref, f32[16,2,128]{2,1,0:T(2,128)S(1)} %all_to_all.15.e_ref, bf16[768,128]{1,0:T(8,128)(2,1)} %g_ref.1), custom_call_target="tpu_custom_call" | custom-call | tf_op jit(solution)/shard_map/pallas_call | solution.py:397
  48.8 7.2 %all-to-all-start.1 = ((bf16[8,384,128]{2,1,0:T(8,128)(2,1)}), bf16[8,384,128]{2,1,0:T(8,128)(2,1)S(1)}, u32[]{:S(2)}, u32[]{:S(2)}) async-start(bf16[8,384,128]{2,1,0:T(8,128)(2,1)} %shard_map.155), calls=%async_computation.1 | async-start | bytes 1572864 | tf_op jit(solution)/shard_map/all_to_all | solution.py:400
  59.5 17.2 %collective-permute-done.10.r1 = bf16[784,256]{1,0:T(8,128)(2,1)S(1)} collective-permute-done((bf16[784,256]{1,0:T(8,128)(2,1)S(1)}, bf16[784,256]{1,0:T(8,128)(2,1)S(1)}, u32[]{:S(2)}, u32[]{:S(2)}) %collective-permute-start.10) | collective-permute-done | bytes 401440 | tf_op jit(solution)/shard_map/ppermute | solution.py:367
  78.5 5.6 %shard_map.156 = (bf16[384,2048]{1,0:T(8,128)(2,1)S(1)}, bf16[384,2048]{1,0:T(8,128)(2,1)S(1)}, bf16[384,256]{1,0:T(8,128)(2,1)S(1)}, bf16[384,256]{1,0:T(8,128)(2,1)S(1)}) custom-call(bf16[8,384,128]{2,1,0:T(8,128)(2,1)S(1)} %all-to-all-done.1.br_ref, bf16[1024,256]{1,0:T(8,128)(2,1)S(1)} %copy-done.1, bf16[1024,256]{1,0:T(8,128)(2,1)S(1)} %collective-permute-done.1.w1, ...), custom_call_target="tpu_custom_call" | custom-call | tf_op jit(solution)/shard_map/pallas_call | solution.py:407
  86.6 3.0 %collective-permute-done.13.oth_ref = bf16[384,2048]{1,0:T(8,128)(2,1)S(1)} collective-permute-done((bf16[384,2048]{1,0:T(8,128)(2,1)S(1)}, bf16[384,2048]{1,0:T(8,128)(2,1)S(1)}, u32[]{:S(2)}, u32[]{:S(2)}) %collective-permute-start.13) | collective-permute-done | bytes 1572896 | tf_op jit(solution)/shard_map/ppermute | solution.py:335
  89.6 9.2 %shard_map.158 = (bf16[384,512]{1,0:T(8,128)(2,1)S(1)}, bf16[384,512]{1,0:T(8,128)(2,1)S(1)}, bf16[384,704]{1,0:T(8,128)(2,1)S(1)}, bf16[384,704]{1,0:T(8,128)(2,1)S(1)}, bf16[16,704,128]{2,1,0:T(8,128)(2,1)S(1)}) custom-call(bf16[384,2048]{1,0:T(8,128)(2,1)S(1)} %collective-permute-done.13.oth_ref, bf16[384,2048]{1,0:T(8,128)(2,1)} %copy-done, ...), custom_call_target="tpu_custom_call" | custom-call | tf_op jit(solution)/shard_map/pallas_call | solution.py:422
  98.8 2.0 %shard_map.159 = (bf16[3,384,512]{2,1,0:T(8,128)(2,1)S(1)}, bf16[3,384,512]{2,1,0:T(8,128)(2,1)S(1)}) custom-call(bf16[384,704]{1,0:T(8,128)(2,1)S(1)} %get-tuple-element.42.hoth_ref, bf16[384,704]{1,0:T(8,128)(2,1)S(1)} %get-tuple-element.43.hid_ref, bf16[16,704,128]{2,1,0:T(8,128)(2,1)S(1)} %get-tuple-element.44.dn), custom_call_target="tpu_custom_call" | custom-call | tf_op jit(solution)/shard_map/pallas_call | solution.py:434
  101.4 2.9 %collective-permute-done.17.b_ref = bf16[384,512]{1,0:T(8,128)(2,1)S(1)} collective-permute-done((bf16[384,512]{1,0:T(8,128)(2,1)S(1)}, bf16[384,512]{1,0:T(8,128)(2,1)S(1)}, u32[]{:S(2)}, u32[]{:S(2)}) %collective-permute-start.17) | collective-permute-done | bytes 393248 | tf_op jit(solution)/shard_map/ppermute | solution.py:335
  104.5 2.7 %collective-permute-start.19 = (bf16[192,512]{1,0:T(8,128)(2,1)S(1)}, bf16[192,512]{1,0:T(8,128)(2,1)S(1)}, u32[]{:S(2)}, u32[]{:S(2)}) collective-permute-start(bf16[192,512]{1,0:T(8,128)(2,1)S(1)} %get-tuple-element.53), channel_id=1, source_target_pairs={{0,6},{2,0},{4,2},{6,4},{1,7},{3,1},{5,3},{7,5},{8,14},{10,8},{12,... | collective-permute-start | bytes 589832 | tf_op jit(solution)/shard_map/ppermute | solution.py:441
  107.2 4.6 %collective-permute-done.18.r_ref = bf16[192,512]{1,0:T(8,128)(2,1)S(1)} collective-permute-done((bf16[192,512]{1,0:T(8,128)(2,1)S(1)}, bf16[192,512]{1,0:T(8,128)(2,1)S(1)}, u32[]{:S(2)}, u32[]{:S(2)}) %collective-permute-start.18) | collective-permute-done | bytes 196640 | tf_op jit(solution)/shard_map/ppermute | solution.py:440
  112.2 2.7 %collective-permute-start.21 = (bf16[192,512]{1,0:T(8,128)(2,1)S(1)}, bf16[192,512]{1,0:T(8,128)(2,1)S(1)}, u32[]{:S(2)}, u32[]{:S(2)}) collective-permute-start(bf16[192,512]{1,0:T(8,128)(2,1)S(1)} %get-tuple-element.59), channel_id=1, source_target_pairs={{0,6},{2,0},{4,2},{6,4},{1,7},{3,1},{5,3},{7,5},{8,14},{10,8},{12,... | collective-permute-start | bytes 589832 | tf_op jit(solution)/shard_map/ppermute | solution.py:453
  114.9 2.7 %collective-permute-start.16 = (bf16[192,512]{1,0:T(8,128)(2,1)S(1)}, bf16[192,512]{1,0:T(8,128)(2,1)S(1)}, u32[]{:S(2)}, u32[]{:S(2)}) collective-permute-start(bf16[192,512]{1,0:T(8,128)(2,1)S(1)} %get-tuple-element.49), channel_id=1, source_target_pairs={{0,6},{2,0},{4,2},{6,4},{1,7},{3,1},{5,3},{7,5},{8,14},{10,8},{12,... | collective-permute-start | bytes 589832 | tf_op jit(solution)/shard_map/ppermute | solution.py:449
  117.6 2.3 %collective-permute-start.23 = (bf16[384,256]{1,0:T(8,128)(2,1)S(1)}, bf16[384,256]{1,0:T(8,128)(2,1)S(1)}, u32[]{:S(2)}, u32[]{:S(2)}) collective-permute-start(bf16[384,256]{1,0:T(8,128)(2,1)S(1)} %copy-done.6), channel_id=1, source_target_pairs={{0,1},{1,0},{2,3},{3,2},{4,5},{5,4},{6,7},{7,6},{8,9},{9,8},{10,11... | collective-permute-start | bytes 589832 | tf_op jit(solution)/shard_map/ppermute | solution.py:335
  119.9 3.1 %collective-permute-done.15.fl_ref = bf16[192,512]{1,0:T(8,128)(2,1)S(1)} collective-permute-done((bf16[192,512]{1,0:T(8,128)(2,1)S(1)}, bf16[192,512]{1,0:T(8,128)(2,1)S(1)}, u32[]{:S(2)}, u32[]{:S(2)}) %collective-permute-start.15) | collective-permute-done | bytes 196640 | tf_op jit(solution)/shard_map/ppermute | solution.py:448
  124.0 1.9 %collective-permute-start.22 = (bf16[384,256]{1,0:T(8,128)(2,1)S(1)}, bf16[384,256]{1,0:T(8,128)(2,1)S(1)}, u32[]{:S(2)}, u32[]{:S(2)}) collective-permute-start(bf16[384,256]{1,0:T(8,128)(2,1)S(1)} %get-tuple-element.65), channel_id=1, source_target_pairs={{0,1},{1,0},{2,3},{3,2},{4,5},{5,4},{6,7},{7,6},{8,9},{9,8},{10,11... | collective-permute-start | bytes 589832 | tf_op jit(solution)/shard_map/ppermute | solution.py:335
  125.9 4.3 %all-to-all-start.2 = ((f32[8,3,128]{2,1,0:T(4,128)}), f32[8,3,128]{2,1,0:T(4,128)S(1)}, u32[]{:S(2)}, u32[]{:S(2)}) async-start(f32[8,3,128]{2,1,0:T(4,128)} %get-tuple-element.68), calls=%async_computation.2 | async-start | bytes 32768 | tf_op jit(solution)/shard_map/all_to_all | solution.py:463
  130.2 4.7 %all-to-all-done.2.sq_ref = f32[8,3,128]{2,1,0:T(4,128)S(1)} async-done(((f32[8,3,128]{2,1,0:T(4,128)}), f32[8,3,128]{2,1,0:T(4,128)S(1)}, u32[]{:S(2)}, u32[]{:S(2)}) %all-to-all-start.2) | async-done | bytes 12320 | tf_op jit(solution)/shard_map/all_to_all | solution.py:463
  (81 shorter events, 15.8 us)
Async XLA Ops:
  6.5 83.0 %all-gather.3.cloned.1.call-start = ((), (), s32[]{:S(2)}) async-start(), calls=%async_computation.3 | async-start | bytes 9191424 | tf_op jit(solution)/shard_map/all_gather | solution.py:353
  8.5 14.6 %collective-permute-start.1 = (bf16[1024,256]{1,0:T(8,128)(2,1)S(1)}, bf16[1024,256]{1,0:T(8,128)(2,1)S(1)}, u32[]{:S(2)}, u32[]{:S(2)}) collective-permute-start(bf16[1024,256]{1,0:T(8,128)(2,1)S(1)} %copy-done.1), channel_id=1, source_target_pairs={{0,2},{2,4},{4,6},{6,0},{1,3},{3,5},{5,7},{7,1},{8,10},{10,12},{12... | collective-permute-start | bytes 1572872 | tf_op jit(solution)/shard_map/ppermute | solution.py:365
  10.6 45.5 %collective-permute-start.2 = (bf16[1024,256]{1,0:T(8,128)(2,1)S(1)}, bf16[1024,256]{1,0:T(8,128)(2,1)S(1)}, u32[]{:S(2)}, u32[]{:S(2)}) collective-permute-start(bf16[1024,256]{1,0:T(8,128)(2,1)S(1)} %copy-done.1), channel_id=1, source_target_pairs={{0,6},{2,0},{4,2},{6,4},{1,7},{3,1},{5,3},{7,5},{8,14},{10,8},{12,... | collective-permute-start | bytes 1572872 | tf_op jit(solution)/shard_map/ppermute | solution.py:368
  12.0 44.6 %collective-permute-start.4 = (bf16[1024,256]{1,0:T(8,128)(2,1)S(1)}, bf16[1024,256]{1,0:T(8,128)(2,1)S(1)}, u32[]{:S(2)}, u32[]{:S(2)}) collective-permute-start(bf16[1024,256]{1,0:T(8,128)(2,1)S(1)} %copy-done.1), channel_id=1, source_target_pairs={{0,1},{1,0},{2,3},{3,2},{4,5},{5,4},{6,7},{7,6},{8,9},{9,8},{10,11... | collective-permute-start | bytes 1572872 | tf_op jit(solution)/shard_map/ppermute | solution.py:335
  13.3 13.4 %collective-permute-start.8 = (bf16[384,256]{1,0:T(8,128)(2,1)S(1)}, bf16[384,256]{1,0:T(8,128)(2,1)S(1)}, u32[]{:S(2)}, u32[]{:S(2)}) collective-permute-start(bf16[384,256]{1,0:T(8,128)(2,1)S(1)} %get-tuple-element.69), channel_id=1, source_target_pairs={{0,1},{1,0},{2,3},{3,2},{4,5},{5,4},{6,7},{7,6},{8,9},{9,8},{10,11... | collective-permute-start | bytes 589832 | tf_op jit(solution)/shard_map/ppermute | solution.py:335
  13.4 10.0 %collective-permute-start.9 = (bf16[6,256]{1,0:T(8,128)(2,1)S(1)}, bf16[6,256]{1,0:T(8,128)(2,1)S(1)}, u32[]{:S(2)}, u32[]{:S(2)}) collective-permute-start(bf16[6,256]{1,0:T(8,128)(2,1)S(1)} %convert_element_type.16), channel_id=1, source_target_pairs={{0,1},{1,0},{2,3},{3,2},{4,5},{5,4},{6,7},{7,6},{8,9},{9,8},{10,11... | collective-permute-start | bytes 9224 | tf_op jit(solution)/shard_map/ppermute | solution.py:335
  23.2 33.3 %collective-permute-start.3 = (bf16[1024,256]{1,0:T(8,128)(2,1)S(1)}, bf16[1024,256]{1,0:T(8,128)(2,1)}, u32[]{:S(2)}, u32[]{:S(2)}) collective-permute-start(bf16[1024,256]{1,0:T(8,128)(2,1)S(1)} %collective-permute-done.1.w1), channel_id=1, source_target_pairs={{0,2},{2,4},{4,6},{6,0},{1,3},{3,5},{5,7},{7,1},{8,10},{10,12},{12... | collective-permute-start | bytes 1572872 | tf_op jit(solution)/shard_map/ppermute | solution.py:401
  27.0 31.2 %collective-permute-start.11 = (bf16[784,256]{1,0:T(8,128)(2,1)S(1)}, bf16[784,256]{1,0:T(8,128)(2,1)}, u32[]{:S(2)}, u32[]{:S(2)}) collective-permute-start(bf16[784,256]{1,0:T(8,128)(2,1)S(1)} %concatenate.31.r0), channel_id=1, source_target_pairs={{0,6},{2,0},{4,2},{6,4},{1,7},{3,1},{5,3},{7,5},{8,14},{10,8},{12,... | collective-permute-start | bytes 1204232 | tf_op jit(solution)/shard_map/ppermute | solution.py:366
  48.8 28.7 %all-to-all-start.1 = ((bf16[8,384,128]{2,1,0:T(8,128)(2,1)}), bf16[8,384,128]{2,1,0:T(8,128)(2,1)S(1)}, u32[]{:S(2)}, u32[]{:S(2)}) async-start(bf16[8,384,128]{2,1,0:T(8,128)(2,1)} %shard_map.155), calls=%async_computation.1 | async-start | bytes 1572864 | tf_op jit(solution)/shard_map/all_to_all | solution.py:400
  55.9 21.6 %collective-permute-start.5 = (bf16[1024,256]{1,0:T(8,128)(2,1)S(1)}, bf16[1024,256]{1,0:T(8,128)(2,1)}, u32[]{:S(2)}, u32[]{:S(2)}) collective-permute-start(bf16[1024,256]{1,0:T(8,128)(2,1)S(1)} %collective-permute-done.1.w1), channel_id=1, source_target_pairs={{0,1},{1,0},{2,3},{3,2},{4,5},{5,4},{6,7},{7,6},{8,9},{9,8},{10,11... | collective-permute-start | bytes 1572872 | tf_op jit(solution)/shard_map/ppermute | solution.py:335
  56.1 21.4 %collective-permute-start.6 = (bf16[1024,256]{1,0:T(8,128)(2,1)S(1)}, bf16[1024,256]{1,0:T(8,128)(2,1)}, u32[]{:S(2)}, u32[]{:S(2)}) collective-permute-start(bf16[1024,256]{1,0:T(8,128)(2,1)S(1)} %collective-permute-done.2.w2), channel_id=1, source_target_pairs={{0,1},{1,0},{2,3},{3,2},{4,5},{5,4},{6,7},{7,6},{8,9},{9,8},{10,11... | collective-permute-start | bytes 1572872 | tf_op jit(solution)/shard_map/ppermute | solution.py:335
  56.4 21.1 %collective-permute-start.7 = (bf16[1024,256]{1,0:T(8,128)(2,1)}, bf16[1024,256]{1,0:T(8,128)(2,1)}, u32[]{:S(2)}, u32[]{:S(2)}) collective-permute-start(bf16[1024,256]{1,0:T(8,128)(2,1)} %collective-permute-done.3.w3), channel_id=1, source_target_pairs={{0,1},{1,0},{2,3},{3,2},{4,5},{5,4},{6,7},{7,6},{8,9},{9,8},{10,11... | collective-permute-start | bytes 1572872 | tf_op jit(solution)/shard_map/ppermute | solution.py:335
  56.6 20.1 %collective-permute-start.10 = (bf16[784,256]{1,0:T(8,128)(2,1)S(1)}, bf16[784,256]{1,0:T(8,128)(2,1)S(1)}, u32[]{:S(2)}, u32[]{:S(2)}) collective-permute-start(bf16[784,256]{1,0:T(8,128)(2,1)S(1)} %concatenate.31.r0), channel_id=1, source_target_pairs={{0,2},{2,4},{4,6},{6,0},{1,3},{3,5},{5,7},{7,1},{8,10},{10,12},{12... | collective-permute-start | bytes 1204232 | tf_op jit(solution)/shard_map/ppermute | solution.py:367
  58.2 19.3 %collective-permute-start.12 = (bf16[784,256]{1,0:T(8,128)(2,1)}, bf16[784,256]{1,0:T(8,128)(2,1)}, u32[]{:S(2)}, u32[]{:S(2)}) collective-permute-start(bf16[784,256]{1,0:T(8,128)(2,1)} %collective-permute-done.11.r2), channel_id=1, source_target_pairs={{0,6},{2,0},{4,2},{6,4},{1,7},{3,1},{5,3},{7,5},{8,14},{10,8},{12,... | collective-permute-start | bytes 1204232 | tf_op jit(solution)/shard_map/ppermute | solution.py:402
  100.8 11.0 %collective-permute-start.14 = (bf16[3,384,512]{2,1,0:T(8,128)(2,1)S(1)}, bf16[3,384,512]{2,1,0:T(8,128)(2,1)S(1)}, u32[]{:S(2)}, u32[]{:S(2)}) collective-permute-start(bf16[3,384,512]{2,1,0:T(8,128)(2,1)S(1)} %get-tuple-element.46), channel_id=1, source_target_pairs={{0,1},{1,0},{2,3},{3,2},{4,5},{5,4},{6,7},{7,6},{8,9},{9,8},{10,11... | collective-permute-start | bytes 3538952 | tf_op jit(solution)/shard_map/ppermute | solution.py:335
  104.4 7.4 %collective-permute-start.18 = (bf16[192,512]{1,0:T(8,128)(2,1)S(1)}, bf16[192,512]{1,0:T(8,128)(2,1)S(1)}, u32[]{:S(2)}, u32[]{:S(2)}) collective-permute-start(bf16[192,512]{1,0:T(8,128)(2,1)S(1)} %get-tuple-element.52), channel_id=1, source_target_pairs={{0,2},{2,4},{4,6},{6,0},{1,3},{3,5},{5,7},{7,1},{8,10},{10,12},{12... | collective-permute-start | bytes 589832 | tf_op jit(solution)/shard_map/ppermute | solution.py:440
  104.5 7.3 %collective-permute-start.19 = (bf16[192,512]{1,0:T(8,128)(2,1)S(1)}, bf16[192,512]{1,0:T(8,128)(2,1)S(1)}, u32[]{:S(2)}, u32[]{:S(2)}) collective-permute-start(bf16[192,512]{1,0:T(8,128)(2,1)S(1)} %get-tuple-element.53), channel_id=1, source_target_pairs={{0,6},{2,0},{4,2},{6,4},{1,7},{3,1},{5,3},{7,5},{8,14},{10,8},{12,... | collective-permute-start | bytes 589832 | tf_op jit(solution)/shard_map/ppermute | solution.py:441
  112.1 7.8 %collective-permute-start.20 = (bf16[192,512]{1,0:T(8,128)(2,1)S(1)}, bf16[192,512]{1,0:T(8,128)(2,1)S(1)}, u32[]{:S(2)}, u32[]{:S(2)}) collective-permute-start(bf16[192,512]{1,0:T(8,128)(2,1)S(1)} %get-tuple-element.58), channel_id=1, source_target_pairs={{0,2},{2,4},{4,6},{6,0},{1,3},{3,5},{5,7},{7,1},{8,10},{10,12},{12... | collective-permute-start | bytes 589832 | tf_op jit(solution)/shard_map/ppermute | solution.py:452
  112.2 7.7 %collective-permute-start.21 = (bf16[192,512]{1,0:T(8,128)(2,1)S(1)}, bf16[192,512]{1,0:T(8,128)(2,1)S(1)}, u32[]{:S(2)}, u32[]{:S(2)}) collective-permute-start(bf16[192,512]{1,0:T(8,128)(2,1)S(1)} %get-tuple-element.59), channel_id=1, source_target_pairs={{0,6},{2,0},{4,2},{6,4},{1,7},{3,1},{5,3},{7,5},{8,14},{10,8},{12,... | collective-permute-start | bytes 589832 | tf_op jit(solution)/shard_map/ppermute | solution.py:453
  114.9 8.1 %collective-permute-start.15 = (bf16[192,512]{1,0:T(8,128)(2,1)S(1)}, bf16[192,512]{1,0:T(8,128)(2,1)S(1)}, u32[]{:S(2)}, u32[]{:S(2)}) collective-permute-start(bf16[192,512]{1,0:T(8,128)(2,1)S(1)} %get-tuple-element.48), channel_id=1, source_target_pairs={{0,2},{2,4},{4,6},{6,0},{1,3},{3,5},{5,7},{7,1},{8,10},{10,12},{12... | collective-permute-start | bytes 589832 | tf_op jit(solution)/shard_map/ppermute | solution.py:448
  114.9 8.1 %collective-permute-start.16 = (bf16[192,512]{1,0:T(8,128)(2,1)S(1)}, bf16[192,512]{1,0:T(8,128)(2,1)S(1)}, u32[]{:S(2)}, u32[]{:S(2)}) collective-permute-start(bf16[192,512]{1,0:T(8,128)(2,1)S(1)} %get-tuple-element.49), channel_id=1, source_target_pairs={{0,6},{2,0},{4,2},{6,4},{1,7},{3,1},{5,3},{7,5},{8,14},{10,8},{12,... | collective-permute-start | bytes 589832 | tf_op jit(solution)/shard_map/ppermute | solution.py:449
  117.6 12.7 %collective-permute-start.23 = (bf16[384,256]{1,0:T(8,128)(2,1)S(1)}, bf16[384,256]{1,0:T(8,128)(2,1)S(1)}, u32[]{:S(2)}, u32[]{:S(2)}) collective-permute-start(bf16[384,256]{1,0:T(8,128)(2,1)S(1)} %copy-done.6), channel_id=1, source_target_pairs={{0,1},{1,0},{2,3},{3,2},{4,5},{5,4},{6,7},{7,6},{8,9},{9,8},{10,11... | collective-permute-start | bytes 589832 | tf_op jit(solution)/shard_map/ppermute | solution.py:335
  124.0 10.9 %collective-permute-start.22 = (bf16[384,256]{1,0:T(8,128)(2,1)S(1)}, bf16[384,256]{1,0:T(8,128)(2,1)S(1)}, u32[]{:S(2)}, u32[]{:S(2)}) collective-permute-start(bf16[384,256]{1,0:T(8,128)(2,1)S(1)} %get-tuple-element.65), channel_id=1, source_target_pairs={{0,1},{1,0},{2,3},{3,2},{4,5},{5,4},{6,7},{7,6},{8,9},{9,8},{10,11... | collective-permute-start | bytes 589832 | tf_op jit(solution)/shard_map/ppermute | solution.py:335
  125.9 9.0 %all-to-all-start.2 = ((f32[8,3,128]{2,1,0:T(4,128)}), f32[8,3,128]{2,1,0:T(4,128)S(1)}, u32[]{:S(2)}, u32[]{:S(2)}) async-start(f32[8,3,128]{2,1,0:T(4,128)} %get-tuple-element.68), calls=%async_computation.2 | async-start | bytes 32768 | tf_op jit(solution)/shard_map/all_to_all | solution.py:463
  (15 other events, 98.0 us)
Sparse Core Ops, SparseCore 0:
  9.5 75.2 all-gather.2

commit v4 on v3

--- a/solution.py
+++ b/solution.py
@@ -189,22 +189,27 @@
     send_ref[...] = stream[:, pl.ds(pl.multiple_of((2 * x + 1 - c) * 256, 256), 256)]
 
 
-def down_copies(w_ref, dn, sem):
-    return [
-        pltpu.make_async_copy(w_ref.at[s, pl.ds(1408, 704)], dn.at[s], sem) for s in range(16)
-    ]
-
-
 def down_dot(lhs, dn, d):
     first = 4 * lax.rem(lax.axis_index("x") + d, 4)
     part = jnp.concatenate([dn[first + i] for i in range(4)], axis=1)
     return jnp.dot(lhs, part, preferred_element_type=F32).astype(BF)
 
 
-def ffn_kernel(oth_ref, own_hbm, w_ref, foth_ref, fown_ref, hoth, hid_ref, dn, gu, own_ref, sem):
-    cuts = ((0, 128), (128, 384), (384, 704))
+CUTS = ((0, 128), (128, 384), (384, 704))
+
+
+def hidden_part(src, gu, lo, hi):
+    turned = (((1,), (1,)), ((), ()))
+    gate = jnp.concatenate([gu[s, lo:hi, :] for s in range(16)], axis=1)
+    up = jnp.concatenate([gu[s, 704 + lo : 704 + hi, :] for s in range(16)], axis=1)
+    g = lax.dot_general(src, gate, turned, preferred_element_type=F32)
+    u = lax.dot_general(src, up, turned, preferred_element_type=F32)
+    return (jax.nn.silu(g) * u).astype(BF)
+
+
+def first_kernel(n_ref, own_hbm, w_ref, far_ref, rest_ref, gu, dn, own_ref, hid, sem):
     groups = []
-    for i, (lo, hi) in enumerate(cuts):
+    for i, (lo, hi) in enumerate(CUTS):
         groups.append(
             [
                 pltpu.make_async_copy(
@@ -216,34 +221,36 @@
                 for base in (0, 704)
             ]
         )
-    downs = down_copies(w_ref, dn, sem.at[3])
+    downs = [
+        pltpu.make_async_copy(w_ref.at[s, pl.ds(1408, 704)], dn.at[s], sem.at[3]) for s in range(16)
+    ]
     own_copy = pltpu.make_async_copy(own_hbm, own_ref, sem.at[4])
-    for group in (groups[0], [own_copy], *groups[1:], downs):
+    for group in groups + [downs, [own_copy]]:
         for cp in group:
             cp.start()
-    turned = (((1,), (1,)), ((), ()))
-    for (lo, hi), group in zip(cuts, groups):
+    for (lo, hi), group in zip(CUTS, groups):
         for cp in group:
             cp.wait()
-        gate = jnp.concatenate([gu[s, lo:hi, :] for s in range(16)], axis=1)
-        up = jnp.concatenate([gu[s, 704 + lo : 704 + hi, :] for s in range(16)], axis=1)
-        for src, dst in ((oth_ref, hoth), (own_ref, hid_ref)):
-            if lo == 0 and src is own_ref:
-                own_copy.wait()
-            g = lax.dot_general(src[...], gate, turned, preferred_element_type=F32)
-            u = lax.dot_general(src[...], up, turned, preferred_element_type=F32)
-            dst[:, lo:hi] = (jax.nn.silu(g) * u).astype(BF)
+        hid[:, lo:hi] = hidden_part(n_ref[...], gu, lo, hi)
     for cp in downs:
         cp.wait()
-    foth_ref[...] = down_dot(hoth[...], dn, 2)
-    fown_ref[...] = down_dot(hid_ref[...], dn, 2)
-
-
-def down_kernel(hoth_ref, hid_ref, dn, oth_ref, own_ref):
-    for src, dst in ((hoth_ref, oth_ref), (hid_ref, own_ref)):
-        lhs = src[...]
-        for i, d in enumerate((1, 3, 0)):
-            dst[i] = down_dot(lhs, dn, d)
+    lhs = hid[...]
+    far_ref[...] = down_dot(lhs, dn, 2)
+    for i, d in enumerate((1, 3, 0)):
+        rest_ref[i] = down_dot(lhs, dn, d)
+    own_copy.wait()
+
+
+def second_kernel(n_ref, gu, dn, far_ref, hid_ref):
+    for lo, hi in CUTS:
+        hid_ref[:, lo:hi] = hidden_part(n_ref[...], gu, lo, hi)
+    far_ref[...] = down_dot(hid_ref[...], dn, 2)
+
+
+def third_kernel(hid_ref, dn, rest_ref):
+    lhs = hid_ref[...]
+    for i, d in enumerate((1, 3, 0)):
+        rest_ref[i] = down_dot(lhs, dn, d)
 
 
 def far_kernel(a_ref, b_ref, right_ref, left_ref):
@@ -419,22 +426,25 @@
     norm_oth = swapped(norm_send)
     sgot = swapped(ssend)
 
-    far_oth, far_own, hid_oth, hid_own, down = call(
-        ffn_kernel,
-        [((half, 512), BF)] * 2 + [((half, 704), BF)] * 2 + [((16, 704, 128), BF)],
+    far_oth, rest_oth, gate_up, down, norm_own = call(
+        first_kernel,
+        [
+            ((half, 512), BF),
+            ((3, half, 512), BF),
+            ((16, 1408, 128), BF),
+            ((16, 704, 128), BF),
+            ((half, 2048), BF),
+        ],
         [VM, HB, HB],
-        [
-            pltpu.VMEM((16, 1408, 128), BF),
-            pltpu.VMEM((half, 2048), BF),
-            pltpu.SemaphoreType.DMA((5,)),
-        ],
-        limit=17,
+        [pltpu.VMEM((half, 704), BF), pltpu.SemaphoreType.DMA((5,))],
+        limit=18,
     )(norm_oth, norm_own, weights)
     far_in = swapped(far_oth)
-    rest_oth, rest_own = call(
-        down_kernel, [((3, half, 512), BF)] * 2, [VM] * 3, limit=14
-    )(hid_oth, hid_own, down)
     rest_in = swapped(rest_oth)
+    far_own, hid_own = call(
+        second_kernel, [((half, 512), BF), ((half, 704), BF)], [VM] * 3, limit=18
+    )(norm_own, gate_up, down)
+    (rest_own,) = call(third_kernel, [((3, half, 512), BF)], [VM] * 2, limit=14)(hid_own, down)
     q = half // 2
     far_r, far_l = call(far_kernel, [((q, 512), BF)] * 2, [VM] * 2)(far_own, far_in)
     pass_r = lax.ppermute(far_r, "x", cyc(4, 1))

time: 143 us -> 142 us (level)
    ppermute x11, waiting for transfers between devices: 5.96 us -> 3.06 us  [swapped(): return lax.ppermute(block, 'c', cyc(2, 1))]
    ppermute x1, waiting for transfers between devices: 8.26 us -> 11.1 us  [steps(): out_left = lax.ppermute(out_weight, 'x', cyc(4, 1))]
    ppermute x1, starting transfers between devices: 2.1 us -> 0.01 us  [steps(): out_left = lax.ppermute(out_weight, 'x', cyc(4, 1))]
    ppermute x1, starting transfers between devices: 1.35 us -> 3.37 us  [steps(): out_right = lax.ppermute(out_weight, 'x', cyc(4, 3))]
    pallas_call x2 -> x3, Pallas kernels: 11.2 us -> 11.2 us  [the longest x1 6.4 us: steps(): call(first_kernel, [((half, 512), BF), ((3, half, 512), BF), ((16, 1408,...]
  transfers between devices with their start and end apart: 27 -> 27, of which waited for: 7 -> 6; matrix products, arithmetic and copies ran while one was open for 1% -> 1% of each run, Pallas kernels for 8% -> 12%
where the time goes in v4:
time: 142 us; the launch traced here: 141 us
  waiting for transfers between devices  42.7 us (30%)
  starting transfers between devices  40 us (28%)
  Pallas kernels  26.2 us (18%)
  blocking collectives  13.8 us (10%)
  between operations  13.7 us (10%)
  local copies, waits for them, and re-layouts  4.61 us (3%)
    ppermute x1, waiting for transfers between devices, steps(): res_left = lax.ppermute(res, 'x', cyc(4, 1))  17.2 us
    all_to_all x1, blocking collectives, steps(): all_ends = lax.all_to_all(ends, SP, 0, 0, tiled=True)  13.8 us
    ppermute x1, waiting for transfers between devices, steps(): out_left = lax.ppermute(out_weight, 'x', cyc(4, 1))  11.1 us
    ppermute x11, starting transfers between devices, swapped(): return lax.ppermute(block, 'c', cyc(2, 1))  7.85 us
    all_to_all x1, starting transfers between devices, steps(): branch = lax.all_to_all(branch, TP, 0, 0, tiled=True)  7.43 us
    pallas_call x1, Pallas kernels, steps(): call(first_kernel, [((half, 512), BF), ((3, half, 512), BF), ((16, 1408,...  6.4 us
    pallas_call x1, Pallas kernels, steps(): call(mix_kernel, [((half, 2048), BF)] * 2 + [((half, 256), BF)] * 2, [VM]...  5.57 us
    all_to_all x1, waiting for transfers between devices, steps(): square = lax.all_to_all(square, TP, 0, 0, tiled=True)  4.65 us
  transfers between devices with their start and end apart: 27, of which 6 were waited for; matrix products, arithmetic and copies ran while one was open for 1% of the time, Pallas kernels for 12%

profile of v4, /device:TPU:1, one launch (start us, length us, event | category | flops | bytes accessed | tf_op | source)
XLA Modules:
  0.0 141.2 jit_solution(8026690361825242091)
XLA Ops:
  6.6 1.9 %shard_map.157 = bf16[2112,128]{1,0:T(8,128)(2,1)} custom-call(bf16[704,128]{1,0:T(8,128)(2,1)} %bitcast.12, bf16[704,128]{1,0:T(8,128)(2,1)} %bitcast.13, bf16[704,128]{1,0:T(8,128)(2,1)} %d_ref.1), custom_call_target="tpu_custom_call" | custom-call | tf_op jit(solution)/shard_map/pallas_call | solution.py:353
  8.5 3.4 %collective-permute-start.2 = (bf16[1024,256]{1,0:T(8,128)(2,1)S(1)}, bf16[1024,256]{1,0:T(8,128)(2,1)S(1)}, u32[]{:S(2)}, u32[]{:S(2)}) collective-permute-start(bf16[1024,256]{1,0:T(8,128)(2,1)S(1)} %copy-done.1), channel_id=1, source_target_pairs={{0,6},{2,0},{4,2},{6,4},{1,7},{3,1},{5,3},{7,5},{8,14},{10,8},{12,... | collective-permute-start | bytes 1572872 | tf_op jit(solution)/shard_map/ppermute | solution.py:375
  14.5 11.1 %collective-permute-done.1.w1 = bf16[1024,256]{1,0:T(8,128)(2,1)S(1)} collective-permute-done((bf16[1024,256]{1,0:T(8,128)(2,1)S(1)}, bf16[1024,256]{1,0:T(8,128)(2,1)S(1)}, u32[]{:S(2)}, u32[]{:S(2)}) %collective-permute-start.1) | collective-permute-done | bytes 524320 | tf_op jit(solution)/shard_map/ppermute | solution.py:372
  25.6 3.2 %collective-permute-start = (f32[16,128]{1,0:T(8,128)S(1)}, f32[16,128]{1,0:T(8,128)S(1)}, u32[]{:S(2)}, u32[]{:S(2)}) collective-permute-start(f32[16,128]{1,0:T(8,128)S(1)} %pad_maximum_fusion), channel_id=1, source_target_pairs={{0,8},{8,16},{16,24},{24,32},{32,40},{40,48},{48,56},{56,64},{64,7... | collective-permute-start | bytes 24584 | tf_op jit(solution)/shard_map/ppermute | solution.py:381
  29.2 2.7 %collective-permute-start.11 = (bf16[784,256]{1,0:T(8,128)(2,1)S(1)}, bf16[784,256]{1,0:T(8,128)(2,1)}, u32[]{:S(2)}, u32[]{:S(2)}) collective-permute-start(bf16[784,256]{1,0:T(8,128)(2,1)S(1)} %concatenate.31.r0), channel_id=1, source_target_pairs={{0,6},{2,0},{4,2},{6,4},{1,7},{3,1},{5,3},{7,5},{8,14},{10,8},{12,... | collective-permute-start | bytes 1204232 | tf_op jit(solution)/shard_map/ppermute | solution.py:373
  31.9 3.1 %shard_map.154 = (f32[768,128]{1,0:T(8,128)S(1)}, f32[768,128]{1,0:T(8,128)S(1)}, f32[16,2,128]{2,1,0:T(2,128)S(1)}) custom-call(bf16[768,128]{1,0:T(8,128)(2,1)} %x_ref.1, f32[16,128]{1,0:T(8,128)S(1)} %collective-permute-done.rim_ref, f32[6,128]{1,0:T(8,128)S(1)} %convert_bitcast_fusion.ids_ref, bf16[4,128]{1,0:T(4,128)(2,1)} %taps_ref.1, ...), custom_call_target="tpu_custom_call" | custom-call | tf_op jit(solution)/shard_map/pallas_call | solution.py:385
  35.1 13.8 %all_to_all.15.e_ref = f32[16,2,128]{2,1,0:T(2,128)S(1)} all-to-all(f32[16,2,128]{2,1,0:T(2,128)S(1)} %get-tuple-element.39), channel_id=1, replica_groups=mesh['z'=4,'y'=4,'x'=4,'c'=2] {'z','y'}, dimensions={0} | all-to-all | bytes 32768 | tf_op jit(solution)/shard_map/all_to_all | solution.py:403
  48.9 2.1 %shard_map.155 = bf16[8,384,128]{2,1,0:T(8,128)(2,1)} custom-call(f32[768,128]{1,0:T(8,128)S(1)} %get-tuple-element.37.s_ref, f32[768,128]{1,0:T(8,128)S(1)} %get-tuple-element.38.p_ref, f32[16,2,128]{2,1,0:T(2,128)S(1)} %all_to_all.15.e_ref, bf16[768,128]{1,0:T(8,128)(2,1)} %g_ref.1), custom_call_target="tpu_custom_call" | custom-call | tf_op jit(solution)/shard_map/pallas_call | solution.py:404
  51.0 7.4 %all-to-all-start.1 = ((bf16[8,384,128]{2,1,0:T(8,128)(2,1)}), bf16[8,384,128]{2,1,0:T(8,128)(2,1)S(1)}, u32[]{:S(2)}, u32[]{:S(2)}) async-start(bf16[8,384,128]{2,1,0:T(8,128)(2,1)} %shard_map.155), calls=%async_computation.1 | async-start | bytes 1572864 | tf_op jit(solution)/shard_map/all_to_all | solution.py:407
  59.1 1.6 %collective-permute-start.10 = (bf16[784,256]{1,0:T(8,128)(2,1)S(1)}, bf16[784,256]{1,0:T(8,128)(2,1)S(1)}, u32[]{:S(2)}, u32[]{:S(2)}) collective-permute-start(bf16[784,256]{1,0:T(8,128)(2,1)S(1)} %concatenate.31.r0), channel_id=1, source_target_pairs={{0,2},{2,4},{4,6},{6,0},{1,3},{3,5},{5,7},{7,1},{8,10},{10,12},{12... | collective-permute-start | bytes 1204232 | tf_op jit(solution)/shard_map/ppermute | solution.py:374
  62.0 17.2 %collective-permute-done.10.r1 = bf16[784,256]{1,0:T(8,128)(2,1)S(1)} collective-permute-done((bf16[784,256]{1,0:T(8,128)(2,1)S(1)}, bf16[784,256]{1,0:T(8,128)(2,1)S(1)}, u32[]{:S(2)}, u32[]{:S(2)}) %collective-permute-start.10) | collective-permute-done | bytes 401440 | tf_op jit(solution)/shard_map/ppermute | solution.py:374
  81.0 5.6 %shard_map.156 = (bf16[384,2048]{1,0:T(8,128)(2,1)S(1)}, bf16[384,2048]{1,0:T(8,128)(2,1)S(1)}, bf16[384,256]{1,0:T(8,128)(2,1)S(1)}, bf16[384,256]{1,0:T(8,128)(2,1)S(1)}) custom-call(bf16[8,384,128]{2,1,0:T(8,128)(2,1)S(1)} %all-to-all-done.1.br_ref, bf16[1024,256]{1,0:T(8,128)(2,1)S(1)} %copy-done.1, bf16[1024,256]{1,0:T(8,128)(2,1)S(1)} %collective-permute-done.1.w1, ...), custom_call_target="tpu_custom_call" | custom-call | tf_op jit(solution)/shard_map/pallas_call | solution.py:414
  89.0 3.0 %collective-permute-done.13.n_ref = bf16[384,2048]{1,0:T(8,128)(2,1)S(1)} collective-permute-done((bf16[384,2048]{1,0:T(8,128)(2,1)S(1)}, bf16[384,2048]{1,0:T(8,128)(2,1)S(1)}, u32[]{:S(2)}, u32[]{:S(2)}) %collective-permute-start.13) | collective-permute-done | bytes 1572896 | tf_op jit(solution)/shard_map/ppermute | solution.py:342
  92.1 6.4 %shard_map.158 = (bf16[384,512]{1,0:T(8,128)(2,1)S(1)}, bf16[3,384,512]{2,1,0:T(8,128)(2,1)S(1)}, bf16[16,1408,128]{2,1,0:T(8,128)(2,1)S(1)}, bf16[16,704,128]{2,1,0:T(8,128)(2,1)S(1)}, bf16[384,2048]{1,0:T(8,128)(2,1)S(1)}) custom-call(bf16[384,2048]{1,0:T(8,128)(2,1)S(1)} %collective-permute-done.13.n_ref, bf16[384,2048]{1,0:T(8,128)(2,1)} %copy-done, ...), custom_call_target="tpu_custom_call" | custom-call | tf_op jit(solution)/shard_map/pallas_call | solution.py:429
  99.1 3.7 %shard_map.159 = (bf16[384,512]{1,0:T(8,128)(2,1)S(1)}, bf16[384,704]{1,0:T(8,128)(2,1)S(1)}) custom-call(bf16[384,2048]{1,0:T(8,128)(2,1)S(1)} %get-tuple-element.42.n_ref, bf16[16,1408,128]{2,1,0:T(8,128)(2,1)S(1)} %get-tuple-element.43.gu, bf16[16,704,128]{2,1,0:T(8,128)(2,1)S(1)} %get-tuple-element.44.dn), custom_call_target="tpu_custom_call" | custom-call | tf_op jit(solution)/shard_map/pallas_call | solution.py:444
  103.0 2.7 %collective-permute-start.19 = (bf16[192,512]{1,0:T(8,128)(2,1)S(1)}, bf16[192,512]{1,0:T(8,128)(2,1)S(1)}, u32[]{:S(2)}, u32[]{:S(2)}) collective-permute-start(bf16[192,512]{1,0:T(8,128)(2,1)S(1)} %get-tuple-element.53), channel_id=1, source_target_pairs={{0,6},{2,0},{4,2},{6,4},{1,7},{3,1},{5,3},{7,5},{8,14},{10,8},{12,... | collective-permute-start | bytes 589832 | tf_op jit(solution)/shard_map/ppermute | solution.py:451
  106.7 3.5 %collective-permute-done.18.r_ref = bf16[192,512]{1,0:T(8,128)(2,1)S(1)} collective-permute-done((bf16[192,512]{1,0:T(8,128)(2,1)S(1)}, bf16[192,512]{1,0:T(8,128)(2,1)S(1)}, u32[]{:S(2)}, u32[]{:S(2)}) %collective-permute-start.18) | collective-permute-done | bytes 196640 | tf_op jit(solution)/shard_map/ppermute | solution.py:450
  110.7 2.7 %collective-permute-start.21 = (bf16[192,512]{1,0:T(8,128)(2,1)S(1)}, bf16[192,512]{1,0:T(8,128)(2,1)S(1)}, u32[]{:S(2)}, u32[]{:S(2)}) collective-permute-start(bf16[192,512]{1,0:T(8,128)(2,1)S(1)} %get-tuple-element.59), channel_id=1, source_target_pairs={{0,6},{2,0},{4,2},{6,4},{1,7},{3,1},{5,3},{7,5},{8,14},{10,8},{12,... | collective-permute-start | bytes 589832 | tf_op jit(solution)/shard_map/ppermute | solution.py:463
  113.3 2.7 %collective-permute-start.16 = (bf16[192,512]{1,0:T(8,128)(2,1)S(1)}, bf16[192,512]{1,0:T(8,128)(2,1)S(1)}, u32[]{:S(2)}, u32[]{:S(2)}) collective-permute-start(bf16[192,512]{1,0:T(8,128)(2,1)S(1)} %get-tuple-element.49), channel_id=1, source_target_pairs={{0,6},{2,0},{4,2},{6,4},{1,7},{3,1},{5,3},{7,5},{8,14},{10,8},{12,... | collective-permute-start | bytes 589832 | tf_op jit(solution)/shard_map/ppermute | solution.py:459
  116.0 2.4 %collective-permute-start.23 = (bf16[384,256]{1,0:T(8,128)(2,1)S(1)}, bf16[384,256]{1,0:T(8,128)(2,1)S(1)}, u32[]{:S(2)}, u32[]{:S(2)}) collective-permute-start(bf16[384,256]{1,0:T(8,128)(2,1)S(1)} %copy-done.6), channel_id=1, source_target_pairs={{0,1},{1,0},{2,3},{3,2},{4,5},{5,4},{6,7},{7,6},{8,9},{9,8},{10,11... | collective-permute-start | bytes 589832 | tf_op jit(solution)/shard_map/ppermute | solution.py:342
  118.4 3.1 %collective-permute-done.15.fl_ref = bf16[192,512]{1,0:T(8,128)(2,1)S(1)} collective-permute-done((bf16[192,512]{1,0:T(8,128)(2,1)S(1)}, bf16[192,512]{1,0:T(8,128)(2,1)S(1)}, u32[]{:S(2)}, u32[]{:S(2)}) %collective-permute-start.15) | collective-permute-done | bytes 196640 | tf_op jit(solution)/shard_map/ppermute | solution.py:458
  122.4 1.9 %collective-permute-start.22 = (bf16[384,256]{1,0:T(8,128)(2,1)S(1)}, bf16[384,256]{1,0:T(8,128)(2,1)S(1)}, u32[]{:S(2)}, u32[]{:S(2)}) collective-permute-start(bf16[384,256]{1,0:T(8,128)(2,1)S(1)} %get-tuple-element.65), channel_id=1, source_target_pairs={{0,1},{1,0},{2,3},{3,2},{4,5},{5,4},{6,7},{7,6},{8,9},{9,8},{10,11... | collective-permute-start | bytes 589832 | tf_op jit(solution)/shard_map/ppermute | solution.py:342
  124.4 4.3 %all-to-all-start.2 = ((f32[8,3,128]{2,1,0:T(4,128)}), f32[8,3,128]{2,1,0:T(4,128)S(1)}, u32[]{:S(2)}, u32[]{:S(2)}) async-start(f32[8,3,128]{2,1,0:T(4,128)} %get-tuple-element.68), calls=%async_computation.2 | async-start | bytes 32768 | tf_op jit(solution)/shard_map/all_to_all | solution.py:473
  128.7 4.7 %all-to-all-done.2.sq_ref = f32[8,3,128]{2,1,0:T(4,128)S(1)} async-done(((f32[8,3,128]{2,1,0:T(4,128)}), f32[8,3,128]{2,1,0:T(4,128)S(1)}, u32[]{:S(2)}, u32[]{:S(2)}) %all-to-all-start.2) | async-done | bytes 12320 | tf_op jit(solution)/shard_map/all_to_all | solution.py:473
  (82 shorter events, 13.4 us)
Async XLA Ops:
  6.5 85.5 %all-gather.3.cloned.1.call-start = ((), (), s32[]{:S(2)}) async-start(), calls=%async_computation.3 | async-start | bytes 9191424 | tf_op jit(solution)/shard_map/all_gather | solution.py:360
  8.5 50.0 %collective-permute-start.2 = (bf16[1024,256]{1,0:T(8,128)(2,1)S(1)}, bf16[1024,256]{1,0:T(8,128)(2,1)S(1)}, u32[]{:S(2)}, u32[]{:S(2)}) collective-permute-start(bf16[1024,256]{1,0:T(8,128)(2,1)S(1)} %copy-done.1), channel_id=1, source_target_pairs={{0,6},{2,0},{4,2},{6,4},{1,7},{3,1},{5,3},{7,5},{8,14},{10,8},{12,... | collective-permute-start | bytes 1572872 | tf_op jit(solution)/shard_map/ppermute | solution.py:375
  11.9 13.7 %collective-permute-start.1 = (bf16[1024,256]{1,0:T(8,128)(2,1)S(1)}, bf16[1024,256]{1,0:T(8,128)(2,1)S(1)}, u32[]{:S(2)}, u32[]{:S(2)}) collective-permute-start(bf16[1024,256]{1,0:T(8,128)(2,1)S(1)} %copy-done.1), channel_id=1, source_target_pairs={{0,2},{2,4},{4,6},{6,0},{1,3},{3,5},{5,7},{7,1},{8,10},{10,12},{12... | collective-permute-start | bytes 1572872 | tf_op jit(solution)/shard_map/ppermute | solution.py:372
  11.9 47.2 %collective-permute-start.4 = (bf16[1024,256]{1,0:T(8,128)(2,1)S(1)}, bf16[1024,256]{1,0:T(8,128)(2,1)S(1)}, u32[]{:S(2)}, u32[]{:S(2)}) collective-permute-start(bf16[1024,256]{1,0:T(8,128)(2,1)S(1)} %copy-done.1), channel_id=1, source_target_pairs={{0,1},{1,0},{2,3},{3,2},{4,5},{5,4},{6,7},{7,6},{8,9},{9,8},{10,11... | collective-permute-start | bytes 1572872 | tf_op jit(solution)/shard_map/ppermute | solution.py:342
  12.9 12.7 %collective-permute-start.9 = (bf16[6,256]{1,0:T(8,128)(2,1)S(1)}, bf16[6,256]{1,0:T(8,128)(2,1)S(1)}, u32[]{:S(2)}, u32[]{:S(2)}) collective-permute-start(bf16[6,256]{1,0:T(8,128)(2,1)S(1)} %convert_element_type.16), channel_id=1, source_target_pairs={{0,1},{1,0},{2,3},{3,2},{4,5},{5,4},{6,7},{7,6},{8,9},{9,8},{10,11... | collective-permute-start | bytes 9224 | tf_op jit(solution)/shard_map/ppermute | solution.py:342
  13.1 15.8 %collective-permute-start.8 = (bf16[384,256]{1,0:T(8,128)(2,1)S(1)}, bf16[384,256]{1,0:T(8,128)(2,1)S(1)}, u32[]{:S(2)}, u32[]{:S(2)}) collective-permute-start(bf16[384,256]{1,0:T(8,128)(2,1)S(1)} %get-tuple-element.69), channel_id=1, source_target_pairs={{0,1},{1,0},{2,3},{3,2},{4,5},{5,4},{6,7},{7,6},{8,9},{9,8},{10,11... | collective-permute-start | bytes 589832 | tf_op jit(solution)/shard_map/ppermute | solution.py:342
  25.6 33.3 %collective-permute-start.3 = (bf16[1024,256]{1,0:T(8,128)(2,1)S(1)}, bf16[1024,256]{1,0:T(8,128)(2,1)}, u32[]{:S(2)}, u32[]{:S(2)}) collective-permute-start(bf16[1024,256]{1,0:T(8,128)(2,1)S(1)} %collective-permute-done.1.w1), channel_id=1, source_target_pairs={{0,2},{2,4},{4,6},{6,0},{1,3},{3,5},{5,7},{7,1},{8,10},{10,12},{12... | collective-permute-start | bytes 1572872 | tf_op jit(solution)/shard_map/ppermute | solution.py:408
  29.2 31.5 %collective-permute-start.11 = (bf16[784,256]{1,0:T(8,128)(2,1)S(1)}, bf16[784,256]{1,0:T(8,128)(2,1)}, u32[]{:S(2)}, u32[]{:S(2)}) collective-permute-start(bf16[784,256]{1,0:T(8,128)(2,1)S(1)} %concatenate.31.r0), channel_id=1, source_target_pairs={{0,6},{2,0},{4,2},{6,4},{1,7},{3,1},{5,3},{7,5},{8,14},{10,8},{12,... | collective-permute-start | bytes 1204232 | tf_op jit(solution)/shard_map/ppermute | solution.py:373
  51.0 29.0 %all-to-all-start.1 = ((bf16[8,384,128]{2,1,0:T(8,128)(2,1)}), bf16[8,384,128]{2,1,0:T(8,128)(2,1)S(1)}, u32[]{:S(2)}, u32[]{:S(2)}) async-start(bf16[8,384,128]{2,1,0:T(8,128)(2,1)} %shard_map.155), calls=%async_computation.1 | async-start | bytes 1572864 | tf_op jit(solution)/shard_map/all_to_all | solution.py:407
  58.4 21.6 %collective-permute-start.5 = (bf16[1024,256]{1,0:T(8,128)(2,1)S(1)}, bf16[1024,256]{1,0:T(8,128)(2,1)}, u32[]{:S(2)}, u32[]{:S(2)}) collective-permute-start(bf16[1024,256]{1,0:T(8,128)(2,1)S(1)} %collective-permute-done.1.w1), channel_id=1, source_target_pairs={{0,1},{1,0},{2,3},{3,2},{4,5},{5,4},{6,7},{7,6},{8,9},{9,8},{10,11... | collective-permute-start | bytes 1572872 | tf_op jit(solution)/shard_map/ppermute | solution.py:342
  58.6 21.4 %collective-permute-start.6 = (bf16[1024,256]{1,0:T(8,128)(2,1)S(1)}, bf16[1024,256]{1,0:T(8,128)(2,1)}, u32[]{:S(2)}, u32[]{:S(2)}) collective-permute-start(bf16[1024,256]{1,0:T(8,128)(2,1)S(1)} %collective-permute-done.2.w2), channel_id=1, source_target_pairs={{0,1},{1,0},{2,3},{3,2},{4,5},{5,4},{6,7},{7,6},{8,9},{9,8},{10,11... | collective-permute-start | bytes 1572872 | tf_op jit(solution)/shard_map/ppermute | solution.py:342
  58.9 21.1 %collective-permute-start.7 = (bf16[1024,256]{1,0:T(8,128)(2,1)}, bf16[1024,256]{1,0:T(8,128)(2,1)}, u32[]{:S(2)}, u32[]{:S(2)}) collective-permute-start(bf16[1024,256]{1,0:T(8,128)(2,1)} %collective-permute-done.3.w3), channel_id=1, source_target_pairs={{0,1},{1,0},{2,3},{3,2},{4,5},{5,4},{6,7},{7,6},{8,9},{9,8},{10,11... | collective-permute-start | bytes 1572872 | tf_op jit(solution)/shard_map/ppermute | solution.py:342
  59.1 20.1 %collective-permute-start.10 = (bf16[784,256]{1,0:T(8,128)(2,1)S(1)}, bf16[784,256]{1,0:T(8,128)(2,1)S(1)}, u32[]{:S(2)}, u32[]{:S(2)}) collective-permute-start(bf16[784,256]{1,0:T(8,128)(2,1)S(1)} %concatenate.31.r0), channel_id=1, source_target_pairs={{0,2},{2,4},{4,6},{6,0},{1,3},{3,5},{5,7},{7,1},{8,10},{10,12},{12... | collective-permute-start | bytes 1204232 | tf_op jit(solution)/shard_map/ppermute | solution.py:374
  60.7 19.3 %collective-permute-start.12 = (bf16[784,256]{1,0:T(8,128)(2,1)}, bf16[784,256]{1,0:T(8,128)(2,1)}, u32[]{:S(2)}, u32[]{:S(2)}) collective-permute-start(bf16[784,256]{1,0:T(8,128)(2,1)} %collective-permute-done.11.r2), channel_id=1, source_target_pairs={{0,6},{2,0},{4,2},{6,4},{1,7},{3,1},{5,3},{7,5},{8,14},{10,8},{12,... | collective-permute-start | bytes 1204232 | tf_op jit(solution)/shard_map/ppermute | solution.py:409
  98.5 11.8 %collective-permute-start.14 = (bf16[3,384,512]{2,1,0:T(8,128)(2,1)S(1)}, bf16[3,384,512]{2,1,0:T(8,128)(2,1)S(1)}, u32[]{:S(2)}, u32[]{:S(2)}) collective-permute-start(bf16[3,384,512]{2,1,0:T(8,128)(2,1)S(1)} %get-tuple-element.46), channel_id=1, source_target_pairs={{0,1},{1,0},{2,3},{3,2},{4,5},{5,4},{6,7},{7,6},{8,9},{9,8},{10,11... | collective-permute-start | bytes 3538952 | tf_op jit(solution)/shard_map/ppermute | solution.py:342
  102.9 7.4 %collective-permute-start.18 = (bf16[192,512]{1,0:T(8,128)(2,1)S(1)}, bf16[192,512]{1,0:T(8,128)(2,1)S(1)}, u32[]{:S(2)}, u32[]{:S(2)}) collective-permute-start(bf16[192,512]{1,0:T(8,128)(2,1)S(1)} %get-tuple-element.52), channel_id=1, source_target_pairs={{0,2},{2,4},{4,6},{6,0},{1,3},{3,5},{5,7},{7,1},{8,10},{10,12},{12... | collective-permute-start | bytes 589832 | tf_op jit(solution)/shard_map/ppermute | solution.py:450
  103.0 7.3 %collective-permute-start.19 = (bf16[192,512]{1,0:T(8,128)(2,1)S(1)}, bf16[192,512]{1,0:T(8,128)(2,1)S(1)}, u32[]{:S(2)}, u32[]{:S(2)}) collective-permute-start(bf16[192,512]{1,0:T(8,128)(2,1)S(1)} %get-tuple-element.53), channel_id=1, source_target_pairs={{0,6},{2,0},{4,2},{6,4},{1,7},{3,1},{5,3},{7,5},{8,14},{10,8},{12,... | collective-permute-start | bytes 589832 | tf_op jit(solution)/shard_map/ppermute | solution.py:451
  110.6 7.8 %collective-permute-start.20 = (bf16[192,512]{1,0:T(8,128)(2,1)S(1)}, bf16[192,512]{1,0:T(8,128)(2,1)S(1)}, u32[]{:S(2)}, u32[]{:S(2)}) collective-permute-start(bf16[192,512]{1,0:T(8,128)(2,1)S(1)} %get-tuple-element.58), channel_id=1, source_target_pairs={{0,2},{2,4},{4,6},{6,0},{1,3},{3,5},{5,7},{7,1},{8,10},{10,12},{12... | collective-permute-start | bytes 589832 | tf_op jit(solution)/shard_map/ppermute | solution.py:462
  110.7 7.7 %collective-permute-start.21 = (bf16[192,512]{1,0:T(8,128)(2,1)S(1)}, bf16[192,512]{1,0:T(8,128)(2,1)S(1)}, u32[]{:S(2)}, u32[]{:S(2)}) collective-permute-start(bf16[192,512]{1,0:T(8,128)(2,1)S(1)} %get-tuple-element.59), channel_id=1, source_target_pairs={{0,6},{2,0},{4,2},{6,4},{1,7},{3,1},{5,3},{7,5},{8,14},{10,8},{12,... | collective-permute-start | bytes 589832 | tf_op jit(solution)/shard_map/ppermute | solution.py:463
  113.3 8.1 %collective-permute-start.15 = (bf16[192,512]{1,0:T(8,128)(2,1)S(1)}, bf16[192,512]{1,0:T(8,128)(2,1)S(1)}, u32[]{:S(2)}, u32[]{:S(2)}) collective-permute-start(bf16[192,512]{1,0:T(8,128)(2,1)S(1)} %get-tuple-element.48), channel_id=1, source_target_pairs={{0,2},{2,4},{4,6},{6,0},{1,3},{3,5},{5,7},{7,1},{8,10},{10,12},{12... | collective-permute-start | bytes 589832 | tf_op jit(solution)/shard_map/ppermute | solution.py:458
  113.3 8.1 %collective-permute-start.16 = (bf16[192,512]{1,0:T(8,128)(2,1)S(1)}, bf16[192,512]{1,0:T(8,128)(2,1)S(1)}, u32[]{:S(2)}, u32[]{:S(2)}) collective-permute-start(bf16[192,512]{1,0:T(8,128)(2,1)S(1)} %get-tuple-element.49), channel_id=1, source_target_pairs={{0,6},{2,0},{4,2},{6,4},{1,7},{3,1},{5,3},{7,5},{8,14},{10,8},{12,... | collective-permute-start | bytes 589832 | tf_op jit(solution)/shard_map/ppermute | solution.py:459
  116.0 12.7 %collective-permute-start.23 = (bf16[384,256]{1,0:T(8,128)(2,1)S(1)}, bf16[384,256]{1,0:T(8,128)(2,1)S(1)}, u32[]{:S(2)}, u32[]{:S(2)}) collective-permute-start(bf16[384,256]{1,0:T(8,128)(2,1)S(1)} %copy-done.6), channel_id=1, source_target_pairs={{0,1},{1,0},{2,3},{3,2},{4,5},{5,4},{6,7},{7,6},{8,9},{9,8},{10,11... | collective-permute-start | bytes 589832 | tf_op jit(solution)/shard_map/ppermute | solution.py:342
  122.4 10.9 %collective-permute-start.22 = (bf16[384,256]{1,0:T(8,128)(2,1)S(1)}, bf16[384,256]{1,0:T(8,128)(2,1)S(1)}, u32[]{:S(2)}, u32[]{:S(2)}) collective-permute-start(bf16[384,256]{1,0:T(8,128)(2,1)S(1)} %get-tuple-element.65), channel_id=1, source_target_pairs={{0,1},{1,0},{2,3},{3,2},{4,5},{5,4},{6,7},{7,6},{8,9},{9,8},{10,11... | collective-permute-start | bytes 589832 | tf_op jit(solution)/shard_map/ppermute | solution.py:342
  124.4 9.0 %all-to-all-start.2 = ((f32[8,3,128]{2,1,0:T(4,128)}), f32[8,3,128]{2,1,0:T(4,128)S(1)}, u32[]{:S(2)}, u32[]{:S(2)}) async-start(f32[8,3,128]{2,1,0:T(4,128)} %get-tuple-element.68), calls=%async_computation.2 | async-start | bytes 32768 | tf_op jit(solution)/shard_map/all_to_all | solution.py:473
  (15 other events, 103.0 us)
Sparse Core Ops, SparseCore 0:
  9.5 75.3 all-gather.2

commit v5 on v4

--- a/solution.py
+++ b/solution.py
@@ -199,12 +199,14 @@
 
 
 def hidden_part(src, gu, lo, hi):
-    turned = (((1,), (1,)), ((), ()))
-    gate = jnp.concatenate([gu[s, lo:hi, :] for s in range(16)], axis=1)
-    up = jnp.concatenate([gu[s, 704 + lo : 704 + hi, :] for s in range(16)], axis=1)
-    g = lax.dot_general(src, gate, turned, preferred_element_type=F32)
-    u = lax.dot_general(src, up, turned, preferred_element_type=F32)
-    return (jax.nn.silu(g) * u).astype(BF)
+    rows = [
+        jnp.concatenate([gu[s, base + lo : base + hi, :] for s in range(16)], axis=1)
+        for base in (0, 704)
+    ]
+    act = lax.dot_general(
+        src, jnp.concatenate(rows), (((1,), (1,)), ((), ())), preferred_element_type=F32
+    )
+    return (jax.nn.silu(act[:, : hi - lo]) * act[:, hi - lo :]).astype(BF)
 
 
 def first_kernel(n_ref, own_hbm, w_ref, far_ref, rest_ref, gu, dn, own_ref, hid, sem):
@@ -222,9 +224,9 @@
             ]
         )
     downs = [
-        pltpu.make_async_copy(w_ref.at[s, pl.ds(1408, 704)], dn.at[s], sem.at[3]) for s in range(16)
+        pltpu.make_async_copy(w_ref.at[s, pl.ds(1408, 704)], dn.at[s], sem.at[4]) for s in range(16)
     ]
-    own_copy = pltpu.make_async_copy(own_hbm, own_ref, sem.at[4])
+    own_copy = pltpu.make_async_copy(own_hbm, own_ref, sem.at[5])
     for group in groups + [downs, [own_copy]]:
         for cp in group:
             cp.start()
@@ -436,7 +438,7 @@
             ((half, 2048), BF),
         ],
         [VM, HB, HB],
-        [pltpu.VMEM((half, 704), BF), pltpu.SemaphoreType.DMA((5,))],
+        [pltpu.VMEM((half, 704), BF), pltpu.SemaphoreType.DMA((6,))],
         limit=18,
     )(norm_oth, norm_own, weights)
     far_in = swapped(far_oth)

time: 142 us -> 141 us (level)
  transfers between devices with their start and end apart: 27 -> 27, of which waited for: 6 -> 6; matrix products, arithmetic and copies ran while one was open for 1% -> 1% of each run, Pallas kernels for 12% -> 11%
where the time goes in v5:
time: 141 us
  waiting for transfers between devices  42.7 us (30%)
  starting transfers between devices  40 us (28%)
  Pallas kernels  25.6 us (18%)
  blocking collectives  13.8 us (10%)
  between operations  13.7 us (10%)
  local copies, waits for them, and re-layouts  4.61 us (3%)
    ppermute x1, waiting for transfers between devices, steps(): res_left = lax.ppermute(res, 'x', cyc(4, 1))  17.2 us
    all_to_all x1, blocking collectives, steps(): all_ends = lax.all_to_all(ends, SP, 0, 0, tiled=True)  13.8 us
    ppermute x1, waiting for transfers between devices, steps(): out_left = lax.ppermute(out_weight, 'x', cyc(4, 1))  11.1 us
    ppermute x11, starting transfers between devices, swapped(): return lax.ppermute(block, 'c', cyc(2, 1))  7.85 us
    all_to_all x1, starting transfers between devices, steps(): branch = lax.all_to_all(branch, TP, 0, 0, tiled=True)  7.43 us
    pallas_call x1, Pallas kernels, steps(): call(first_kernel, [((half, 512), BF), ((3, half, 512), BF), ((16, 1408,...  6.52 us
    pallas_call x1, Pallas kernels, steps(): call(mix_kernel, [((half, 2048), BF)] * 2 + [((half, 256), BF)] * 2, [VM]...  5.57 us
    all_to_all x1, waiting for transfers between devices, steps(): square = lax.all_to_all(square, TP, 0, 0, tiled=True)  4.65 us
  transfers between devices with their start and end apart: 27, of which 6 were waited for; matrix products, arithmetic and copies ran while one was open for 1% of the time, Pallas kernels for 11%

profile of v5, /device:TPU:1, one launch (start us, length us, event | category | flops | bytes accessed | tf_op | source)
XLA Modules:
  0.0 140.6 jit_solution(7185476593828041869)
XLA Ops:
  6.6 1.9 %shard_map.157 = bf16[2112,128]{1,0:T(8,128)(2,1)} custom-call(bf16[704,128]{1,0:T(8,128)(2,1)} %bitcast.12, bf16[704,128]{1,0:T(8,128)(2,1)} %bitcast.13, bf16[704,128]{1,0:T(8,128)(2,1)} %d_ref.1), custom_call_target="tpu_custom_call" | custom-call | tf_op jit(solution)/shard_map/pallas_call | solution.py:355
  8.5 3.4 %collective-permute-start.2 = (bf16[1024,256]{1,0:T(8,128)(2,1)S(1)}, bf16[1024,256]{1,0:T(8,128)(2,1)S(1)}, u32[]{:S(2)}, u32[]{:S(2)}) collective-permute-start(bf16[1024,256]{1,0:T(8,128)(2,1)S(1)} %copy-done.1), channel_id=1, source_target_pairs={{0,6},{2,0},{4,2},{6,4},{1,7},{3,1},{5,3},{7,5},{8,14},{10,8},{12,... | collective-permute-start | bytes 1572872 | tf_op jit(solution)/shard_map/ppermute | solution.py:377
  14.5 11.1 %collective-permute-done.1.w1 = bf16[1024,256]{1,0:T(8,128)(2,1)S(1)} collective-permute-done((bf16[1024,256]{1,0:T(8,128)(2,1)S(1)}, bf16[1024,256]{1,0:T(8,128)(2,1)S(1)}, u32[]{:S(2)}, u32[]{:S(2)}) %collective-permute-start.1) | collective-permute-done | bytes 524320 | tf_op jit(solution)/shard_map/ppermute | solution.py:374
  25.6 3.2 %collective-permute-start = (f32[16,128]{1,0:T(8,128)S(1)}, f32[16,128]{1,0:T(8,128)S(1)}, u32[]{:S(2)}, u32[]{:S(2)}) collective-permute-start(f32[16,128]{1,0:T(8,128)S(1)} %pad_maximum_fusion), channel_id=1, source_target_pairs={{0,8},{8,16},{16,24},{24,32},{32,40},{40,48},{48,56},{56,64},{64,7... | collective-permute-start | bytes 24584 | tf_op jit(solution)/shard_map/ppermute | solution.py:383
  29.2 2.7 %collective-permute-start.11 = (bf16[784,256]{1,0:T(8,128)(2,1)S(1)}, bf16[784,256]{1,0:T(8,128)(2,1)}, u32[]{:S(2)}, u32[]{:S(2)}) collective-permute-start(bf16[784,256]{1,0:T(8,128)(2,1)S(1)} %concatenate.31.r0), channel_id=1, source_target_pairs={{0,6},{2,0},{4,2},{6,4},{1,7},{3,1},{5,3},{7,5},{8,14},{10,8},{12,... | collective-permute-start | bytes 1204232 | tf_op jit(solution)/shard_map/ppermute | solution.py:375
  31.9 3.1 %shard_map.154 = (f32[768,128]{1,0:T(8,128)S(1)}, f32[768,128]{1,0:T(8,128)S(1)}, f32[16,2,128]{2,1,0:T(2,128)S(1)}) custom-call(bf16[768,128]{1,0:T(8,128)(2,1)} %x_ref.1, f32[16,128]{1,0:T(8,128)S(1)} %collective-permute-done.rim_ref, f32[6,128]{1,0:T(8,128)S(1)} %convert_bitcast_fusion.ids_ref, bf16[4,128]{1,0:T(4,128)(2,1)} %taps_ref.1, ...), custom_call_target="tpu_custom_call" | custom-call | tf_op jit(solution)/shard_map/pallas_call | solution.py:387
  35.1 13.8 %all_to_all.15.e_ref = f32[16,2,128]{2,1,0:T(2,128)S(1)} all-to-all(f32[16,2,128]{2,1,0:T(2,128)S(1)} %get-tuple-element.39), channel_id=1, replica_groups=mesh['z'=4,'y'=4,'x'=4,'c'=2] {'z','y'}, dimensions={0} | all-to-all | bytes 32768 | tf_op jit(solution)/shard_map/all_to_all | solution.py:405
  48.9 2.1 %shard_map.155 = bf16[8,384,128]{2,1,0:T(8,128)(2,1)} custom-call(f32[768,128]{1,0:T(8,128)S(1)} %get-tuple-element.37.s_ref, f32[768,128]{1,0:T(8,128)S(1)} %get-tuple-element.38.p_ref, f32[16,2,128]{2,1,0:T(2,128)S(1)} %all_to_all.15.e_ref, bf16[768,128]{1,0:T(8,128)(2,1)} %g_ref.1), custom_call_target="tpu_custom_call" | custom-call | tf_op jit(solution)/shard_map/pallas_call | solution.py:406
  51.0 7.4 %all-to-all-start.1 = ((bf16[8,384,128]{2,1,0:T(8,128)(2,1)}), bf16[8,384,128]{2,1,0:T(8,128)(2,1)S(1)}, u32[]{:S(2)}, u32[]{:S(2)}) async-start(bf16[8,384,128]{2,1,0:T(8,128)(2,1)} %shard_map.155), calls=%async_computation.1 | async-start | bytes 1572864 | tf_op jit(solution)/shard_map/all_to_all | solution.py:409
  59.1 1.6 %collective-permute-start.10 = (bf16[784,256]{1,0:T(8,128)(2,1)S(1)}, bf16[784,256]{1,0:T(8,128)(2,1)S(1)}, u32[]{:S(2)}, u32[]{:S(2)}) collective-permute-start(bf16[784,256]{1,0:T(8,128)(2,1)S(1)} %concatenate.31.r0), channel_id=1, source_target_pairs={{0,2},{2,4},{4,6},{6,0},{1,3},{3,5},{5,7},{7,1},{8,10},{10,12},{12... | collective-permute-start | bytes 1204232 | tf_op jit(solution)/shard_map/ppermute | solution.py:376
  62.0 17.2 %collective-permute-done.10.r1 = bf16[784,256]{1,0:T(8,128)(2,1)S(1)} collective-permute-done((bf16[784,256]{1,0:T(8,128)(2,1)S(1)}, bf16[784,256]{1,0:T(8,128)(2,1)S(1)}, u32[]{:S(2)}, u32[]{:S(2)}) %collective-permute-start.10) | collective-permute-done | bytes 401440 | tf_op jit(solution)/shard_map/ppermute | solution.py:376
  81.0 5.6 %shard_map.156 = (bf16[384,2048]{1,0:T(8,128)(2,1)S(1)}, bf16[384,2048]{1,0:T(8,128)(2,1)S(1)}, bf16[384,256]{1,0:T(8,128)(2,1)S(1)}, bf16[384,256]{1,0:T(8,128)(2,1)S(1)}) custom-call(bf16[8,384,128]{2,1,0:T(8,128)(2,1)S(1)} %all-to-all-done.1.br_ref, bf16[1024,256]{1,0:T(8,128)(2,1)S(1)} %copy-done.1, bf16[1024,256]{1,0:T(8,128)(2,1)S(1)} %collective-permute-done.1.w1, ...), custom_call_target="tpu_custom_call" | custom-call | tf_op jit(solution)/shard_map/pallas_call | solution.py:416
  89.0 3.0 %collective-permute-done.13.n_ref = bf16[384,2048]{1,0:T(8,128)(2,1)S(1)} collective-permute-done((bf16[384,2048]{1,0:T(8,128)(2,1)S(1)}, bf16[384,2048]{1,0:T(8,128)(2,1)S(1)}, u32[]{:S(2)}, u32[]{:S(2)}) %collective-permute-start.13) | collective-permute-done | bytes 1572896 | tf_op jit(solution)/shard_map/ppermute | solution.py:344
  92.1 6.5 %shard_map.158 = (bf16[384,512]{1,0:T(8,128)(2,1)S(1)}, bf16[3,384,512]{2,1,0:T(8,128)(2,1)S(1)}, bf16[16,1408,128]{2,1,0:T(8,128)(2,1)S(1)}, bf16[16,704,128]{2,1,0:T(8,128)(2,1)S(1)}, bf16[384,2048]{1,0:T(8,128)(2,1)S(1)}) custom-call(bf16[384,2048]{1,0:T(8,128)(2,1)S(1)} %collective-permute-done.13.n_ref, bf16[384,2048]{1,0:T(8,128)(2,1)} %copy-done, ...), custom_call_target="tpu_custom_call" | custom-call | tf_op jit(solution)/shard_map/pallas_call | solution.py:431
  99.2 3.0 %shard_map.159 = (bf16[384,512]{1,0:T(8,128)(2,1)S(1)}, bf16[384,704]{1,0:T(8,128)(2,1)S(1)}) custom-call(bf16[384,2048]{1,0:T(8,128)(2,1)S(1)} %get-tuple-element.42.n_ref, bf16[16,1408,128]{2,1,0:T(8,128)(2,1)S(1)} %get-tuple-element.43.gu, bf16[16,704,128]{2,1,0:T(8,128)(2,1)S(1)} %get-tuple-element.44.dn), custom_call_target="tpu_custom_call" | custom-call | tf_op jit(solution)/shard_map/pallas_call | solution.py:446
  102.4 2.7 %collective-permute-start.19 = (bf16[192,512]{1,0:T(8,128)(2,1)S(1)}, bf16[192,512]{1,0:T(8,128)(2,1)S(1)}, u32[]{:S(2)}, u32[]{:S(2)}) collective-permute-start(bf16[192,512]{1,0:T(8,128)(2,1)S(1)} %get-tuple-element.53), channel_id=1, source_target_pairs={{0,6},{2,0},{4,2},{6,4},{1,7},{3,1},{5,3},{7,5},{8,14},{10,8},{12,... | collective-permute-start | bytes 589832 | tf_op jit(solution)/shard_map/ppermute | solution.py:453
  106.1 3.5 %collective-permute-done.18.r_ref = bf16[192,512]{1,0:T(8,128)(2,1)S(1)} collective-permute-done((bf16[192,512]{1,0:T(8,128)(2,1)S(1)}, bf16[192,512]{1,0:T(8,128)(2,1)S(1)}, u32[]{:S(2)}, u32[]{:S(2)}) %collective-permute-start.18) | collective-permute-done | bytes 196640 | tf_op jit(solution)/shard_map/ppermute | solution.py:452
  110.1 2.7 %collective-permute-start.21 = (bf16[192,512]{1,0:T(8,128)(2,1)S(1)}, bf16[192,512]{1,0:T(8,128)(2,1)S(1)}, u32[]{:S(2)}, u32[]{:S(2)}) collective-permute-start(bf16[192,512]{1,0:T(8,128)(2,1)S(1)} %get-tuple-element.59), channel_id=1, source_target_pairs={{0,6},{2,0},{4,2},{6,4},{1,7},{3,1},{5,3},{7,5},{8,14},{10,8},{12,... | collective-permute-start | bytes 589832 | tf_op jit(solution)/shard_map/ppermute | solution.py:465
  112.8 2.7 %collective-permute-start.16 = (bf16[192,512]{1,0:T(8,128)(2,1)S(1)}, bf16[192,512]{1,0:T(8,128)(2,1)S(1)}, u32[]{:S(2)}, u32[]{:S(2)}) collective-permute-start(bf16[192,512]{1,0:T(8,128)(2,1)S(1)} %get-tuple-element.49), channel_id=1, source_target_pairs={{0,6},{2,0},{4,2},{6,4},{1,7},{3,1},{5,3},{7,5},{8,14},{10,8},{12,... | collective-permute-start | bytes 589832 | tf_op jit(solution)/shard_map/ppermute | solution.py:461
  115.4 2.3 %collective-permute-start.23 = (bf16[384,256]{1,0:T(8,128)(2,1)S(1)}, bf16[384,256]{1,0:T(8,128)(2,1)S(1)}, u32[]{:S(2)}, u32[]{:S(2)}) collective-permute-start(bf16[384,256]{1,0:T(8,128)(2,1)S(1)} %copy-done.6), channel_id=1, source_target_pairs={{0,1},{1,0},{2,3},{3,2},{4,5},{5,4},{6,7},{7,6},{8,9},{9,8},{10,11... | collective-permute-start | bytes 589832 | tf_op jit(solution)/shard_map/ppermute | solution.py:344
  117.8 3.1 %collective-permute-done.15.fl_ref = bf16[192,512]{1,0:T(8,128)(2,1)S(1)} collective-permute-done((bf16[192,512]{1,0:T(8,128)(2,1)S(1)}, bf16[192,512]{1,0:T(8,128)(2,1)S(1)}, u32[]{:S(2)}, u32[]{:S(2)}) %collective-permute-start.15) | collective-permute-done | bytes 196640 | tf_op jit(solution)/shard_map/ppermute | solution.py:460
  121.8 1.9 %collective-permute-start.22 = (bf16[384,256]{1,0:T(8,128)(2,1)S(1)}, bf16[384,256]{1,0:T(8,128)(2,1)S(1)}, u32[]{:S(2)}, u32[]{:S(2)}) collective-permute-start(bf16[384,256]{1,0:T(8,128)(2,1)S(1)} %get-tuple-element.65), channel_id=1, source_target_pairs={{0,1},{1,0},{2,3},{3,2},{4,5},{5,4},{6,7},{7,6},{8,9},{9,8},{10,11... | collective-permute-start | bytes 589832 | tf_op jit(solution)/shard_map/ppermute | solution.py:344
  123.8 4.3 %all-to-all-start.2 = ((f32[8,3,128]{2,1,0:T(4,128)}), f32[8,3,128]{2,1,0:T(4,128)S(1)}, u32[]{:S(2)}, u32[]{:S(2)}) async-start(f32[8,3,128]{2,1,0:T(4,128)} %get-tuple-element.68), calls=%async_computation.2 | async-start | bytes 32768 | tf_op jit(solution)/shard_map/all_to_all | solution.py:475
  128.1 4.7 %all-to-all-done.2.sq_ref = f32[8,3,128]{2,1,0:T(4,128)S(1)} async-done(((f32[8,3,128]{2,1,0:T(4,128)}), f32[8,3,128]{2,1,0:T(4,128)S(1)}, u32[]{:S(2)}, u32[]{:S(2)}) %all-to-all-start.2) | async-done | bytes 12320 | tf_op jit(solution)/shard_map/all_to_all | solution.py:475
  (82 shorter events, 13.4 us)
Async XLA Ops:
  6.5 85.5 %all-gather.3.cloned.1.call-start = ((), (), s32[]{:S(2)}) async-start(), calls=%async_computation.3 | async-start | bytes 9191424 | tf_op jit(solution)/shard_map/all_gather | solution.py:362
  8.5 50.0 %collective-permute-start.2 = (bf16[1024,256]{1,0:T(8,128)(2,1)S(1)}, bf16[1024,256]{1,0:T(8,128)(2,1)S(1)}, u32[]{:S(2)}, u32[]{:S(2)}) collective-permute-start(bf16[1024,256]{1,0:T(8,128)(2,1)S(1)} %copy-done.1), channel_id=1, source_target_pairs={{0,6},{2,0},{4,2},{6,4},{1,7},{3,1},{5,3},{7,5},{8,14},{10,8},{12,... | collective-permute-start | bytes 1572872 | tf_op jit(solution)/shard_map/ppermute | solution.py:377
  11.9 13.7 %collective-permute-start.1 = (bf16[1024,256]{1,0:T(8,128)(2,1)S(1)}, bf16[1024,256]{1,0:T(8,128)(2,1)S(1)}, u32[]{:S(2)}, u32[]{:S(2)}) collective-permute-start(bf16[1024,256]{1,0:T(8,128)(2,1)S(1)} %copy-done.1), channel_id=1, source_target_pairs={{0,2},{2,4},{4,6},{6,0},{1,3},{3,5},{5,7},{7,1},{8,10},{10,12},{12... | collective-permute-start | bytes 1572872 | tf_op jit(solution)/shard_map/ppermute | solution.py:374
  11.9 47.2 %collective-permute-start.4 = (bf16[1024,256]{1,0:T(8,128)(2,1)S(1)}, bf16[1024,256]{1,0:T(8,128)(2,1)S(1)}, u32[]{:S(2)}, u32[]{:S(2)}) collective-permute-start(bf16[1024,256]{1,0:T(8,128)(2,1)S(1)} %copy-done.1), channel_id=1, source_target_pairs={{0,1},{1,0},{2,3},{3,2},{4,5},{5,4},{6,7},{7,6},{8,9},{9,8},{10,11... | collective-permute-start | bytes 1572872 | tf_op jit(solution)/shard_map/ppermute | solution.py:344
  12.9 12.7 %collective-permute-start.9 = (bf16[6,256]{1,0:T(8,128)(2,1)S(1)}, bf16[6,256]{1,0:T(8,128)(2,1)S(1)}, u32[]{:S(2)}, u32[]{:S(2)}) collective-permute-start(bf16[6,256]{1,0:T(8,128)(2,1)S(1)} %convert_element_type.16), channel_id=1, source_target_pairs={{0,1},{1,0},{2,3},{3,2},{4,5},{5,4},{6,7},{7,6},{8,9},{9,8},{10,11... | collective-permute-start | bytes 9224 | tf_op jit(solution)/shard_map/ppermute | solution.py:344
  13.1 15.8 %collective-permute-start.8 = (bf16[384,256]{1,0:T(8,128)(2,1)S(1)}, bf16[384,256]{1,0:T(8,128)(2,1)S(1)}, u32[]{:S(2)}, u32[]{:S(2)}) collective-permute-start(bf16[384,256]{1,0:T(8,128)(2,1)S(1)} %get-tuple-element.69), channel_id=1, source_target_pairs={{0,1},{1,0},{2,3},{3,2},{4,5},{5,4},{6,7},{7,6},{8,9},{9,8},{10,11... | collective-permute-start | bytes 589832 | tf_op jit(solution)/shard_map/ppermute | solution.py:344
  25.6 33.3 %collective-permute-start.3 = (bf16[1024,256]{1,0:T(8,128)(2,1)S(1)}, bf16[1024,256]{1,0:T(8,128)(2,1)}, u32[]{:S(2)}, u32[]{:S(2)}) collective-permute-start(bf16[1024,256]{1,0:T(8,128)(2,1)S(1)} %collective-permute-done.1.w1), channel_id=1, source_target_pairs={{0,2},{2,4},{4,6},{6,0},{1,3},{3,5},{5,7},{7,1},{8,10},{10,12},{12... | collective-permute-start | bytes 1572872 | tf_op jit(solution)/shard_map/ppermute | solution.py:410
  29.2 31.5 %collective-permute-start.11 = (bf16[784,256]{1,0:T(8,128)(2,1)S(1)}, bf16[784,256]{1,0:T(8,128)(2,1)}, u32[]{:S(2)}, u32[]{:S(2)}) collective-permute-start(bf16[784,256]{1,0:T(8,128)(2,1)S(1)} %concatenate.31.r0), channel_id=1, source_target_pairs={{0,6},{2,0},{4,2},{6,4},{1,7},{3,1},{5,3},{7,5},{8,14},{10,8},{12,... | collective-permute-start | bytes 1204232 | tf_op jit(solution)/shard_map/ppermute | solution.py:375
  51.0 29.0 %all-to-all-start.1 = ((bf16[8,384,128]{2,1,0:T(8,128)(2,1)}), bf16[8,384,128]{2,1,0:T(8,128)(2,1)S(1)}, u32[]{:S(2)}, u32[]{:S(2)}) async-start(bf16[8,384,128]{2,1,0:T(8,128)(2,1)} %shard_map.155), calls=%async_computation.1 | async-start | bytes 1572864 | tf_op jit(solution)/shard_map/all_to_all | solution.py:409
  58.4 21.6 %collective-permute-start.5 = (bf16[1024,256]{1,0:T(8,128)(2,1)S(1)}, bf16[1024,256]{1,0:T(8,128)(2,1)}, u32[]{:S(2)}, u32[]{:S(2)}) collective-permute-start(bf16[1024,256]{1,0:T(8,128)(2,1)S(1)} %collective-permute-done.1.w1), channel_id=1, source_target_pairs={{0,1},{1,0},{2,3},{3,2},{4,5},{5,4},{6,7},{7,6},{8,9},{9,8},{10,11... | collective-permute-start | bytes 1572872 | tf_op jit(solution)/shard_map/ppermute | solution.py:344
  58.6 21.4 %collective-permute-start.6 = (bf16[1024,256]{1,0:T(8,128)(2,1)S(1)}, bf16[1024,256]{1,0:T(8,128)(2,1)}, u32[]{:S(2)}, u32[]{:S(2)}) collective-permute-start(bf16[1024,256]{1,0:T(8,128)(2,1)S(1)} %collective-permute-done.2.w2), channel_id=1, source_target_pairs={{0,1},{1,0},{2,3},{3,2},{4,5},{5,4},{6,7},{7,6},{8,9},{9,8},{10,11... | collective-permute-start | bytes 1572872 | tf_op jit(solution)/shard_map/ppermute | solution.py:344
  58.9 21.1 %collective-permute-start.7 = (bf16[1024,256]{1,0:T(8,128)(2,1)}, bf16[1024,256]{1,0:T(8,128)(2,1)}, u32[]{:S(2)}, u32[]{:S(2)}) collective-permute-start(bf16[1024,256]{1,0:T(8,128)(2,1)} %collective-permute-done.3.w3), channel_id=1, source_target_pairs={{0,1},{1,0},{2,3},{3,2},{4,5},{5,4},{6,7},{7,6},{8,9},{9,8},{10,11... | collective-permute-start | bytes 1572872 | tf_op jit(solution)/shard_map/ppermute | solution.py:344
  59.1 20.1 %collective-permute-start.10 = (bf16[784,256]{1,0:T(8,128)(2,1)S(1)}, bf16[784,256]{1,0:T(8,128)(2,1)S(1)}, u32[]{:S(2)}, u32[]{:S(2)}) collective-permute-start(bf16[784,256]{1,0:T(8,128)(2,1)S(1)} %concatenate.31.r0), channel_id=1, source_target_pairs={{0,2},{2,4},{4,6},{6,0},{1,3},{3,5},{5,7},{7,1},{8,10},{10,12},{12... | collective-permute-start | bytes 1204232 | tf_op jit(solution)/shard_map/ppermute | solution.py:376
  60.7 19.3 %collective-permute-start.12 = (bf16[784,256]{1,0:T(8,128)(2,1)}, bf16[784,256]{1,0:T(8,128)(2,1)}, u32[]{:S(2)}, u32[]{:S(2)}) collective-permute-start(bf16[784,256]{1,0:T(8,128)(2,1)} %collective-permute-done.11.r2), channel_id=1, source_target_pairs={{0,6},{2,0},{4,2},{6,4},{1,7},{3,1},{5,3},{7,5},{8,14},{10,8},{12,... | collective-permute-start | bytes 1204232 | tf_op jit(solution)/shard_map/ppermute | solution.py:411
  98.6 11.1 %collective-permute-start.14 = (bf16[3,384,512]{2,1,0:T(8,128)(2,1)S(1)}, bf16[3,384,512]{2,1,0:T(8,128)(2,1)S(1)}, u32[]{:S(2)}, u32[]{:S(2)}) collective-permute-start(bf16[3,384,512]{2,1,0:T(8,128)(2,1)S(1)} %get-tuple-element.46), channel_id=1, source_target_pairs={{0,1},{1,0},{2,3},{3,2},{4,5},{5,4},{6,7},{7,6},{8,9},{9,8},{10,11... | collective-permute-start | bytes 3538952 | tf_op jit(solution)/shard_map/ppermute | solution.py:344
  102.3 7.4 %collective-permute-start.18 = (bf16[192,512]{1,0:T(8,128)(2,1)S(1)}, bf16[192,512]{1,0:T(8,128)(2,1)S(1)}, u32[]{:S(2)}, u32[]{:S(2)}) collective-permute-start(bf16[192,512]{1,0:T(8,128)(2,1)S(1)} %get-tuple-element.52), channel_id=1, source_target_pairs={{0,2},{2,4},{4,6},{6,0},{1,3},{3,5},{5,7},{7,1},{8,10},{10,12},{12... | collective-permute-start | bytes 589832 | tf_op jit(solution)/shard_map/ppermute | solution.py:452
  102.4 7.3 %collective-permute-start.19 = (bf16[192,512]{1,0:T(8,128)(2,1)S(1)}, bf16[192,512]{1,0:T(8,128)(2,1)S(1)}, u32[]{:S(2)}, u32[]{:S(2)}) collective-permute-start(bf16[192,512]{1,0:T(8,128)(2,1)S(1)} %get-tuple-element.53), channel_id=1, source_target_pairs={{0,6},{2,0},{4,2},{6,4},{1,7},{3,1},{5,3},{7,5},{8,14},{10,8},{12,... | collective-permute-start | bytes 589832 | tf_op jit(solution)/shard_map/ppermute | solution.py:453
  110.0 7.8 %collective-permute-start.20 = (bf16[192,512]{1,0:T(8,128)(2,1)S(1)}, bf16[192,512]{1,0:T(8,128)(2,1)S(1)}, u32[]{:S(2)}, u32[]{:S(2)}) collective-permute-start(bf16[192,512]{1,0:T(8,128)(2,1)S(1)} %get-tuple-element.58), channel_id=1, source_target_pairs={{0,2},{2,4},{4,6},{6,0},{1,3},{3,5},{5,7},{7,1},{8,10},{10,12},{12... | collective-permute-start | bytes 589832 | tf_op jit(solution)/shard_map/ppermute | solution.py:464
  110.1 7.7 %collective-permute-start.21 = (bf16[192,512]{1,0:T(8,128)(2,1)S(1)}, bf16[192,512]{1,0:T(8,128)(2,1)S(1)}, u32[]{:S(2)}, u32[]{:S(2)}) collective-permute-start(bf16[192,512]{1,0:T(8,128)(2,1)S(1)} %get-tuple-element.59), channel_id=1, source_target_pairs={{0,6},{2,0},{4,2},{6,4},{1,7},{3,1},{5,3},{7,5},{8,14},{10,8},{12,... | collective-permute-start | bytes 589832 | tf_op jit(solution)/shard_map/ppermute | solution.py:465
  112.8 8.1 %collective-permute-start.15 = (bf16[192,512]{1,0:T(8,128)(2,1)S(1)}, bf16[192,512]{1,0:T(8,128)(2,1)S(1)}, u32[]{:S(2)}, u32[]{:S(2)}) collective-permute-start(bf16[192,512]{1,0:T(8,128)(2,1)S(1)} %get-tuple-element.48), channel_id=1, source_target_pairs={{0,2},{2,4},{4,6},{6,0},{1,3},{3,5},{5,7},{7,1},{8,10},{10,12},{12... | collective-permute-start | bytes 589832 | tf_op jit(solution)/shard_map/ppermute | solution.py:460
  112.8 8.1 %collective-permute-start.16 = (bf16[192,512]{1,0:T(8,128)(2,1)S(1)}, bf16[192,512]{1,0:T(8,128)(2,1)S(1)}, u32[]{:S(2)}, u32[]{:S(2)}) collective-permute-start(bf16[192,512]{1,0:T(8,128)(2,1)S(1)} %get-tuple-element.49), channel_id=1, source_target_pairs={{0,6},{2,0},{4,2},{6,4},{1,7},{3,1},{5,3},{7,5},{8,14},{10,8},{12,... | collective-permute-start | bytes 589832 | tf_op jit(solution)/shard_map/ppermute | solution.py:461
  115.4 12.7 %collective-permute-start.23 = (bf16[384,256]{1,0:T(8,128)(2,1)S(1)}, bf16[384,256]{1,0:T(8,128)(2,1)S(1)}, u32[]{:S(2)}, u32[]{:S(2)}) collective-permute-start(bf16[384,256]{1,0:T(8,128)(2,1)S(1)} %copy-done.6), channel_id=1, source_target_pairs={{0,1},{1,0},{2,3},{3,2},{4,5},{5,4},{6,7},{7,6},{8,9},{9,8},{10,11... | collective-permute-start | bytes 589832 | tf_op jit(solution)/shard_map/ppermute | solution.py:344
  121.8 10.9 %collective-permute-start.22 = (bf16[384,256]{1,0:T(8,128)(2,1)S(1)}, bf16[384,256]{1,0:T(8,128)(2,1)S(1)}, u32[]{:S(2)}, u32[]{:S(2)}) collective-permute-start(bf16[384,256]{1,0:T(8,128)(2,1)S(1)} %get-tuple-element.65), channel_id=1, source_target_pairs={{0,1},{1,0},{2,3},{3,2},{4,5},{5,4},{6,7},{7,6},{8,9},{9,8},{10,11... | collective-permute-start | bytes 589832 | tf_op jit(solution)/shard_map/ppermute | solution.py:344
  123.8 9.0 %all-to-all-start.2 = ((f32[8,3,128]{2,1,0:T(4,128)}), f32[8,3,128]{2,1,0:T(4,128)S(1)}, u32[]{:S(2)}, u32[]{:S(2)}) async-start(f32[8,3,128]{2,1,0:T(4,128)} %get-tuple-element.68), calls=%async_computation.2 | async-start | bytes 32768 | tf_op jit(solution)/shard_map/all_to_all | solution.py:475
  (15 other events, 102.3 us)
Sparse Core Ops, SparseCore 0:
  9.5 75.3 all-gather.2

commit v6 on v5

--- a/solution.py
+++ b/solution.py
@@ -195,7 +195,7 @@
     return jnp.dot(lhs, part, preferred_element_type=F32).astype(BF)
 
 
-CUTS = ((0, 128), (128, 384), (384, 704))
+CUTS = ((0, 128), (128, 384), (384, 640), (640, 704))
 
 
 def hidden_part(src, gu, lo, hi):
@@ -287,15 +287,9 @@
         else:
             more = fl_ref[lo - q : lo - q + 64, :].astype(F32) + bot_ref[lo - q : lo - q + 64, :].astype(F32)
         v = (own_ref[at, :] + more).astype(BF)
-        for first, core in ((0, 0), (256, 1)):
-
-            @pl.when(c == core)
-            def _():
-                keep_ref[at, :] = v[:, first : first + 256]
-
-            @pl.when(c != core)
-            def _():
-                send_ref[at, :] = v[:, first : first + 256]
+        low, high = v[:, :256], v[:, 256:]
+        keep_ref[at, :] = jnp.where(c == 0, low, high)
+        send_ref[at, :] = jnp.where(c == 0, high, low)
 
     for k in range(2 * q // 128):
         t = jnp.zeros((128, 128), F32)

time: 141 us -> 141 us (level)
  no operation moved by 1% of the time
where the time goes in v6:
time: 141 us
  waiting for transfers between devices  42.7 us (30%)
  starting transfers between devices  40 us (28%)
  Pallas kernels  25.6 us (18%)
  blocking collectives  13.8 us (10%)
  between operations  13.7 us (10%)
  local copies, waits for them, and re-layouts  4.61 us (3%)
    ppermute x1, waiting for transfers between devices, steps(): res_left = lax.ppermute(res, 'x', cyc(4, 1))  17.2 us
    all_to_all x1, blocking collectives, steps(): all_ends = lax.all_to_all(ends, SP, 0, 0, tiled=True)  13.8 us
    ppermute x1, waiting for transfers between devices, steps(): out_left = lax.ppermute(out_weight, 'x', cyc(4, 1))  11.1 us
    ppermute x11, starting transfers between devices, swapped(): return lax.ppermute(block, 'c', cyc(2, 1))  7.84 us
    all_to_all x1, starting transfers between devices, steps(): branch = lax.all_to_all(branch, TP, 0, 0, tiled=True)  7.43 us
    pallas_call x1, Pallas kernels, steps(): call(first_kernel, [((half, 512), BF), ((3, half, 512), BF), ((16, 1408,...  6.67 us
    pallas_call x1, Pallas kernels, steps(): call(mix_kernel, [((half, 2048), BF)] * 2 + [((half, 256), BF)] * 2, [VM]...  5.57 us
    all_to_all x1, waiting for transfers between devices, steps(): square = lax.all_to_all(square, TP, 0, 0, tiled=True)  4.65 us
  transfers between devices with their start and end apart: 27, of which 6 were waited for; matrix products, arithmetic and copies ran while one was open for 1% of the time, Pallas kernels for 11%

profile of v6, /device:TPU:1, one launch (start us, length us, event | category | flops | bytes accessed | tf_op | source)
XLA Modules:
  0.0 140.6 jit_solution(12705792940127406270)
XLA Ops:
  6.6 1.9 %shard_map.157 = bf16[2112,128]{1,0:T(8,128)(2,1)} custom-call(bf16[704,128]{1,0:T(8,128)(2,1)} %bitcast.12, bf16[704,128]{1,0:T(8,128)(2,1)} %bitcast.13, bf16[704,128]{1,0:T(8,128)(2,1)} %d_ref.1), custom_call_target="tpu_custom_call" | custom-call | tf_op jit(solution)/shard_map/pallas_call | solution.py:349
  8.5 3.4 %collective-permute-start.2 = (bf16[1024,256]{1,0:T(8,128)(2,1)S(1)}, bf16[1024,256]{1,0:T(8,128)(2,1)S(1)}, u32[]{:S(2)}, u32[]{:S(2)}) collective-permute-start(bf16[1024,256]{1,0:T(8,128)(2,1)S(1)} %copy-done.1), channel_id=1, source_target_pairs={{0,6},{2,0},{4,2},{6,4},{1,7},{3,1},{5,3},{7,5},{8,14},{10,8},{12,... | collective-permute-start | bytes 1572872 | tf_op jit(solution)/shard_map/ppermute | solution.py:371
  14.5 11.1 %collective-permute-done.1.w1 = bf16[1024,256]{1,0:T(8,128)(2,1)S(1)} collective-permute-done((bf16[1024,256]{1,0:T(8,128)(2,1)S(1)}, bf16[1024,256]{1,0:T(8,128)(2,1)S(1)}, u32[]{:S(2)}, u32[]{:S(2)}) %collective-permute-start.1) | collective-permute-done | bytes 524320 | tf_op jit(solution)/shard_map/ppermute | solution.py:368
  25.6 3.2 %collective-permute-start = (f32[16,128]{1,0:T(8,128)S(1)}, f32[16,128]{1,0:T(8,128)S(1)}, u32[]{:S(2)}, u32[]{:S(2)}) collective-permute-start(f32[16,128]{1,0:T(8,128)S(1)} %pad_maximum_fusion), channel_id=1, source_target_pairs={{0,8},{8,16},{16,24},{24,32},{32,40},{40,48},{48,56},{56,64},{64,7... | collective-permute-start | bytes 24584 | tf_op jit(solution)/shard_map/ppermute | solution.py:377
  29.2 2.7 %collective-permute-start.11 = (bf16[784,256]{1,0:T(8,128)(2,1)S(1)}, bf16[784,256]{1,0:T(8,128)(2,1)}, u32[]{:S(2)}, u32[]{:S(2)}) collective-permute-start(bf16[784,256]{1,0:T(8,128)(2,1)S(1)} %concatenate.31.r0), channel_id=1, source_target_pairs={{0,6},{2,0},{4,2},{6,4},{1,7},{3,1},{5,3},{7,5},{8,14},{10,8},{12,... | collective-permute-start | bytes 1204232 | tf_op jit(solution)/shard_map/ppermute | solution.py:369
  31.9 3.1 %shard_map.154 = (f32[768,128]{1,0:T(8,128)S(1)}, f32[768,128]{1,0:T(8,128)S(1)}, f32[16,2,128]{2,1,0:T(2,128)S(1)}) custom-call(bf16[768,128]{1,0:T(8,128)(2,1)} %x_ref.1, f32[16,128]{1,0:T(8,128)S(1)} %collective-permute-done.rim_ref, f32[6,128]{1,0:T(8,128)S(1)} %convert_bitcast_fusion.ids_ref, bf16[4,128]{1,0:T(4,128)(2,1)} %taps_ref.1, ...), custom_call_target="tpu_custom_call" | custom-call | tf_op jit(solution)/shard_map/pallas_call | solution.py:381
  35.1 13.8 %all_to_all.15.e_ref = f32[16,2,128]{2,1,0:T(2,128)S(1)} all-to-all(f32[16,2,128]{2,1,0:T(2,128)S(1)} %get-tuple-element.39), channel_id=1, replica_groups=mesh['z'=4,'y'=4,'x'=4,'c'=2] {'z','y'}, dimensions={0} | all-to-all | bytes 32768 | tf_op jit(solution)/shard_map/all_to_all | solution.py:399
  48.9 2.1 %shard_map.155 = bf16[8,384,128]{2,1,0:T(8,128)(2,1)} custom-call(f32[768,128]{1,0:T(8,128)S(1)} %get-tuple-element.37.s_ref, f32[768,128]{1,0:T(8,128)S(1)} %get-tuple-element.38.p_ref, f32[16,2,128]{2,1,0:T(2,128)S(1)} %all_to_all.15.e_ref, bf16[768,128]{1,0:T(8,128)(2,1)} %g_ref.1), custom_call_target="tpu_custom_call" | custom-call | tf_op jit(solution)/shard_map/pallas_call | solution.py:400
  51.0 7.4 %all-to-all-start.1 = ((bf16[8,384,128]{2,1,0:T(8,128)(2,1)}), bf16[8,384,128]{2,1,0:T(8,128)(2,1)S(1)}, u32[]{:S(2)}, u32[]{:S(2)}) async-start(bf16[8,384,128]{2,1,0:T(8,128)(2,1)} %shard_map.155), calls=%async_computation.1 | async-start | bytes 1572864 | tf_op jit(solution)/shard_map/all_to_all | solution.py:403
  59.1 1.6 %collective-permute-start.10 = (bf16[784,256]{1,0:T(8,128)(2,1)S(1)}, bf16[784,256]{1,0:T(8,128)(2,1)S(1)}, u32[]{:S(2)}, u32[]{:S(2)}) collective-permute-start(bf16[784,256]{1,0:T(8,128)(2,1)S(1)} %concatenate.31.r0), channel_id=1, source_target_pairs={{0,2},{2,4},{4,6},{6,0},{1,3},{3,5},{5,7},{7,1},{8,10},{10,12},{12... | collective-permute-start | bytes 1204232 | tf_op jit(solution)/shard_map/ppermute | solution.py:370
  62.0 17.2 %collective-permute-done.10.r1 = bf16[784,256]{1,0:T(8,128)(2,1)S(1)} collective-permute-done((bf16[784,256]{1,0:T(8,128)(2,1)S(1)}, bf16[784,256]{1,0:T(8,128)(2,1)S(1)}, u32[]{:S(2)}, u32[]{:S(2)}) %collective-permute-start.10) | collective-permute-done | bytes 401440 | tf_op jit(solution)/shard_map/ppermute | solution.py:370
  81.0 5.6 %shard_map.156 = (bf16[384,2048]{1,0:T(8,128)(2,1)S(1)}, bf16[384,2048]{1,0:T(8,128)(2,1)S(1)}, bf16[384,256]{1,0:T(8,128)(2,1)S(1)}, bf16[384,256]{1,0:T(8,128)(2,1)S(1)}) custom-call(bf16[8,384,128]{2,1,0:T(8,128)(2,1)S(1)} %all-to-all-done.1.br_ref, bf16[1024,256]{1,0:T(8,128)(2,1)S(1)} %copy-done.1, bf16[1024,256]{1,0:T(8,128)(2,1)S(1)} %collective-permute-done.1.w1, ...), custom_call_target="tpu_custom_call" | custom-call | tf_op jit(solution)/shard_map/pallas_call | solution.py:410
  89.0 3.0 %collective-permute-done.13.n_ref = bf16[384,2048]{1,0:T(8,128)(2,1)S(1)} collective-permute-done((bf16[384,2048]{1,0:T(8,128)(2,1)S(1)}, bf16[384,2048]{1,0:T(8,128)(2,1)S(1)}, u32[]{:S(2)}, u32[]{:S(2)}) %collective-permute-start.13) | collective-permute-done | bytes 1572896 | tf_op jit(solution)/shard_map/ppermute | solution.py:338
  92.1 6.7 %shard_map.158 = (bf16[384,512]{1,0:T(8,128)(2,1)S(1)}, bf16[3,384,512]{2,1,0:T(8,128)(2,1)S(1)}, bf16[16,1408,128]{2,1,0:T(8,128)(2,1)S(1)}, bf16[16,704,128]{2,1,0:T(8,128)(2,1)S(1)}, bf16[384,2048]{1,0:T(8,128)(2,1)S(1)}) custom-call(bf16[384,2048]{1,0:T(8,128)(2,1)S(1)} %collective-permute-done.13.n_ref, bf16[384,2048]{1,0:T(8,128)(2,1)} %copy-done, ...), custom_call_target="tpu_custom_call" | custom-call | tf_op jit(solution)/shard_map/pallas_call | solution.py:425
  99.3 2.9 %shard_map.159 = (bf16[384,512]{1,0:T(8,128)(2,1)S(1)}, bf16[384,704]{1,0:T(8,128)(2,1)S(1)}) custom-call(bf16[384,2048]{1,0:T(8,128)(2,1)S(1)} %get-tuple-element.42.n_ref, bf16[16,1408,128]{2,1,0:T(8,128)(2,1)S(1)} %get-tuple-element.43.gu, bf16[16,704,128]{2,1,0:T(8,128)(2,1)S(1)} %get-tuple-element.44.dn), custom_call_target="tpu_custom_call" | custom-call | tf_op jit(solution)/shard_map/pallas_call | solution.py:440
  102.5 2.7 %collective-permute-start.19 = (bf16[192,512]{1,0:T(8,128)(2,1)S(1)}, bf16[192,512]{1,0:T(8,128)(2,1)S(1)}, u32[]{:S(2)}, u32[]{:S(2)}) collective-permute-start(bf16[192,512]{1,0:T(8,128)(2,1)S(1)} %get-tuple-element.53), channel_id=1, source_target_pairs={{0,6},{2,0},{4,2},{6,4},{1,7},{3,1},{5,3},{7,5},{8,14},{10,8},{12,... | collective-permute-start | bytes 589832 | tf_op jit(solution)/shard_map/ppermute | solution.py:447
  106.2 3.5 %collective-permute-done.18.r_ref = bf16[192,512]{1,0:T(8,128)(2,1)S(1)} collective-permute-done((bf16[192,512]{1,0:T(8,128)(2,1)S(1)}, bf16[192,512]{1,0:T(8,128)(2,1)S(1)}, u32[]{:S(2)}, u32[]{:S(2)}) %collective-permute-start.18) | collective-permute-done | bytes 196640 | tf_op jit(solution)/shard_map/ppermute | solution.py:446
  110.2 2.7 %collective-permute-start.21 = (bf16[192,512]{1,0:T(8,128)(2,1)S(1)}, bf16[192,512]{1,0:T(8,128)(2,1)S(1)}, u32[]{:S(2)}, u32[]{:S(2)}) collective-permute-start(bf16[192,512]{1,0:T(8,128)(2,1)S(1)} %get-tuple-element.59), channel_id=1, source_target_pairs={{0,6},{2,0},{4,2},{6,4},{1,7},{3,1},{5,3},{7,5},{8,14},{10,8},{12,... | collective-permute-start | bytes 589832 | tf_op jit(solution)/shard_map/ppermute | solution.py:459
  112.8 2.7 %collective-permute-start.16 = (bf16[192,512]{1,0:T(8,128)(2,1)S(1)}, bf16[192,512]{1,0:T(8,128)(2,1)S(1)}, u32[]{:S(2)}, u32[]{:S(2)}) collective-permute-start(bf16[192,512]{1,0:T(8,128)(2,1)S(1)} %get-tuple-element.49), channel_id=1, source_target_pairs={{0,6},{2,0},{4,2},{6,4},{1,7},{3,1},{5,3},{7,5},{8,14},{10,8},{12,... | collective-permute-start | bytes 589832 | tf_op jit(solution)/shard_map/ppermute | solution.py:455
  115.5 2.4 %collective-permute-start.23 = (bf16[384,256]{1,0:T(8,128)(2,1)S(1)}, bf16[384,256]{1,0:T(8,128)(2,1)S(1)}, u32[]{:S(2)}, u32[]{:S(2)}) collective-permute-start(bf16[384,256]{1,0:T(8,128)(2,1)S(1)} %copy-done.6), channel_id=1, source_target_pairs={{0,1},{1,0},{2,3},{3,2},{4,5},{5,4},{6,7},{7,6},{8,9},{9,8},{10,11... | collective-permute-start | bytes 589832 | tf_op jit(solution)/shard_map/ppermute | solution.py:338
  117.9 3.1 %collective-permute-done.15.fl_ref = bf16[192,512]{1,0:T(8,128)(2,1)S(1)} collective-permute-done((bf16[192,512]{1,0:T(8,128)(2,1)S(1)}, bf16[192,512]{1,0:T(8,128)(2,1)S(1)}, u32[]{:S(2)}, u32[]{:S(2)}) %collective-permute-start.15) | collective-permute-done | bytes 196640 | tf_op jit(solution)/shard_map/ppermute | solution.py:454
  121.9 1.9 %collective-permute-start.22 = (bf16[384,256]{1,0:T(8,128)(2,1)S(1)}, bf16[384,256]{1,0:T(8,128)(2,1)S(1)}, u32[]{:S(2)}, u32[]{:S(2)}) collective-permute-start(bf16[384,256]{1,0:T(8,128)(2,1)S(1)} %get-tuple-element.65), channel_id=1, source_target_pairs={{0,1},{1,0},{2,3},{3,2},{4,5},{5,4},{6,7},{7,6},{8,9},{9,8},{10,11... | collective-permute-start | bytes 589832 | tf_op jit(solution)/shard_map/ppermute | solution.py:338
  123.8 4.3 %all-to-all-start.2 = ((f32[8,3,128]{2,1,0:T(4,128)}), f32[8,3,128]{2,1,0:T(4,128)S(1)}, u32[]{:S(2)}, u32[]{:S(2)}) async-start(f32[8,3,128]{2,1,0:T(4,128)} %get-tuple-element.68), calls=%async_computation.2 | async-start | bytes 32768 | tf_op jit(solution)/shard_map/all_to_all | solution.py:469
  128.1 4.7 %all-to-all-done.2.sq_ref = f32[8,3,128]{2,1,0:T(4,128)S(1)} async-done(((f32[8,3,128]{2,1,0:T(4,128)}), f32[8,3,128]{2,1,0:T(4,128)S(1)}, u32[]{:S(2)}, u32[]{:S(2)}) %all-to-all-start.2) | async-done | bytes 12320 | tf_op jit(solution)/shard_map/all_to_all | solution.py:469
  (82 shorter events, 13.4 us)
Async XLA Ops:
  6.5 85.5 %all-gather.3.cloned.1.call-start = ((), (), s32[]{:S(2)}) async-start(), calls=%async_computation.3 | async-start | bytes 9191424 | tf_op jit(solution)/shard_map/all_gather | solution.py:356
  8.5 50.0 %collective-permute-start.2 = (bf16[1024,256]{1,0:T(8,128)(2,1)S(1)}, bf16[1024,256]{1,0:T(8,128)(2,1)S(1)}, u32[]{:S(2)}, u32[]{:S(2)}) collective-permute-start(bf16[1024,256]{1,0:T(8,128)(2,1)S(1)} %copy-done.1), channel_id=1, source_target_pairs={{0,6},{2,0},{4,2},{6,4},{1,7},{3,1},{5,3},{7,5},{8,14},{10,8},{12,... | collective-permute-start | bytes 1572872 | tf_op jit(solution)/shard_map/ppermute | solution.py:371
  11.9 13.7 %collective-permute-start.1 = (bf16[1024,256]{1,0:T(8,128)(2,1)S(1)}, bf16[1024,256]{1,0:T(8,128)(2,1)S(1)}, u32[]{:S(2)}, u32[]{:S(2)}) collective-permute-start(bf16[1024,256]{1,0:T(8,128)(2,1)S(1)} %copy-done.1), channel_id=1, source_target_pairs={{0,2},{2,4},{4,6},{6,0},{1,3},{3,5},{5,7},{7,1},{8,10},{10,12},{12... | collective-permute-start | bytes 1572872 | tf_op jit(solution)/shard_map/ppermute | solution.py:368
  11.9 47.2 %collective-permute-start.4 = (bf16[1024,256]{1,0:T(8,128)(2,1)S(1)}, bf16[1024,256]{1,0:T(8,128)(2,1)S(1)}, u32[]{:S(2)}, u32[]{:S(2)}) collective-permute-start(bf16[1024,256]{1,0:T(8,128)(2,1)S(1)} %copy-done.1), channel_id=1, source_target_pairs={{0,1},{1,0},{2,3},{3,2},{4,5},{5,4},{6,7},{7,6},{8,9},{9,8},{10,11... | collective-permute-start | bytes 1572872 | tf_op jit(solution)/shard_map/ppermute | solution.py:338
  12.9 12.7 %collective-permute-start.9 = (bf16[6,256]{1,0:T(8,128)(2,1)S(1)}, bf16[6,256]{1,0:T(8,128)(2,1)S(1)}, u32[]{:S(2)}, u32[]{:S(2)}) collective-permute-start(bf16[6,256]{1,0:T(8,128)(2,1)S(1)} %convert_element_type.16), channel_id=1, source_target_pairs={{0,1},{1,0},{2,3},{3,2},{4,5},{5,4},{6,7},{7,6},{8,9},{9,8},{10,11... | collective-permute-start | bytes 9224 | tf_op jit(solution)/shard_map/ppermute | solution.py:338
  13.1 15.8 %collective-permute-start.8 = (bf16[384,256]{1,0:T(8,128)(2,1)S(1)}, bf16[384,256]{1,0:T(8,128)(2,1)S(1)}, u32[]{:S(2)}, u32[]{:S(2)}) collective-permute-start(bf16[384,256]{1,0:T(8,128)(2,1)S(1)} %get-tuple-element.69), channel_id=1, source_target_pairs={{0,1},{1,0},{2,3},{3,2},{4,5},{5,4},{6,7},{7,6},{8,9},{9,8},{10,11... | collective-permute-start | bytes 589832 | tf_op jit(solution)/shard_map/ppermute | solution.py:338
  25.6 33.3 %collective-permute-start.3 = (bf16[1024,256]{1,0:T(8,128)(2,1)S(1)}, bf16[1024,256]{1,0:T(8,128)(2,1)}, u32[]{:S(2)}, u32[]{:S(2)}) collective-permute-start(bf16[1024,256]{1,0:T(8,128)(2,1)S(1)} %collective-permute-done.1.w1), channel_id=1, source_target_pairs={{0,2},{2,4},{4,6},{6,0},{1,3},{3,5},{5,7},{7,1},{8,10},{10,12},{12... | collective-permute-start | bytes 1572872 | tf_op jit(solution)/shard_map/ppermute | solution.py:404
  29.2 31.5 %collective-permute-start.11 = (bf16[784,256]{1,0:T(8,128)(2,1)S(1)}, bf16[784,256]{1,0:T(8,128)(2,1)}, u32[]{:S(2)}, u32[]{:S(2)}) collective-permute-start(bf16[784,256]{1,0:T(8,128)(2,1)S(1)} %concatenate.31.r0), channel_id=1, source_target_pairs={{0,6},{2,0},{4,2},{6,4},{1,7},{3,1},{5,3},{7,5},{8,14},{10,8},{12,... | collective-permute-start | bytes 1204232 | tf_op jit(solution)/shard_map/ppermute | solution.py:369
  51.0 29.0 %all-to-all-start.1 = ((bf16[8,384,128]{2,1,0:T(8,128)(2,1)}), bf16[8,384,128]{2,1,0:T(8,128)(2,1)S(1)}, u32[]{:S(2)}, u32[]{:S(2)}) async-start(bf16[8,384,128]{2,1,0:T(8,128)(2,1)} %shard_map.155), calls=%async_computation.1 | async-start | bytes 1572864 | tf_op jit(solution)/shard_map/all_to_all | solution.py:403
  58.4 21.6 %collective-permute-start.5 = (bf16[1024,256]{1,0:T(8,128)(2,1)S(1)}, bf16[1024,256]{1,0:T(8,128)(2,1)}, u32[]{:S(2)}, u32[]{:S(2)}) collective-permute-start(bf16[1024,256]{1,0:T(8,128)(2,1)S(1)} %collective-permute-done.1.w1), channel_id=1, source_target_pairs={{0,1},{1,0},{2,3},{3,2},{4,5},{5,4},{6,7},{7,6},{8,9},{9,8},{10,11... | collective-permute-start | bytes 1572872 | tf_op jit(solution)/shard_map/ppermute | solution.py:338
  58.6 21.4 %collective-permute-start.6 = (bf16[1024,256]{1,0:T(8,128)(2,1)S(1)}, bf16[1024,256]{1,0:T(8,128)(2,1)}, u32[]{:S(2)}, u32[]{:S(2)}) collective-permute-start(bf16[1024,256]{1,0:T(8,128)(2,1)S(1)} %collective-permute-done.2.w2), channel_id=1, source_target_pairs={{0,1},{1,0},{2,3},{3,2},{4,5},{5,4},{6,7},{7,6},{8,9},{9,8},{10,11... | collective-permute-start | bytes 1572872 | tf_op jit(solution)/shard_map/ppermute | solution.py:338
  58.9 21.1 %collective-permute-start.7 = (bf16[1024,256]{1,0:T(8,128)(2,1)}, bf16[1024,256]{1,0:T(8,128)(2,1)}, u32[]{:S(2)}, u32[]{:S(2)}) collective-permute-start(bf16[1024,256]{1,0:T(8,128)(2,1)} %collective-permute-done.3.w3), channel_id=1, source_target_pairs={{0,1},{1,0},{2,3},{3,2},{4,5},{5,4},{6,7},{7,6},{8,9},{9,8},{10,11... | collective-permute-start | bytes 1572872 | tf_op jit(solution)/shard_map/ppermute | solution.py:338
  59.1 20.1 %collective-permute-start.10 = (bf16[784,256]{1,0:T(8,128)(2,1)S(1)}, bf16[784,256]{1,0:T(8,128)(2,1)S(1)}, u32[]{:S(2)}, u32[]{:S(2)}) collective-permute-start(bf16[784,256]{1,0:T(8,128)(2,1)S(1)} %concatenate.31.r0), channel_id=1, source_target_pairs={{0,2},{2,4},{4,6},{6,0},{1,3},{3,5},{5,7},{7,1},{8,10},{10,12},{12... | collective-permute-start | bytes 1204232 | tf_op jit(solution)/shard_map/ppermute | solution.py:370
  60.7 19.3 %collective-permute-start.12 = (bf16[784,256]{1,0:T(8,128)(2,1)}, bf16[784,256]{1,0:T(8,128)(2,1)}, u32[]{:S(2)}, u32[]{:S(2)}) collective-permute-start(bf16[784,256]{1,0:T(8,128)(2,1)} %collective-permute-done.11.r2), channel_id=1, source_target_pairs={{0,6},{2,0},{4,2},{6,4},{1,7},{3,1},{5,3},{7,5},{8,14},{10,8},{12,... | collective-permute-start | bytes 1204232 | tf_op jit(solution)/shard_map/ppermute | solution.py:405
  98.7 11.0 %collective-permute-start.14 = (bf16[3,384,512]{2,1,0:T(8,128)(2,1)S(1)}, bf16[3,384,512]{2,1,0:T(8,128)(2,1)S(1)}, u32[]{:S(2)}, u32[]{:S(2)}) collective-permute-start(bf16[3,384,512]{2,1,0:T(8,128)(2,1)S(1)} %get-tuple-element.46), channel_id=1, source_target_pairs={{0,1},{1,0},{2,3},{3,2},{4,5},{5,4},{6,7},{7,6},{8,9},{9,8},{10,11... | collective-permute-start | bytes 3538952 | tf_op jit(solution)/shard_map/ppermute | solution.py:338
  102.4 7.4 %collective-permute-start.18 = (bf16[192,512]{1,0:T(8,128)(2,1)S(1)}, bf16[192,512]{1,0:T(8,128)(2,1)S(1)}, u32[]{:S(2)}, u32[]{:S(2)}) collective-permute-start(bf16[192,512]{1,0:T(8,128)(2,1)S(1)} %get-tuple-element.52), channel_id=1, source_target_pairs={{0,2},{2,4},{4,6},{6,0},{1,3},{3,5},{5,7},{7,1},{8,10},{10,12},{12... | collective-permute-start | bytes 589832 | tf_op jit(solution)/shard_map/ppermute | solution.py:446
  102.5 7.3 %collective-permute-start.19 = (bf16[192,512]{1,0:T(8,128)(2,1)S(1)}, bf16[192,512]{1,0:T(8,128)(2,1)S(1)}, u32[]{:S(2)}, u32[]{:S(2)}) collective-permute-start(bf16[192,512]{1,0:T(8,128)(2,1)S(1)} %get-tuple-element.53), channel_id=1, source_target_pairs={{0,6},{2,0},{4,2},{6,4},{1,7},{3,1},{5,3},{7,5},{8,14},{10,8},{12,... | collective-permute-start | bytes 589832 | tf_op jit(solution)/shard_map/ppermute | solution.py:447
  110.1 7.8 %collective-permute-start.20 = (bf16[192,512]{1,0:T(8,128)(2,1)S(1)}, bf16[192,512]{1,0:T(8,128)(2,1)S(1)}, u32[]{:S(2)}, u32[]{:S(2)}) collective-permute-start(bf16[192,512]{1,0:T(8,128)(2,1)S(1)} %get-tuple-element.58), channel_id=1, source_target_pairs={{0,2},{2,4},{4,6},{6,0},{1,3},{3,5},{5,7},{7,1},{8,10},{10,12},{12... | collective-permute-start | bytes 589832 | tf_op jit(solution)/shard_map/ppermute | solution.py:458
  110.2 7.7 %collective-permute-start.21 = (bf16[192,512]{1,0:T(8,128)(2,1)S(1)}, bf16[192,512]{1,0:T(8,128)(2,1)S(1)}, u32[]{:S(2)}, u32[]{:S(2)}) collective-permute-start(bf16[192,512]{1,0:T(8,128)(2,1)S(1)} %get-tuple-element.59), channel_id=1, source_target_pairs={{0,6},{2,0},{4,2},{6,4},{1,7},{3,1},{5,3},{7,5},{8,14},{10,8},{12,... | collective-permute-start | bytes 589832 | tf_op jit(solution)/shard_map/ppermute | solution.py:459
  112.8 8.1 %collective-permute-start.15 = (bf16[192,512]{1,0:T(8,128)(2,1)S(1)}, bf16[192,512]{1,0:T(8,128)(2,1)S(1)}, u32[]{:S(2)}, u32[]{:S(2)}) collective-permute-start(bf16[192,512]{1,0:T(8,128)(2,1)S(1)} %get-tuple-element.48), channel_id=1, source_target_pairs={{0,2},{2,4},{4,6},{6,0},{1,3},{3,5},{5,7},{7,1},{8,10},{10,12},{12... | collective-permute-start | bytes 589832 | tf_op jit(solution)/shard_map/ppermute | solution.py:454
  112.8 8.1 %collective-permute-start.16 = (bf16[192,512]{1,0:T(8,128)(2,1)S(1)}, bf16[192,512]{1,0:T(8,128)(2,1)S(1)}, u32[]{:S(2)}, u32[]{:S(2)}) collective-permute-start(bf16[192,512]{1,0:T(8,128)(2,1)S(1)} %get-tuple-element.49), channel_id=1, source_target_pairs={{0,6},{2,0},{4,2},{6,4},{1,7},{3,1},{5,3},{7,5},{8,14},{10,8},{12,... | collective-permute-start | bytes 589832 | tf_op jit(solution)/shard_map/ppermute | solution.py:455
  115.5 12.6 %collective-permute-start.23 = (bf16[384,256]{1,0:T(8,128)(2,1)S(1)}, bf16[384,256]{1,0:T(8,128)(2,1)S(1)}, u32[]{:S(2)}, u32[]{:S(2)}) collective-permute-start(bf16[384,256]{1,0:T(8,128)(2,1)S(1)} %copy-done.6), channel_id=1, source_target_pairs={{0,1},{1,0},{2,3},{3,2},{4,5},{5,4},{6,7},{7,6},{8,9},{9,8},{10,11... | collective-permute-start | bytes 589832 | tf_op jit(solution)/shard_map/ppermute | solution.py:338
  121.9 10.9 %collective-permute-start.22 = (bf16[384,256]{1,0:T(8,128)(2,1)S(1)}, bf16[384,256]{1,0:T(8,128)(2,1)S(1)}, u32[]{:S(2)}, u32[]{:S(2)}) collective-permute-start(bf16[384,256]{1,0:T(8,128)(2,1)S(1)} %get-tuple-element.65), channel_id=1, source_target_pairs={{0,1},{1,0},{2,3},{3,2},{4,5},{5,4},{6,7},{7,6},{8,9},{9,8},{10,11... | collective-permute-start | bytes 589832 | tf_op jit(solution)/shard_map/ppermute | solution.py:338
  123.8 9.0 %all-to-all-start.2 = ((f32[8,3,128]{2,1,0:T(4,128)}), f32[8,3,128]{2,1,0:T(4,128)S(1)}, u32[]{:S(2)}, u32[]{:S(2)}) async-start(f32[8,3,128]{2,1,0:T(4,128)} %get-tuple-element.68), calls=%async_computation.2 | async-start | bytes 32768 | tf_op jit(solution)/shard_map/all_to_all | solution.py:469
  (15 other events, 102.2 us)
Sparse Core Ops, SparseCore 0:
  9.5 75.3 all-gather.2
